TPU v7x, 512 devices: a whole 4x4x16 slice. The times are simulated.
512 devices in a mesh: sp: 64 (over z, y), tp: 8 (over x, core).
Axes of the slice: x: 4, y: 4, z: 16, core: 2. Of those that a mesh axis runs over, the one named last changes fastest.
Arguments:
- query_heads: bfloat16 [8192, 1024], P('sp', 'tp'), may hold values from -12 to 12
- key_heads: bfloat16 [8192, 1024], P('sp', 'tp'), may hold values from -6 to 6
- value_heads: bfloat16 [8192, 1024], P('sp', 'tp'), may hold values from -6 to 6
- decay_sums: float32 [8192, 8], P('sp', 'tp'), may hold values from -1346 to 0, as said below
- row_logsums: float32 [8192, 8], P('sp', 'tp'), may hold values from -9216 to 17408
- head_outputs: bfloat16 [8192, 1024], P('sp', 'tp'), may hold values from -1.796875 to 1.796875
- out_cotangent: bfloat16 [8192, 1024], P('sp', 'tp'), may hold values from -64 to 64
- normed_input: bfloat16 [8192, 2048], P('sp', 'tp'), may hold values from -16 to 16
Outputs:
- query_grads: bfloat16 [8192, 1024], P('sp', 'tp')
- key_grads: bfloat16 [8192, 1024], P('sp', 'tp')
- value_grads: bfloat16 [8192, 1024], P('sp', 'tp')
- weight_grad: float32 [2048, 1024], P('sp', 'tp')
Inputs may be any that keep to these rules, and one draw needn't show every extreme that they name: `decay_sums`: each head's values never rise along the positions.
All inputs are finite; a program needn't handle non-finite values.
Results may differ from a plain program's by a relative error of at most 0.005.
Values may be sent and summed in bfloat16 or wider, within the bound.
No kernel may reach another device: no remote copies, remote signals or barrier semaphores. Data moves between devices by JAX's collectives and lax.ppermute only.
A program may use at most 64 MiB of HBM per device.

v0:
```python
import jax
import jax.numpy as jnp
from jax import lax
from jax.sharding import Mesh
from jax.sharding import PartitionSpec as P

TP = ("tp_0", "tp_1")


def in_one_piece(arrays, axis, dim, along):
    ends, at = ([], 0)
    for a in arrays[:-1]:
        at += a.shape[along]
        ends.append(at)
    both = jnp.concatenate(arrays, axis=along)
    return tuple(jnp.split(lax.all_gather(both, axis, axis=dim, tiled=True), ends, axis=along))


def edges_of(length, count):
    turn = length // count
    if turn >= 8:
        turn -= turn % 8
    return [turn * k for k in range(1, count)]


def gather_in_order(shard, axes, order):
    parts = shard[None]
    for k in order:
        parts = lax.all_gather(parts, axes[k], axis=0, tiled=True)
    block = [lax.axis_size(axes[k]) for k in reversed(order)]
    parts = parts.reshape(*block, *shard.shape)
    turned = sorted(range(len(order)), key=lambda place: order[len(order) - 1 - place])
    return parts.transpose(*turned, *range(len(order), parts.ndim)).reshape(-1, *shard.shape)


def in_order(parts, dim):
    parts = jnp.moveaxis(parts, 0, dim)
    shape = parts.shape
    return parts.reshape(*shape[:dim], shape[dim] * shape[dim + 1], *shape[dim + 2 :])


def spread_gather(shard, axes, dim):
    cut = max(range(max(1, shard.ndim - 1)), key=lambda d: shard.shape[d])
    count, gathered = (len(axes), [])
    for first, section in enumerate(jnp.split(shard, edges_of(shard.shape[cut], count), axis=cut)):
        if section.size:
            order = [(first - k) % count for k in range(count)]
            gathered.append(gather_in_order(section, axes, order))
    return in_order(jnp.concatenate(gathered, axis=cut + 1), dim)


def in_blocks(shard, dim, devices):
    before, after = (shard.shape[:dim], shard.shape[dim + 1 :])
    return jnp.moveaxis(shard.reshape(*before, devices, -1, *after), dim, 0)


def summed_on_arrival(shard, axis, dim):
    devices = lax.axis_size(axis)
    parts = lax.all_to_all(in_blocks(shard, dim, devices), axis, 0, 0, tiled=True)
    return jnp.sum(parts, axis=0)


def block_length(whole_rows):
    length = whole_rows
    while length > 1024 and length % 2 == 0:
        length = length // 2
    return length


def split_heads(block, head_count):
    return block.reshape(block.shape[0], head_count, block.shape[1] // head_count)


def attention_weights(
    query_part, key_part, norm_part, gate_query, gate_key, query_pos, key_pos, score_scale
):
    scores = (
        jnp.einsum("ahd,bhd->hab", query_part, key_part, preferred_element_type=jnp.float32)
        * score_scale
    )
    scores = scores + (gate_query.T[:, :, None] - gate_key.T[:, None, :])
    allowed = key_pos[None, None, :] <= query_pos[None, :, None]
    return jnp.exp(jnp.where(allowed, scores - norm_part.T[:, :, None], -jnp.inf))


def score_slopes(weights, grad_part, value_part, term_part):
    flows = jnp.einsum("ahd,bhd->hab", grad_part, value_part, preferred_element_type=jnp.float32)
    return weights * (flows - term_part.T[:, :, None])


def over_blocks(visit_block, running, members):
    whole_rows = members[0].shape[0]
    length = block_length(whole_rows)
    number = whole_rows // length
    stacked = tuple((member.reshape((number, length) + member.shape[1:]) for member in members))

    def visit_one(carried, scanned):
        block_index, block_parts = scanned
        token_places = block_index * length + jnp.arange(length, dtype=jnp.int32)
        return (visit_block(carried, block_parts, token_places), None)

    result, unused = lax.scan(visit_one, running, (jnp.arange(number, dtype=jnp.int32), stacked))
    return result


def per_device(
    query_heads,
    key_heads,
    value_heads,
    decay_sums,
    row_logsums,
    head_outputs,
    out_cotangent,
    normed_input,
):
    own_rows, row_width = query_heads.shape
    head_count = decay_sums.shape[1]
    score_scale = (row_width // head_count) ** (-0.5)
    own_pos = lax.axis_index("sp") * own_rows + jnp.arange(own_rows, dtype=jnp.int32)
    own_query = split_heads(query_heads, head_count)
    own_key = split_heads(key_heads, head_count)
    own_value = split_heads(value_heads, head_count)
    own_grad = split_heads(out_cotangent, head_count)
    row_terms = jnp.einsum(
        "ahd,ahd->ah",
        split_heads(head_outputs, head_count),
        own_grad,
        preferred_element_type=jnp.float32,
    )
    all_gates, all_logsums, all_terms = in_one_piece(
        (decay_sums, row_logsums, row_terms), "sp", 0, 1
    )

    def query_side(query_sum, key_part, value_part, key_pos):
        gate_key = lax.dynamic_slice_in_dim(all_gates, key_pos[0], key_pos.shape[0], 0)

        def query_compute(running):
            weights = attention_weights(
                own_query,
                key_part,
                row_logsums,
                decay_sums,
                gate_key,
                own_pos,
                key_pos,
                score_scale,
            )
            slopes = score_slopes(weights, own_grad, value_part, row_terms)
            return running + jnp.einsum(
                "hab,bhd->ahd",
                slopes.astype(jnp.bfloat16),
                key_part,
                preferred_element_type=jnp.float32,
            )

        return lax.cond(
            key_pos[0] <= own_pos[-1], query_compute, lambda running: running, query_sum
        )

    def key_side(key_sums, query_part, grad_part, query_pos):
        length = query_pos.shape[0]
        gate_query = lax.dynamic_slice_in_dim(all_gates, query_pos[0], length, 0)
        norm_part = lax.dynamic_slice_in_dim(all_logsums, query_pos[0], length, 0)
        term_part = lax.dynamic_slice_in_dim(all_terms, query_pos[0], length, 0)

        def key_compute(running):
            key_sum, value_sum = running
            weights = attention_weights(
                query_part,
                own_key,
                norm_part,
                gate_query,
                decay_sums,
                query_pos,
                own_pos,
                score_scale,
            )
            slopes = score_slopes(weights, grad_part, own_value, term_part)
            key_sum = key_sum + jnp.einsum(
                "hab,ahd->bhd",
                slopes.astype(jnp.bfloat16),
                query_part,
                preferred_element_type=jnp.float32,
            )
            value_sum = value_sum + jnp.einsum(
                "hab,ahd->bhd",
                weights.astype(jnp.bfloat16),
                grad_part,
                preferred_element_type=jnp.float32,
            )
            return (key_sum, value_sum)

        return lax.cond(query_pos[-1] >= own_pos[0], key_compute, lambda running: running, key_sums)

    zero_sums = jnp.zeros((own_rows, head_count, row_width // head_count), jnp.float32)

    def visit_block(carried, block_parts, token_places):
        query_sum = query_side(
            carried[0],
            split_heads(block_parts[0], head_count),
            split_heads(block_parts[1], head_count),
            token_places,
        )
        key_sum, value_sum = key_side(
            (carried[1], carried[2]),
            split_heads(block_parts[2], head_count),
            split_heads(block_parts[3], head_count),
            token_places,
        )
        return (query_sum, key_sum, value_sum)

    query_sum, key_sum, value_sum = over_blocks(
        visit_block,
        (zero_sums, zero_sums, zero_sums),
        in_one_piece((key_heads, value_heads, query_heads, out_cotangent), "sp", 0, 1),
    )
    query_grads = (query_sum * score_scale).astype(jnp.bfloat16).reshape(own_rows, row_width)
    key_grads = (key_sum * score_scale).astype(jnp.bfloat16).reshape(own_rows, row_width)
    value_grads = value_sum.astype(jnp.bfloat16).reshape(own_rows, row_width)
    whole_input = spread_gather(normed_input, TP, 1)
    weight_grad = summed_on_arrival(
        lax.dot_general(
            whole_input, query_grads, (((0,), (0,)), ((), ())), preferred_element_type=jnp.float32
        ),
        "sp",
        0,
    )
    return (query_grads, key_grads, value_grads, weight_grad)


def solution(mesh):
    finer = Mesh(mesh.devices.reshape(mesh.shape["sp"], 4, 2), ("sp", "tp_0", "tp_1"))
    in_specs = (
        P("sp", TP),
        P("sp", TP),
        P("sp", TP),
        P("sp", TP),
        P("sp", TP),
        P("sp", TP),
        P("sp", TP),
        P("sp", TP),
    )
    out_specs = (P("sp", TP), P("sp", TP), P("sp", TP), P("sp", TP))
    return jax.shard_map(
        per_device, mesh=finer, in_specs=in_specs, out_specs=out_specs, check_vma=False
    )
```

profile of v0, /device:TPU:6, one launch (start us, length us, event | category | flops | bytes accessed | tf_op | source)
XLA Modules:
  0.0 321.9 jit_solution(6763742555694524463)
XLA Ops:
  7.2 1.5 pad_maximum_fusion.1
  9.5 14.6 %all-gather = bf16[256,256]{1,0:T(8,128)(2,1)S(1)} all-gather(bf16[64,256]{1,0:T(8,128)(2,1)S(1)} %get-tuple-element.388), channel_id=2, replica_groups=mesh['sp'=64,'tp_0'=4,'tp_1'=2] {'tp_0'}, dimensions={0}, use_global_device_ids=true | all-gather | bytes 163840 | tf_op jit(solution)/shard_map/all_gather | solution.py:29
  24.1 2.0 all_gather.21
  26.4 1.9 all-gather.1
  28.2 12.2 %all_gather.23 = bf16[8,64,256]{2,1,0:T(8,128)(2,1)S(1)} all-gather(bf16[2,64,256]{2,1,0:T(8,128)(2,1)S(1)} %bitcast.136), channel_id=1, replica_groups=mesh['sp'=64,'tp_0'=4,'tp_1'=2] {'tp_0'}, dimensions={0}, use_global_device_ids=true | all-gather | bytes 327680 | tf_op jit(solution)/shard_map/all_gather | solution.py:29
  41.6 104.4 %all_gather.18 = f32[8192,3]{0,1:T(4,128)S(1)} all-gather(f32[128,3]{0,1:T(4,128)S(1)} %pad_maximum_fusion.2), channel_id=1, replica_groups=mesh['sp'=64,'tp_0'=4,'tp_1'=2] {'sp'}, dimensions={0}, use_global_device_ids=true | all-gather | bytes 99840 | tf_op jit(solution)/shard_map/all_gather | solution.py:16
  146.4 25.1 %all-gather.4.cloned.1.call-done = bf16[8192,512]{1,0:T(8,128)(2,1)} async-done(((bf16[128,512]{1,0:T(8,128)(2,1)}), bf16[8192,512]{1,0:T(8,128)(2,1)}) %all-gather.4.cloned.1.call-update) | async-done | bytes 8388624 | tf_op jit(solution)/shard_map/all_gather | solution.py:16
  171.6 6.0 %fusion.71 = (bf16[8192,128]{1,0:T(8,128)(2,1)S(1)}, bf16[8192,128]{1,0:T(8,128)(2,1)}, bf16[8192,128]{1,0:T(8,128)(2,1)}, bf16[8192,128]{1,0:T(8,128)(2,1)}) fusion(bf16[8192,512]{1,0:T(8,128)(2,1)} %all-gather.4.cloned.1.call-done), kind=kLoop, calls=%fused_computation.80 | loop fusion | bytes 16777216 | tf_op jit(solution)/shard_map/split | solution.py:16
  177.6 80.3 %while.17 = (s32[]{:T(128)}, f32[128,1,128]{0,2,1:T(8,128)S(1)}, f32[128,1,128]{0,2,1:T(8,128)S(1)}, f32[128,1,128]{0,2,1:T(8,128)S(1)}, s32[8]{0:T(128)S(1)}, /...) while((s32[]{:T(128)}, f32[128,1,128]{0,2,1:T(8,128)S(1)}, ...), condition=%wide.region_5.6_spmd, body=%wide.region_0.5_spmd.sunk | while | flops 237421568 | bytes 5041043 | solution.py:102
  182.8 3.3 %conditional.5 = ((f32[128,1,128]{0,2,1:T(8,128)S(1)}, f32[128,1,128]{0,2,1:T(8,128)S(1)})) conditional(s32[]{:T(128)} %bitcast.124, (f32[128,1,128]{0,2,1:T(8,128)S(1)}, f32[128,1,128]{0,2,1:T(8,128)S(1)}) %tuple.61, (bf16[8,1024,128]{2,1,0:T(8,128)(2,1)}, s32[]{:T(128)}, s32[128]{0:T(128)S(1)}, s32[1024]{0:T(1024)S(1)}, ...), branch_computations={%region_3.3_spmd, %region_4.4_spmd} | conditional | flops 135561216 | bytes 2984480 | solution.py:193
  182.9 1.5 fusion.37
  187.3 2.8 conditional.4
  188.5 1.6 fusion.10
  195.3 3.3 %conditional.5 = ((f32[128,1,128]{0,2,1:T(8,128)S(1)}, f32[128,1,128]{0,2,1:T(8,128)S(1)})) conditional(s32[]{:T(128)} %bitcast.124, (f32[128,1,128]{0,2,1:T(8,128)S(1)}, f32[128,1,128]{0,2,1:T(8,128)S(1)}) %tuple.61, (bf16[8,1024,128]{2,1,0:T(8,128)(2,1)}, s32[]{:T(128)}, s32[128]{0:T(128)S(1)}, s32[1024]{0:T(1024)S(1)}, ...), branch_computations={%region_3.3_spmd, %region_4.4_spmd} | conditional | flops 135561216 | bytes 2984480 | solution.py:193
  195.4 1.5 fusion.37
  196.8 1.4 fusion.43
  205.0 3.3 %conditional.5 = ((f32[128,1,128]{0,2,1:T(8,128)S(1)}, f32[128,1,128]{0,2,1:T(8,128)S(1)})) conditional(s32[]{:T(128)} %bitcast.124, (f32[128,1,128]{0,2,1:T(8,128)S(1)}, f32[128,1,128]{0,2,1:T(8,128)S(1)}) %tuple.61, (bf16[8,1024,128]{2,1,0:T(8,128)(2,1)}, s32[]{:T(128)}, s32[128]{0:T(128)S(1)}, s32[1024]{0:T(1024)S(1)}, ...), branch_computations={%region_3.3_spmd, %region_4.4_spmd} | conditional | flops 135561216 | bytes 2984480 | solution.py:193
  205.1 1.5 fusion.37
  206.5 1.4 fusion.43
  214.6 3.3 %conditional.5 = ((f32[128,1,128]{0,2,1:T(8,128)S(1)}, f32[128,1,128]{0,2,1:T(8,128)S(1)})) conditional(s32[]{:T(128)} %bitcast.124, (f32[128,1,128]{0,2,1:T(8,128)S(1)}, f32[128,1,128]{0,2,1:T(8,128)S(1)}) %tuple.61, (bf16[8,1024,128]{2,1,0:T(8,128)(2,1)}, s32[]{:T(128)}, s32[128]{0:T(128)S(1)}, s32[1024]{0:T(1024)S(1)}, ...), branch_computations={%region_3.3_spmd, %region_4.4_spmd} | conditional | flops 135561216 | bytes 2984480 | solution.py:193
  214.7 1.5 fusion.37
  216.2 1.4 fusion.43
  224.3 3.3 %conditional.5 = ((f32[128,1,128]{0,2,1:T(8,128)S(1)}, f32[128,1,128]{0,2,1:T(8,128)S(1)})) conditional(s32[]{:T(128)} %bitcast.124, (f32[128,1,128]{0,2,1:T(8,128)S(1)}, f32[128,1,128]{0,2,1:T(8,128)S(1)}) %tuple.61, (bf16[8,1024,128]{2,1,0:T(8,128)(2,1)}, s32[]{:T(128)}, s32[128]{0:T(128)S(1)}, s32[1024]{0:T(1024)S(1)}, ...), branch_computations={%region_3.3_spmd, %region_4.4_spmd} | conditional | flops 135561216 | bytes 2984480 | solution.py:193
  224.4 1.5 fusion.37
  234.0 3.3 %conditional.5 = ((f32[128,1,128]{0,2,1:T(8,128)S(1)}, f32[128,1,128]{0,2,1:T(8,128)S(1)})) conditional(s32[]{:T(128)} %bitcast.124, (f32[128,1,128]{0,2,1:T(8,128)S(1)}, f32[128,1,128]{0,2,1:T(8,128)S(1)}) %tuple.61, (bf16[8,1024,128]{2,1,0:T(8,128)(2,1)}, s32[]{:T(128)}, s32[128]{0:T(128)S(1)}, s32[1024]{0:T(1024)S(1)}, ...), branch_computations={%region_3.3_spmd, %region_4.4_spmd} | conditional | flops 135561216 | bytes 2984480 | solution.py:193
  234.1 1.5 fusion.37
  243.7 3.3 %conditional.5 = ((f32[128,1,128]{0,2,1:T(8,128)S(1)}, f32[128,1,128]{0,2,1:T(8,128)S(1)})) conditional(s32[]{:T(128)} %bitcast.124, (f32[128,1,128]{0,2,1:T(8,128)S(1)}, f32[128,1,128]{0,2,1:T(8,128)S(1)}) %tuple.61, (bf16[8,1024,128]{2,1,0:T(8,128)(2,1)}, s32[]{:T(128)}, s32[128]{0:T(128)S(1)}, s32[1024]{0:T(1024)S(1)}, ...), branch_computations={%region_3.3_spmd, %region_4.4_spmd} | conditional | flops 135561216 | bytes 2984480 | solution.py:193
  243.8 1.5 fusion.37
  253.4 3.3 %conditional.5 = ((f32[128,1,128]{0,2,1:T(8,128)S(1)}, f32[128,1,128]{0,2,1:T(8,128)S(1)})) conditional(s32[]{:T(128)} %bitcast.124, (f32[128,1,128]{0,2,1:T(8,128)S(1)}, f32[128,1,128]{0,2,1:T(8,128)S(1)}) %tuple.61, (bf16[8,1024,128]{2,1,0:T(8,128)(2,1)}, s32[]{:T(128)}, s32[128]{0:T(128)S(1)}, s32[1024]{0:T(1024)S(1)}, ...), branch_computations={%region_3.3_spmd, %region_4.4_spmd} | conditional | flops 135561216 | bytes 2984480 | solution.py:193
  253.5 1.5 fusion.37
  259.3 7.5 %all-to-all-start = ((f32[64,32,128]{2,1,0:T(8,128)}), f32[64,32,128]{2,1,0:T(8,128)S(1)}, u32[]{:S(2)}, u32[]{:S(2)}) async-start(f32[64,32,128]{2,1,0:T(8,128)} %fusion.65), calls=%async_computation | async-start | bytes 2097152 | tf_op jit(solution)/shard_map/all_to_all | solution.py:59
  268.3 46.1 %all-to-all-done = f32[64,32,128]{2,1,0:T(8,128)S(1)} async-done(((f32[64,32,128]{2,1,0:T(8,128)}), f32[64,32,128]{2,1,0:T(8,128)S(1)}, u32[]{:S(2)}, u32[]{:S(2)}) %all-to-all-start) | async-done | bytes 1048608 | tf_op jit(solution)/shard_map/all_to_all | solution.py:59
  (125 shorter events, 27.4 us)
Async XLA Ops:
  7.2 33.6 %copy-start = (bf16[128,128]{1,0:T(8,128)(2,1)S(1)}, bf16[128,128]{1,0:T(8,128)(2,1)}, u32[]{:S(2)}) copy-start(bf16[128,128]{1,0:T(8,128)(2,1)} %param.20) | copy-start | bytes 98308
  7.2 33.6 %copy-start.2 = (bf16[128,128]{1,0:T(8,128)(2,1)S(1)}, bf16[128,128]{1,0:T(8,128)(2,1)}, u32[]{:S(2)}) copy-start(bf16[128,128]{1,0:T(8,128)(2,1)} %param.19) | copy-start | bytes 98308
  7.2 33.7 %copy-start.5 = (f32[128,1]{0,1:T(1,128)S(1)}, f32[128,1]{0,1:T(1,128)}, u32[]{:S(2)}) copy-start(f32[128,1]{0,1:T(1,128)} %param.18) | copy-start | bytes 1540
  7.2 164.4 %all-gather.4.cloned.1.call-start = ((), (), s32[]{:S(2)}) async-start(), calls=%async_computation.1 | async-start | bytes 8519680 | tf_op jit(solution)/shard_map/all_gather | solution.py:16
  40.9 105.1 %copy-start.4 = (f32[128]{0:T(128)}, f32[128]{0:T(128)S(1)}, u32[]{:S(2)}) copy-start(f32[128]{0:T(128)S(1)} %fusion.63) | copy-start | bytes 1540
  146.4 31.2 %copy-start.1 = (bf16[128,128]{1,0:T(8,128)(2,1)S(1)}, bf16[128,128]{1,0:T(8,128)(2,1)}, u32[]{:S(2)}) copy-start(bf16[128,128]{1,0:T(8,128)(2,1)} %param.16) | copy-start | bytes 98308
  146.4 31.2 %copy-start.3 = (bf16[128,128]{1,0:T(8,128)(2,1)S(1)}, bf16[128,128]{1,0:T(8,128)(2,1)}, u32[]{:S(2)}) copy-start(bf16[128,128]{1,0:T(8,128)(2,1)} %param.14) | copy-start | bytes 98308
  177.6 5.2 %copy-start.6 = (s32[8]{0:T(128)}, s32[8]{0:T(128)S(1)}, u32[]{:S(2)}) copy-start(s32[8]{0:T(128)S(1)} %get-tuple-element.581) | copy-start | bytes 100 | tf_op jit(solution)/shard_map/while
  186.0 4.0 %copy-start.7 = (s32[8]{0:T(128)S(1)}, s32[8]{0:T(128)}, u32[]{:S(2)}) copy-start(s32[8]{0:T(128)} %copy-done.6) | copy-start | bytes 100 | tf_op jit(solution)/shard_map/while
  190.1 5.2 %copy-start.6 = (s32[8]{0:T(128)}, s32[8]{0:T(128)S(1)}, u32[]{:S(2)}) copy-start(s32[8]{0:T(128)S(1)} %get-tuple-element.581) | copy-start | bytes 100 | tf_op jit(solution)/shard_map/while
  198.5 1.2 copy-start.7
  199.8 5.2 %copy-start.6 = (s32[8]{0:T(128)}, s32[8]{0:T(128)S(1)}, u32[]{:S(2)}) copy-start(s32[8]{0:T(128)S(1)} %get-tuple-element.581) | copy-start | bytes 100 | tf_op jit(solution)/shard_map/while
  208.2 1.2 copy-start.7
  209.5 5.2 %copy-start.6 = (s32[8]{0:T(128)}, s32[8]{0:T(128)S(1)}, u32[]{:S(2)}) copy-start(s32[8]{0:T(128)S(1)} %get-tuple-element.581) | copy-start | bytes 100 | tf_op jit(solution)/shard_map/while
  217.9 1.2 copy-start.7
  219.2 5.2 %copy-start.6 = (s32[8]{0:T(128)}, s32[8]{0:T(128)S(1)}, u32[]{:S(2)}) copy-start(s32[8]{0:T(128)S(1)} %get-tuple-element.581) | copy-start | bytes 100 | tf_op jit(solution)/shard_map/while
  227.6 1.2 copy-start.7
  228.9 5.2 %copy-start.6 = (s32[8]{0:T(128)}, s32[8]{0:T(128)S(1)}, u32[]{:S(2)}) copy-start(s32[8]{0:T(128)S(1)} %get-tuple-element.581) | copy-start | bytes 100 | tf_op jit(solution)/shard_map/while
  237.3 1.2 copy-start.7
  238.6 5.2 %copy-start.6 = (s32[8]{0:T(128)}, s32[8]{0:T(128)S(1)}, u32[]{:S(2)}) copy-start(s32[8]{0:T(128)S(1)} %get-tuple-element.581) | copy-start | bytes 100 | tf_op jit(solution)/shard_map/while
  247.0 1.2 copy-start.7
  248.2 5.2 %copy-start.6 = (s32[8]{0:T(128)}, s32[8]{0:T(128)S(1)}, u32[]{:S(2)}) copy-start(s32[8]{0:T(128)S(1)} %get-tuple-element.581) | copy-start | bytes 100 | tf_op jit(solution)/shard_map/while
  256.7 1.2 copy-start.7
  259.3 55.1 %all-to-all-start = ((f32[64,32,128]{2,1,0:T(8,128)}), f32[64,32,128]{2,1,0:T(8,128)S(1)}, u32[]{:S(2)}, u32[]{:S(2)}) async-start(f32[64,32,128]{2,1,0:T(8,128)} %fusion.65), calls=%async_computation | async-start | bytes 2097152 | tf_op jit(solution)/shard_map/all_to_all | solution.py:59
Sparse Core Ops, SparseCore 0:
  10.9 160.5 all-gather.3
where the time goes:
time: 323 us; the launch traced here: 322 us
  blocking collectives  135 us (42%)
  waiting for transfers between devices  71.3 us (22%)
  loops' own time  41.6 us (13%)
  matrix products  29.2 us (9%)
  local copies, waits for them, and re-layouts  19.1 us (6%)
  between operations  14.2 us (4%)
  starting transfers between devices  7.55 us (2%)
  other arithmetic  3.92 us (1%)
    all_gather x1, blocking collectives, in_one_piece(): lax.all_gather(both, axis, axis=dim, tiled=True)  104 us
    all_to_all x1, waiting for transfers between devices, summed_on_arrival(): lax.all_to_all(in_blocks(shard, dim, devices), axis, 0, 0, tiled=True)  46.1 us
    another operation x1, loops' own time, over_blocks(): lax.scan(visit_one, running, (jnp.arange(number, dtype=jnp.int32), stacked))  41.2 us
    all_gather x4, blocking collectives, gather_in_order(): parts = lax.all_gather(parts, axes[k], axis=0, tiled=True)  30.7 us
    all_gather x1, waiting for transfers between devices, in_one_piece(): lax.all_gather(both, axis, axis=dim, tiled=True)  25.1 us
    dot_general x8, matrix products, attention_weights(): jnp.einsum('ahd,bhd->hab', query_part, key_part, preferred_element_type=j...  11.7 us
    dot_general x8, matrix products, key_compute(): jnp.einsum('hab,ahd->bhd', slopes.astype(jnp.bfloat16), query_part, prefe...  11.2 us
    all_to_all x1, starting transfers between devices, summed_on_arrival(): lax.all_to_all(in_blocks(shard, dim, devices), axis, 0, 0, tiled=True)  7.51 us
  transfers between devices with their start and end apart: 2, of which 2 were waited for; matrix products, arithmetic and copies ran while one was open for 1% of the time, Pallas kernels for 0%

commit v1 on v0

v1 whole, which is shorter than its diff:
```python
import functools

import jax
import jax.numpy as jnp
from jax import lax
from jax.experimental import pallas as pl
from jax.experimental.pallas import tpu as pltpu
from jax.sharding import Mesh
from jax.sharding import PartitionSpec as P

SP = ("z", "y")
TP = ("x", "c")
NZ, NY, NX, NC = 16, 4, 4, 2
T = 128
H = 128
SCALE = H**-0.5
ZB = 2 * T + 8
YB = 4 * T + 16
RB = 4 * T + 2 * T
f32 = jnp.float32
bf16 = jnp.bfloat16


def nt(a, b):
    return lax.dot_general(a, b, (((1,), (1,)), ((), ())), preferred_element_type=f32)


def nn(a, b):
    return lax.dot_general(a, b, (((1,), (0,)), ((), ())), preferred_element_type=f32)


def three(x):
    hi = x.astype(bf16)
    rest = x - hi.astype(f32)
    mid = rest.astype(bf16)
    low = (rest - mid.astype(f32)).astype(bf16)
    return [hi, mid, low]


def pack_body(place, q, k, v, g, lse, o, do, zsend, own):
    z = place[0]
    terms = o[...].astype(f32) * do[...].astype(f32)
    r = jnp.sum(terms.T, axis=0, keepdims=True)
    gate = g[...]
    a = gate - lse[...]
    zero = jnp.zeros((1, T), bf16)
    q_stats = three(a) + three(r)
    k_stats = three(gate)
    q_rows = jnp.concatenate(q_stats + [zero, zero], axis=0)
    k_rows = jnp.concatenate(k_stats + [zero] * 5, axis=0)
    own[0:T] = q[...]
    own[T : 2 * T] = do[...]
    own[2 * T : 3 * T] = k[...]
    own[3 * T : 4 * T] = v[...]
    own[4 * T : YB] = jnp.concatenate(q_stats + k_stats + [zero] * 7, axis=0)

    def one(j, carry):
        @pl.when(j > z)
        def _():
            zsend[j, 0:T] = k[...]
            zsend[j, T : 2 * T] = v[...]
            zsend[j, 2 * T : ZB] = k_rows

        @pl.when(j <= z)
        def _():
            zsend[j, 0:T] = q[...]
            zsend[j, T : 2 * T] = do[...]
            zsend[j, 2 * T : ZB] = q_rows

        return carry

    lax.fori_loop(0, NZ, one, 0)


def joined(rows):
    w = rows.astype(f32)
    return w[0:1] + w[1:2] + w[2:3]


def upright(row):
    i = lax.broadcasted_iota(jnp.int32, (T, T), 0)
    j = lax.broadcasted_iota(jnp.int32, (T, T), 1)
    return jnp.sum(jnp.where(i == j, row, 0.0), axis=1, keepdims=True)


def attend_body(place, recv, grp, ysend, dq, dk, dv):
    z = place[0]
    y = place[1]
    qg = jnp.concatenate([grp[i, 0:T] for i in range(NY)], axis=0)
    dog = jnp.concatenate([grp[i, T : 2 * T] for i in range(NY)], axis=0)
    kg = jnp.concatenate([grp[i, 2 * T : 3 * T] for i in range(NY)], axis=0)
    vg = jnp.concatenate([grp[i, 3 * T : 4 * T] for i in range(NY)], axis=0)
    stats = [grp[i, 4 * T : YB] for i in range(NY)]
    a_col = jnp.concatenate([upright(joined(s[0:3])) for s in stats], axis=0)
    r_col = jnp.concatenate([upright(joined(s[3:6])) for s in stats], axis=0)
    g_col = jnp.concatenate([upright(joined(s[6:9])) for s in stats], axis=0)

    def query_part(k, v, g_row, mask):
        s = nt(qg, k) * SCALE + (a_col - g_row)
        if mask is not None:
            s = jnp.where(mask, s, -jnp.inf)
        w = jnp.exp(s)
        sl = (w * (nt(dog, v) - r_col)).astype(bf16)
        return nn(sl, k)

    def key_part(q, do, a_row, r_row, mask):
        s = nt(kg, q) * SCALE + (a_row - g_col)
        if mask is not None:
            s = jnp.where(mask, s, -jnp.inf)
        w = jnp.exp(s)
        sl = (w * (nt(vg, do) - r_row)).astype(bf16)
        return nn(sl, q), nn(w.astype(bf16), do)

    big = lax.broadcasted_iota(jnp.int32, (NY * T, T), 0)
    small = lax.broadcasted_iota(jnp.int32, (NY * T, T), 1) + y * T
    own_stats = grp[y, 4 * T : YB]
    dq[...] = query_part(grp[y, 2 * T : 3 * T], grp[y, 3 * T : 4 * T], joined(own_stats[6:9]), small <= big)
    first = key_part(
        grp[y, 0:T], grp[y, T : 2 * T], joined(own_stats[0:3]), joined(own_stats[3:6]), big <= small
    )
    dk[...] = first[0]
    dv[...] = first[1]

    def below(j, carry):
        dq[...] += query_part(recv[j, 0:T], recv[j, T : 2 * T], joined(recv[j, 2 * T : ZB][0:3]), None)
        return carry

    def above(j, carry):
        rows = recv[j, 2 * T : ZB]
        more = key_part(recv[j, 0:T], recv[j, T : 2 * T], joined(rows[0:3]), joined(rows[3:6]), None)
        dk[...] += more[0]
        dv[...] += more[1]
        return carry

    lax.fori_loop(0, z, below, 0)
    lax.fori_loop(z + 1, NZ, above, 0)
    sums = dq[...].astype(bf16)
    for i in range(NY):
        ysend[i, 0 : 4 * T] = sums
        ysend[i, 4 * T : 5 * T] = dk[i * T : (i + 1) * T].astype(bf16)
        ysend[i, 5 * T : 6 * T] = dv[i * T : (i + 1) * T].astype(bf16)


def finish_body(place, yrecv, xt, q_out, k_out, v_out, zs, dq):
    y = place[1]

    def total(lo, hi):
        w = [yrecv[i, lo:hi].astype(f32) for i in range(NY)]
        return (w[0] + w[1]) + (w[2] + w[3])

    dq[...] = (total(0, 4 * T) * SCALE).astype(bf16)
    q_out[...] = dq[pl.ds(pl.multiple_of(y * T, T), T)]
    k_out[...] = (total(4 * T, 5 * T) * SCALE).astype(bf16)
    v_out[...] = total(5 * T, 6 * T).astype(bf16)
    acc = None
    for i in range(NY):
        part = nn(xt[:, i].reshape(NX * NC * 64, T), dq[i * T : (i + 1) * T])
        acc = part if acc is None else acc + part
    zs[...] = acc.astype(bf16).reshape(NZ, 32, H)


def vmem(count):
    return [pl.BlockSpec(memory_space=pltpu.VMEM)] * count


def call(body, name, out_shape, scratch, count):
    return pl.pallas_call(
        body,
        name=name,
        in_specs=[pl.BlockSpec(memory_space=pltpu.SMEM)] + vmem(count),
        out_specs=tuple(vmem(len(out_shape))),
        out_shape=tuple(jax.ShapeDtypeStruct(s, d) for s, d in out_shape),
        scratch_shapes=scratch,
    )


def per_device(q, k, v, g, lse, o, do, x):
    place = jnp.stack([lax.axis_index("z"), lax.axis_index("y")]).astype(jnp.int32)
    pack = call(pack_body, "pack", [((NZ, ZB, H), bf16), ((YB, H), bf16)], [], 7)
    zsend, own = pack(place, q, k, v, g.reshape(1, T), lse.reshape(1, T), o, do)
    recv = lax.all_to_all(zsend, "z", 0, 0, tiled=True)
    grp = lax.all_gather(own, "y", axis=0, tiled=False)
    xt = x.T.reshape(2, NY, 32, T).transpose(1, 0, 2, 3).reshape(NY, 64, T)
    xt = lax.all_to_all(xt, "y", 0, 0, tiled=True)
    xt = lax.all_gather(xt, TP, axis=0, tiled=False)
    block = (NY * T, H)
    attend = call(attend_body, "attend", [((NY, RB, H), bf16)], [pltpu.VMEM(block, f32)] * 3, 2)
    (ysend,) = attend(place, recv, grp)
    yrecv = lax.all_to_all(ysend, "y", 0, 0, tiled=True)
    one = ((T, H), bf16)
    finish = call(finish_body, "finish", [one, one, one, ((NZ, 32, H), bf16)], [pltpu.VMEM(block, bf16)], 2)
    q_grad, k_grad, v_grad, zs = finish(place, yrecv, xt)
    back = lax.all_to_all(zs, "z", 0, 0, tiled=True)
    return q_grad, k_grad, v_grad, jnp.sum(back.astype(f32), axis=0)


def solution(mesh):
    finer = Mesh(mesh.devices.reshape(NZ, NY, NX, NC), ("z", "y", "x", "c"))
    spec = P(SP, TP)
    return jax.shard_map(
        per_device, mesh=finer, in_specs=(spec,) * 8, out_specs=(spec,) * 4, check_vma=False
    )
```

time: 323 us -> 144 us (0.45)
  blocking collectives: 135 us -> 51.8 us
  loops' own time: 41.6 us -> 0 us
  matrix products: 29.2 us -> 0 us
  waiting for transfers between devices: 71.3 us -> 50.4 us
  local copies, waits for them, and re-layouts: 19.1 us -> 1.64 us
  starting transfers between devices: 7.55 us -> 23.4 us
  between operations: 14.2 us -> 0.67 us
  Pallas kernels: 0 us -> 13.4 us
    all_gather x5 -> x2, blocking collectives: 135 us -> 28.6 us  [the longest x1 14.4 us: per_device(): grp = lax.all_gather(own, 'y', axis=0, tiled=False)]
    another operation x17 -> x0, loops' own time: 41.6 us -> none  [the longest x1 41.2 us: over_blocks(): lax.scan(visit_one, running, (jnp.arange(number, dtype=jnp.int32), stacked))]
    dot_general x27 -> x0, matrix products: 29.2 us -> none  [the longest x8 11.7 us: attention_weights(): jnp.einsum('ahd,bhd->hab', query_part, key_part, preferred_element_type=j...]
    all_gather x1 -> x0, waiting for transfers between devices: 25.1 us -> none  [in_one_piece(): lax.all_gather(both, axis, axis=dim, tiled=True)]
    all_to_all x0 -> x1, blocking collectives: none -> 23.2 us  [per_device(): back = lax.all_to_all(zs, 'z', 0, 0, tiled=True)]
    all_to_all x1 -> x3, starting transfers between devices: 7.51 us -> 23.4 us  [the longest x1 15.3 us: per_device(): recv = lax.all_to_all(zsend, 'z', 0, 0, tiled=True)]
    pallas_call x0 -> x3, Pallas kernels: none -> 13.4 us  [the longest x1 8.82 us: per_device(): ysend, = attend(place, recv, grp)]
    split x3 -> x0, local copies, waits for them, and re-layouts: 6.81 us -> none  [the longest x2 6.02 us: in_one_piece(): jnp.split(lax.all_gather(both, axis, axis=dim, tiled=True), ends, axis=al...]
  transfers between devices with their start and end apart: 2 -> 3, of which waited for: 2 -> 1; matrix products, arithmetic and copies ran while one was open for 1% -> 1% of each run, Pallas kernels for 0% -> 6%
where the time goes in v1:
time: 144 us; the launch traced here: 143 us
  blocking collectives  51.8 us (36%)
  waiting for transfers between devices  50.4 us (35%)
  starting transfers between devices  23.4 us (16%)
  Pallas kernels  13.4 us (9%)
  local copies, waits for them, and re-layouts  1.64 us (1%)
    all_to_all x1, waiting for transfers between devices, per_device(): recv = lax.all_to_all(zsend, 'z', 0, 0, tiled=True)  50.4 us
    all_to_all x1, blocking collectives, per_device(): back = lax.all_to_all(zs, 'z', 0, 0, tiled=True)  23.2 us
    all_to_all x1, starting transfers between devices, per_device(): recv = lax.all_to_all(zsend, 'z', 0, 0, tiled=True)  15.3 us
    all_gather x1, blocking collectives, per_device(): grp = lax.all_gather(own, 'y', axis=0, tiled=False)  14.4 us
    all_gather x1, blocking collectives, per_device(): xt = lax.all_gather(xt, TP, axis=0, tiled=False)  14.2 us
    pallas_call x1, Pallas kernels, per_device(): ysend, = attend(place, recv, grp)  8.82 us
    all_to_all x1, starting transfers between devices, per_device(): xt = lax.all_to_all(xt, 'y', 0, 0, tiled=True)  4.46 us
    all_to_all x1, starting transfers between devices, per_device(): yrecv = lax.all_to_all(ysend, 'y', 0, 0, tiled=True)  3.65 us
  transfers between devices with their start and end apart: 3, of which 1 were waited for; matrix products, arithmetic and copies ran while one was open for 1% of the time, Pallas kernels for 6%

profile of v1, /device:TPU:6, one launch (start us, length us, event | category | flops | bytes accessed | tf_op | source)
XLA Modules:
  0.0 142.7 jit_solution(1863356149477591324)
XLA Ops:
  0.6 0.7 pad_add_fusion.place
  1.3 2.3 %pack.1 = (bf16[16,264,128]{2,1,0:T(8,128)(2,1)}, bf16[528,128]{1,0:T(8,128)(2,1)}) custom-call(s32[2]{0:T(128)} %pad_add_fusion.place, bf16[128,128]{1,0:T(8,128)(2,1)} %q.1, bf16[128,128]{1,0:T(8,128)(2,1)} %k.1, bf16[128,128]{1,0:T(8,128)(2,1)} %v.1, f32[1,128]{1,0:T(1,128)} %bitcast.15, f32[1,128]{1,0:T(1,128)} %bitcast.16, bf16[128,128]{1,0:T(8,128)(2,1)} %o.1, ...), custom_call_target="tpu_custom_call" | custom-call | tf_op jit(solution)/shard_map/pack/pallas_call | solution.py:180
  3.6 0.0 copy-start.3
  3.6 0.0 copy-start.2
  3.6 15.3 %all-to-all-start = ((bf16[16,264,128]{2,1,0:T(8,128)(2,1)}), bf16[16,264,128]{2,1,0:T(8,128)(2,1)S(1)}, u32[]{:S(2)}, u32[]{:S(2)}) async-start(bf16[16,264,128]{2,1,0:T(8,128)(2,1)} %get-tuple-element.10), calls=%async_computation | async-start | bytes 2162688 | tf_op jit(solution)/shard_map/all_to_all | solution.py:181
  18.9 0.0 copy-done.3
  18.9 0.1 copy.16
  19.1 0.6 copy.17
  19.7 50.4 %all-to-all-done.recv = bf16[16,264,128]{2,1,0:T(8,128)(2,1)S(1)} async-done(((bf16[16,264,128]{2,1,0:T(8,128)(2,1)}), bf16[16,264,128]{2,1,0:T(8,128)(2,1)S(1)}, u32[]{:S(2)}, u32[]{:S(2)}) %all-to-all-start) | async-done | bytes 1081376 | tf_op jit(solution)/shard_map/all_to_all | solution.py:181
  70.1 0.0 copy-start
  70.1 4.5 %all-to-all-start.2 = ((bf16[4,64,128]{2,1,0:T(8,128)(2,1)}), bf16[4,64,128]{2,1,0:T(8,128)(2,1)S(1)}, u32[]{:S(2)}, u32[]{:S(2)}) async-start(bf16[4,64,128]{2,1,0:T(8,128)(2,1)} %bitcast.8), calls=%async_computation.2 | async-start | bytes 131072 | tf_op jit(solution)/shard_map/all_to_all | solution.py:184
  74.6 0.0 copy-done.2
  74.6 14.4 %all-gather = bf16[2112,128]{1,0:T(8,128)(2,1)} all-gather(bf16[528,128]{1,0:T(8,128)(2,1)S(1)} %copy-done.2), channel_id=2, replica_groups=mesh['z'=16,'y'=4,'x'=4,'c'=2] {'y'}, dimensions={0}, use_global_device_ids=true | all-gather | bytes 675840 | tf_op jit(solution)/shard_map/all_gather | solution.py:182
  89.0 0.0 copy-done
  89.0 8.8 %attend.1 = bf16[4,768,128]{2,1,0:T(8,128)(2,1)} custom-call(s32[2]{0:T(128)} %pad_add_fusion.place, bf16[16,264,128]{2,1,0:T(8,128)(2,1)} %copy-done, bf16[4,528,128]{2,1,0:T(8,128)(2,1)} %bitcast.12), custom_call_target="tpu_custom_call" | custom-call | tf_op jit(solution)/shard_map/attend/pallas_call | solution.py:188
  97.8 0.0 all-to-all-done.2
  97.8 3.7 %all-to-all-start.1 = ((bf16[4,768,128]{2,1,0:T(8,128)(2,1)}), bf16[4,768,128]{2,1,0:T(8,128)(2,1)S(1)}, u32[]{:S(2)}, u32[]{:S(2)}) async-start(bf16[4,768,128]{2,1,0:T(8,128)(2,1)} %attend.1), calls=%async_computation.1 | async-start | bytes 1572864 | tf_op jit(solution)/shard_map/all_to_all | solution.py:189
  101.5 14.2 %all-gather.1 = bf16[32,64,128]{2,1,0:T(8,128)(2,1)} all-gather(bf16[4,64,128]{2,1,0:T(8,128)(2,1)S(1)} %all-to-all-done.2), channel_id=3, replica_groups=mesh['z'=16,'y'=4,'x'=4,'c'=2] {'x','c'}, dimensions={0}, use_global_device_ids=true | all-gather | bytes 589824 | tf_op jit(solution)/shard_map/all_gather | solution.py:185
  115.7 0.0 all-to-all-done.1.yrecv
  115.7 0.0 copy-start.1
  115.7 0.9 copy-done.1
  116.5 2.3 %finish.1 = (bf16[128,128]{1,0:T(8,128)(2,1)}, bf16[128,128]{1,0:T(8,128)(2,1)}, bf16[128,128]{1,0:T(8,128)(2,1)}, bf16[16,32,128]{2,1,0:T(8,128)(2,1)}) custom-call(s32[2]{0:T(128)} %pad_add_fusion.place, bf16[4,768,128]{2,1,0:T(8,128)(2,1)} %copy-done.1, bf16[8,4,64,128]{3,2,1,0:T(8,128)(2,1)} %bitcast.13), custom_call_target="tpu_custom_call" | custom-call | tf_op jit(solution)/shard_map/finish/pallas_call | solution.py:192
  118.8 23.2 %all_to_all.20 = bf16[16,32,128]{2,1,0:T(8,128)(2,1)S(1)} all-to-all(bf16[16,32,128]{2,1,0:T(8,128)(2,1)} %get-tuple-element.15), channel_id=1, replica_groups=mesh['z'=16,'y'=4,'x'=4,'c'=2] {'z'}, dimensions={0} | all-to-all | bytes 262144 | tf_op jit(solution)/shard_map/all_to_all | solution.py:193
  142.0 0.6 convert_reduce_fusion
Async XLA Ops:
  3.6 15.3 %copy-start.3 = (bf16[128,256]{1,0:T(8,128)(2,1)S(1)}, bf16[128,256]{1,0:T(8,128)(2,1)}, u32[]{:S(2)}) copy-start(bf16[128,256]{1,0:T(8,128)(2,1)} %param.15) | copy-start | bytes 196612
  3.6 71.0 %copy-start.2 = (bf16[528,128]{1,0:T(8,128)(2,1)S(1)}, bf16[528,128]{1,0:T(8,128)(2,1)}, u32[]{:S(2)}) copy-start(bf16[528,128]{1,0:T(8,128)(2,1)} %get-tuple-element.11) | copy-start | bytes 405508
  3.6 66.5 %all-to-all-start = ((bf16[16,264,128]{2,1,0:T(8,128)(2,1)}), bf16[16,264,128]{2,1,0:T(8,128)(2,1)S(1)}, u32[]{:S(2)}, u32[]{:S(2)}) async-start(bf16[16,264,128]{2,1,0:T(8,128)(2,1)} %get-tuple-element.10), calls=%async_computation | async-start | bytes 2162688 | tf_op jit(solution)/shard_map/all_to_all | solution.py:181
  70.1 18.9 %copy-start = (bf16[16,264,128]{2,1,0:T(8,128)(2,1)}, bf16[16,264,128]{2,1,0:T(8,128)(2,1)S(1)}, u32[]{:S(2)}) copy-start(bf16[16,264,128]{2,1,0:T(8,128)(2,1)S(1)} %all-to-all-done.recv) | copy-start | bytes 3244036
  70.1 27.7 %all-to-all-start.2 = ((bf16[4,64,128]{2,1,0:T(8,128)(2,1)}), bf16[4,64,128]{2,1,0:T(8,128)(2,1)S(1)}, u32[]{:S(2)}, u32[]{:S(2)}) async-start(bf16[4,64,128]{2,1,0:T(8,128)(2,1)} %bitcast.8), calls=%async_computation.2 | async-start | bytes 131072 | tf_op jit(solution)/shard_map/all_to_all | solution.py:184
  97.8 17.8 %all-to-all-start.1 = ((bf16[4,768,128]{2,1,0:T(8,128)(2,1)}), bf16[4,768,128]{2,1,0:T(8,128)(2,1)S(1)}, u32[]{:S(2)}, u32[]{:S(2)}) async-start(bf16[4,768,128]{2,1,0:T(8,128)(2,1)} %attend.1), calls=%async_computation.1 | async-start | bytes 1572864 | tf_op jit(solution)/shard_map/all_to_all | solution.py:189
  115.7 0.9 copy-start.1

commit v2 on v1

--- a/solution.py
+++ b/solution.py
@@ -15,7 +15,9 @@
 H = 128
 SCALE = H**-0.5
 ZB = 2 * T + 8
-YB = 4 * T + 16
+ST = 4 * T
+XB = ST + 16
+YB = XB + 2 * T
 RB = 4 * T + 2 * T
 f32 = jnp.float32
 bf16 = jnp.bfloat16
@@ -37,7 +39,7 @@
     return [hi, mid, low]
 
 
-def pack_body(place, q, k, v, g, lse, o, do, zsend, own):
+def pack_body(place, q, k, v, g, lse, o, do, x, zsend, own):
     z = place[0]
     terms = o[...].astype(f32) * do[...].astype(f32)
     r = jnp.sum(terms.T, axis=0, keepdims=True)
@@ -52,7 +54,8 @@
     own[T : 2 * T] = do[...]
     own[2 * T : 3 * T] = k[...]
     own[3 * T : 4 * T] = v[...]
-    own[4 * T : YB] = jnp.concatenate(q_stats + k_stats + [zero] * 7, axis=0)
+    own[ST:XB] = jnp.concatenate(q_stats + k_stats + [zero] * 7, axis=0)
+    own[XB:YB] = x[...].T
 
     def one(j, carry):
         @pl.when(j > z)
@@ -90,7 +93,7 @@
     dog = jnp.concatenate([grp[i, T : 2 * T] for i in range(NY)], axis=0)
     kg = jnp.concatenate([grp[i, 2 * T : 3 * T] for i in range(NY)], axis=0)
     vg = jnp.concatenate([grp[i, 3 * T : 4 * T] for i in range(NY)], axis=0)
-    stats = [grp[i, 4 * T : YB] for i in range(NY)]
+    stats = [grp[i, ST:XB] for i in range(NY)]
     a_col = jnp.concatenate([upright(joined(s[0:3])) for s in stats], axis=0)
     r_col = jnp.concatenate([upright(joined(s[3:6])) for s in stats], axis=0)
     g_col = jnp.concatenate([upright(joined(s[6:9])) for s in stats], axis=0)
@@ -113,7 +116,7 @@
 
     big = lax.broadcasted_iota(jnp.int32, (NY * T, T), 0)
     small = lax.broadcasted_iota(jnp.int32, (NY * T, T), 1) + y * T
-    own_stats = grp[y, 4 * T : YB]
+    own_stats = grp[y, ST:XB]
     dq[...] = query_part(grp[y, 2 * T : 3 * T], grp[y, 3 * T : 4 * T], joined(own_stats[6:9]), small <= big)
     first = key_part(
         grp[y, 0:T], grp[y, T : 2 * T], joined(own_stats[0:3]), joined(own_stats[3:6]), big <= small
@@ -176,13 +179,14 @@
 
 def per_device(q, k, v, g, lse, o, do, x):
     place = jnp.stack([lax.axis_index("z"), lax.axis_index("y")]).astype(jnp.int32)
-    pack = call(pack_body, "pack", [((NZ, ZB, H), bf16), ((YB, H), bf16)], [], 7)
-    zsend, own = pack(place, q, k, v, g.reshape(1, T), lse.reshape(1, T), o, do)
+    pack = call(pack_body, "pack", [((NZ, ZB, H), bf16), ((YB, H), bf16)], [], 8)
+    zsend, own = pack(place, q, k, v, g.reshape(1, T), lse.reshape(1, T), o, do, x)
     recv = lax.all_to_all(zsend, "z", 0, 0, tiled=True)
     grp = lax.all_gather(own, "y", axis=0, tiled=False)
-    xt = x.T.reshape(2, NY, 32, T).transpose(1, 0, 2, 3).reshape(NY, 64, T)
-    xt = lax.all_to_all(xt, "y", 0, 0, tiled=True)
-    xt = lax.all_gather(xt, TP, axis=0, tiled=False)
+    y = lax.axis_index("y")
+    part = [lax.dynamic_slice_in_dim(grp, XB + half * T + y * 32, 32, 1) for half in range(2)]
+    xt = lax.all_gather(jnp.concatenate(part, axis=1), TP, axis=0, tiled=False)
+    recv, xt = lax.optimization_barrier((recv, xt))
     block = (NY * T, H)
     attend = call(attend_body, "attend", [((NY, RB, H), bf16)], [pltpu.VMEM(block, f32)] * 3, 2)
     (ysend,) = attend(place, recv, grp)

time: 144 us -> 123 us (0.85)
  waiting for transfers between devices: 50.4 us -> 23.1 us
  blocking collectives: 51.8 us -> 67.1 us
  starting transfers between devices: 23.4 us -> 15.3 us
    all_to_all x1, waiting for transfers between devices: 50.4 us -> 23.1 us  [per_device(): recv = lax.all_to_all(zsend, 'z', 0, 0, tiled=True)]
    all_to_all x0 -> x1, blocking collectives: none -> 14.1 us  [per_device(): yrecv = lax.all_to_all(ysend, 'y', 0, 0, tiled=True)]
    all_to_all x2 -> x0, starting transfers between devices: 8.12 us -> none  [the longest x1 4.46 us: per_device(): xt = lax.all_to_all(xt, 'y', 0, 0, tiled=True)]
    all_to_all x1, blocking collectives: 23.2 us -> 25 us  [per_device(): back = lax.all_to_all(zs, 'z', 0, 0, tiled=True)]
  transfers between devices with their start and end apart: 3 -> 1, of which waited for: 1 -> 1; matrix products, arithmetic and copies ran while one was open for 1% -> 0% of each run, Pallas kernels for 6% -> 0%
where the time goes in v2:
time: 123 us; the launch traced here: 122 us
  blocking collectives  67.1 us (55%)
  waiting for transfers between devices  23.1 us (19%)
  starting transfers between devices  15.3 us (12%)
  Pallas kernels  13.6 us (11%)
  other arithmetic  1.24 us (1%)
    all_to_all x1, blocking collectives, per_device(): back = lax.all_to_all(zs, 'z', 0, 0, tiled=True)  25 us
    all_to_all x1, waiting for transfers between devices, per_device(): recv = lax.all_to_all(zsend, 'z', 0, 0, tiled=True)  23.1 us
    all_to_all x1, starting transfers between devices, per_device(): recv = lax.all_to_all(zsend, 'z', 0, 0, tiled=True)  15.3 us
    all_gather x1, blocking collectives, per_device(): xt = lax.all_gather(jnp.concatenate(part, axis=1), TP, axis=0, tiled=False)  14.2 us
    all_to_all x1, blocking collectives, per_device(): yrecv = lax.all_to_all(ysend, 'y', 0, 0, tiled=True)  14.1 us
    all_gather x1, blocking collectives, per_device(): grp = lax.all_gather(own, 'y', axis=0, tiled=False)  13.9 us
    pallas_call x1, Pallas kernels, per_device(): ysend, = attend(place, recv, grp)  8.87 us
  transfers between devices with their start and end apart: 1, of which 1 were waited for; matrix products, arithmetic and copies ran while one was open for 0% of the time, Pallas kernels for 0%

profile of v2, /device:TPU:6, one launch (start us, length us, event | category | flops | bytes accessed | tf_op | source)
XLA Modules:
  0.0 122.0 jit_solution(18314313010933190638)
XLA Ops:
  0.6 0.6 pad_add_fusion.place
  1.2 2.4 %pack.1 = (bf16[16,264,128]{2,1,0:T(8,128)(2,1)}, bf16[784,128]{1,0:T(8,128)(2,1)}) custom-call(s32[2]{0:T(128)} %pad_add_fusion.place, bf16[128,128]{1,0:T(8,128)(2,1)} %q.1, bf16[128,128]{1,0:T(8,128)(2,1)} %k.1, bf16[128,128]{1,0:T(8,128)(2,1)} %v.1, f32[1,128]{1,0:T(1,128)} %bitcast.9, f32[1,128]{1,0:T(1,128)} %bitcast.10, bf16[128,128]{1,0:T(8,128)(2,1)} %o.1, ...), custom_call_target="tpu_custom_call" | custom-call | tf_op jit(solution)/shard_map/pack/pallas_call | solution.py:183
  3.7 0.0 copy-start.2
  3.7 15.3 %all-to-all-start = ((bf16[16,264,128]{2,1,0:T(8,128)(2,1)}), bf16[16,264,128]{2,1,0:T(8,128)(2,1)S(1)}, u32[]{:S(2)}, u32[]{:S(2)}) async-start(bf16[16,264,128]{2,1,0:T(8,128)(2,1)} %get-tuple-element.12), calls=%async_computation | async-start | bytes 2162688 | tf_op jit(solution)/shard_map/all_to_all | solution.py:184
  19.0 0.0 copy-done.2
  19.0 13.9 %all-gather = bf16[3136,128]{1,0:T(8,128)(2,1)S(1)} all-gather(bf16[784,128]{1,0:T(8,128)(2,1)S(1)} %copy-done.2), channel_id=2, replica_groups=mesh['z'=16,'y'=4,'x'=4,'c'=2] {'y'}, dimensions={0}, use_global_device_ids=true | all-gather | bytes 1003520 | tf_op jit(solution)/shard_map/all_gather | solution.py:185
  32.9 0.0 copy-start.1
  32.9 14.2 %all-gather.1 = bf16[32,64,128]{2,1,0:T(8,128)(2,1)} all-gather(bf16[4,64,128]{2,1,0:T(8,128)(2,1)S(1)} %pad_maximum_fusion), channel_id=3, replica_groups=mesh['z'=16,'y'=4,'x'=4,'c'=2] {'x','c'}, dimensions={0}, use_global_device_ids=true | all-gather | bytes 589824 | tf_op jit(solution)/shard_map/all_gather | solution.py:188
  47.1 23.1 %all-to-all-done.recv = bf16[16,264,128]{2,1,0:T(8,128)(2,1)S(1)} async-done(((bf16[16,264,128]{2,1,0:T(8,128)(2,1)}), bf16[16,264,128]{2,1,0:T(8,128)(2,1)S(1)}, u32[]{:S(2)}, u32[]{:S(2)}) %all-to-all-start) | async-done | bytes 1081376 | tf_op jit(solution)/shard_map/all_to_all | solution.py:184
  70.2 0.0 copy-start
  70.2 0.0 copy-done.1
  70.2 1.0 copy-done
  71.2 8.9 %attend.1 = bf16[4,768,128]{2,1,0:T(8,128)(2,1)} custom-call(s32[2]{0:T(128)} %pad_add_fusion.place, bf16[16,264,128]{2,1,0:T(8,128)(2,1)} %copy-done, bf16[4,784,128]{2,1,0:T(8,128)(2,1)} %bitcast.7), custom_call_target="tpu_custom_call" | custom-call | tf_op jit(solution)/shard_map/attend/pallas_call | solution.py:192
  80.1 14.1 %all_to_all.15.yrecv = bf16[4,768,128]{2,1,0:T(8,128)(2,1)} all-to-all(bf16[4,768,128]{2,1,0:T(8,128)(2,1)} %attend.1), channel_id=1, replica_groups=mesh['z'=16,'y'=4,'x'=4,'c'=2] {'y'}, dimensions={0} | all-to-all | bytes 1572864 | tf_op jit(solution)/shard_map/all_to_all | solution.py:193
  94.1 2.3 %finish.1 = (bf16[128,128]{1,0:T(8,128)(2,1)}, bf16[128,128]{1,0:T(8,128)(2,1)}, bf16[128,128]{1,0:T(8,128)(2,1)}, bf16[16,32,128]{2,1,0:T(8,128)(2,1)}) custom-call(s32[2]{0:T(128)} %pad_add_fusion.place, bf16[4,768,128]{2,1,0:T(8,128)(2,1)} %all_to_all.15.yrecv, bf16[8,4,64,128]{3,2,1,0:T(8,128)(2,1)} %bitcast.8), custom_call_target="tpu_custom_call" | custom-call | tf_op jit(solution)/shard_map/finish/pallas_call | solution.py:196
  96.4 25.0 %all_to_all.16 = bf16[16,32,128]{2,1,0:T(8,128)(2,1)S(1)} all-to-all(bf16[16,32,128]{2,1,0:T(8,128)(2,1)} %get-tuple-element.19), channel_id=1, replica_groups=mesh['z'=16,'y'=4,'x'=4,'c'=2] {'z'}, dimensions={0} | all-to-all | bytes 262144 | tf_op jit(solution)/shard_map/all_to_all | solution.py:197
  121.4 0.6 convert_reduce_fusion
  (2 shorter events, 0.0 us)
Async XLA Ops:
  3.7 15.3 %copy-start.2 = (bf16[784,128]{1,0:T(8,128)(2,1)S(1)}, bf16[784,128]{1,0:T(8,128)(2,1)}, u32[]{:S(2)}) copy-start(bf16[784,128]{1,0:T(8,128)(2,1)} %get-tuple-element.13) | copy-start | bytes 602116
  3.7 66.5 %all-to-all-start = ((bf16[16,264,128]{2,1,0:T(8,128)(2,1)}), bf16[16,264,128]{2,1,0:T(8,128)(2,1)S(1)}, u32[]{:S(2)}, u32[]{:S(2)}) async-start(bf16[16,264,128]{2,1,0:T(8,128)(2,1)} %get-tuple-element.12), calls=%async_computation | async-start | bytes 2162688 | tf_op jit(solution)/shard_map/all_to_all | solution.py:184
  32.9 37.3 %copy-start.1 = (bf16[3136,128]{1,0:T(8,128)(2,1)}, bf16[3136,128]{1,0:T(8,128)(2,1)S(1)}, u32[]{:S(2)}) copy-start(bf16[3136,128]{1,0:T(8,128)(2,1)S(1)} %all-gather) | copy-start | bytes 2408452
  70.2 1.0 copy-start

commit v3 on v2

v3 whole, which is shorter than its diff:
```python
import jax
import jax.numpy as jnp
from jax import lax
from jax.experimental import pallas as pl
from jax.experimental.pallas import tpu as pltpu
from jax.sharding import Mesh
from jax.sharding import PartitionSpec as P

SP = ("zp", "zl", "y")
TP = ("x", "c")
NZ, NP, NY, NX, NC = 16, 8, 4, 4, 2
T = 128
H = 128
SCALE = H**-0.5
ZB = 2 * T + 8
ST = 4 * T
XB = ST + 16
YB = XB + 2 * T
RB = 4 * T + 2 * T
f32 = jnp.float32
bf16 = jnp.bfloat16


def nt(a, b):
    return lax.dot_general(a, b, (((1,), (1,)), ((), ())), preferred_element_type=f32)


def nn(a, b):
    return lax.dot_general(a, b, (((1,), (0,)), ((), ())), preferred_element_type=f32)


def three(x):
    hi = x.astype(bf16)
    rest = x - hi.astype(f32)
    mid = rest.astype(bf16)
    low = (rest - mid.astype(f32)).astype(bf16)
    return [hi, mid, low]


def pack_body(place, q, k, v, g, lse, o, do, x, zsend, own):
    zp = place[0]
    zl = place[1]
    terms = o[...].astype(f32) * do[...].astype(f32)
    r = jnp.sum(terms.T, axis=0, keepdims=True)
    gate = g[...]
    a = gate - lse[...]
    zero = jnp.zeros((1, T), bf16)
    q_stats = three(a) + three(r)
    k_stats = three(gate)
    q_rows = jnp.concatenate(q_stats + [zero, zero], axis=0)
    k_rows = jnp.concatenate(k_stats + [zero] * 5, axis=0)
    own[0:T] = q[...]
    own[T : 2 * T] = do[...]
    own[2 * T : 3 * T] = k[...]
    own[3 * T : 4 * T] = v[...]
    own[ST:XB] = jnp.concatenate(q_stats + k_stats + [zero] * 7, axis=0)
    own[XB:YB] = x[...].T

    def one(j, carry):
        up = j + 1 > zp + zl

        @pl.when(up)
        def _():
            zsend[j, 0:T] = k[...]
            zsend[j, T : 2 * T] = v[...]
            zsend[j, 2 * T : ZB] = k_rows

        @pl.when(jnp.logical_not(up))
        def _():
            zsend[j, 0:T] = q[...]
            zsend[j, T : 2 * T] = do[...]
            zsend[j, 2 * T : ZB] = q_rows

        return carry

    lax.fori_loop(0, NP, one, 0)


def joined(rows):
    w = rows.astype(f32)
    return w[0:1] + w[1:2] + w[2:3]


def upright(row):
    i = lax.broadcasted_iota(jnp.int32, (T, T), 0)
    j = lax.broadcasted_iota(jnp.int32, (T, T), 1)
    return jnp.sum(jnp.where(i == j, row, 0.0), axis=1, keepdims=True)


def tall(grp, at):
    return jnp.concatenate([grp[i, at : at + T] for i in range(NY)], axis=0)


def tall_stat(grp, at):
    return jnp.concatenate([upright(joined(grp[i, ST:XB][at : at + 3])) for i in range(NY)], axis=0)


def parts_of(grp):
    qg, dog, kg, vg = (tall(grp, i * T) for i in range(4))
    a_col, r_col, g_col = (tall_stat(grp, 3 * i) for i in range(3))

    def query_part(k, v, g_row, mask=None):
        s = nt(qg, k) * SCALE + (a_col - g_row)
        if mask is not None:
            s = jnp.where(mask, s, -jnp.inf)
        w = jnp.exp(s)
        sl = (w * (nt(dog, v) - r_col)).astype(bf16)
        return nn(sl, k)

    def key_part(q, do, a_row, r_row, mask=None):
        s = nt(kg, q) * SCALE + (a_row - g_col)
        if mask is not None:
            s = jnp.where(mask, s, -jnp.inf)
        w = jnp.exp(s)
        sl = (w * (nt(vg, do) - r_row)).astype(bf16)
        return nn(sl, q), nn(w.astype(bf16), do)

    return query_part, key_part


def received(recv, query_part, key_part, below_end, above_start, dq, dk, dv):
    def below(j, carry):
        rows = recv[j, 2 * T : ZB]
        dq[...] += query_part(recv[j, 0:T], recv[j, T : 2 * T], joined(rows[0:3]))
        return carry

    def above(j, carry):
        rows = recv[j, 2 * T : ZB]
        more = key_part(recv[j, 0:T], recv[j, T : 2 * T], joined(rows[0:3]), joined(rows[3:6]))
        dk[...] += more[0]
        dv[...] += more[1]
        return carry

    lax.fori_loop(0, below_end, below, 0)
    lax.fori_loop(above_start, NP, above, 0)


def first_body(place, recv, grp, dq, dk, dv):
    zp = place[0]
    y = place[2]
    query_part, key_part = parts_of(grp)
    big = lax.broadcasted_iota(jnp.int32, (NY * T, T), 0)
    small = lax.broadcasted_iota(jnp.int32, (NY * T, T), 1) + y * T
    st = grp[y, ST:XB]
    dq[...] = query_part(grp[y, 2 * T : 3 * T], grp[y, 3 * T : 4 * T], joined(st[6:9]), small <= big)
    dk[...], dv[...] = key_part(
        grp[y, 0:T], grp[y, T : 2 * T], joined(st[0:3]), joined(st[3:6]), big <= small
    )
    received(recv, query_part, key_part, zp, zp + 1, dq, dk, dv)


def second_body(place, recv, grp, dq0, dk0, dv0, ysend, dq, dk, dv):
    border = place[0] + place[1]
    query_part, key_part = parts_of(grp)
    dq[...] = dq0[...]
    dk[...] = dk0[...]
    dv[...] = dv0[...]
    received(recv, query_part, key_part, border, border, dq, dk, dv)
    sums = dq[...].astype(bf16)
    for i in range(NY):
        ysend[i, 0 : 4 * T] = sums
        ysend[i, 4 * T : 5 * T] = dk[i * T : (i + 1) * T].astype(bf16)
        ysend[i, 5 * T : 6 * T] = dv[i * T : (i + 1) * T].astype(bf16)


def finish_body(place, yrecv, xt, q_out, k_out, v_out, zs, dq):
    y = place[2]

    def total(lo, hi):
        w = [yrecv[i, lo:hi].astype(f32) for i in range(NY)]
        return (w[0] + w[1]) + (w[2] + w[3])

    dq[...] = (total(0, 4 * T) * SCALE).astype(bf16)
    q_out[...] = dq[pl.ds(pl.multiple_of(y * T, T), T)]
    k_out[...] = (total(4 * T, 5 * T) * SCALE).astype(bf16)
    v_out[...] = total(5 * T, 6 * T).astype(bf16)
    acc = None
    for i in range(NY):
        part = nn(xt[:, i].reshape(NX * NC * 64, T), dq[i * T : (i + 1) * T])
        acc = part if acc is None else acc + part
    zs[...] = acc.astype(bf16).reshape(NZ, 32, H)


def vmem(count):
    return [pl.BlockSpec(memory_space=pltpu.VMEM)] * count


def call(body, name, out_shape, scratch, count):
    return pl.pallas_call(
        body,
        name=name,
        in_specs=[pl.BlockSpec(memory_space=pltpu.SMEM)] + vmem(count),
        out_specs=tuple(vmem(len(out_shape))),
        out_shape=tuple(jax.ShapeDtypeStruct(s, d) for s, d in out_shape),
        scratch_shapes=scratch,
    )


def per_device(q, k, v, g, lse, o, do, x):
    y = lax.axis_index("y")
    place = jnp.stack([lax.axis_index("zp"), lax.axis_index("zl"), y]).astype(jnp.int32)
    pack = call(pack_body, "pack", [((NP, ZB, H), bf16), ((YB, H), bf16)], [], 8)
    zsend, own = pack(place, q, k, v, g.reshape(1, T), lse.reshape(1, T), o, do, x)
    recv = lax.all_to_all(zsend, "zp", 0, 0, tiled=True)
    grp = lax.all_gather(own, "y", axis=0, tiled=False)
    part = [lax.dynamic_slice_in_dim(grp, XB + half * T + y * 32, 32, 1) for half in range(2)]
    xt = lax.all_gather(jnp.concatenate(part, axis=1), TP, axis=0, tiled=False)
    recv, xt = lax.optimization_barrier((recv, xt))
    relayed = lax.ppermute(recv, "zl", [(0, 1), (1, 0)])
    block = (NY * T, H)
    first = call(first_body, "first", [(block, f32)] * 3, [], 2)
    sums = first(place, recv, grp)
    second = call(second_body, "second", [((NY, RB, H), bf16)], [pltpu.VMEM(block, f32)] * 3, 5)
    (ysend,) = second(place, relayed, grp, *sums)
    yrecv = lax.all_to_all(ysend, "y", 0, 0, tiled=True)
    one = ((T, H), bf16)
    finish = call(finish_body, "finish", [one, one, one, ((NZ, 32, H), bf16)], [pltpu.VMEM(block, bf16)], 2)
    q_grad, k_grad, v_grad, zs = finish(place, yrecv, xt)
    back = lax.all_to_all(zs, ("zp", "zl"), 0, 0, tiled=True)
    return q_grad, k_grad, v_grad, jnp.sum(back.astype(f32), axis=0)


def solution(mesh):
    finer = Mesh(mesh.devices.reshape(NP, 2, NY, NX, NC), SP + TP)
    spec = P(SP, TP)
    return jax.shard_map(
        per_device, mesh=finer, in_specs=(spec,) * 8, out_specs=(spec,) * 4, check_vma=False
    )
```

time: 123 us -> 116 us (0.943)
  waiting for transfers between devices: 23.1 us -> 7.67 us
  blocking collectives: 67.1 us -> 70.4 us
  starting transfers between devices: 15.3 us -> 18.3 us
  Pallas kernels: 13.6 us -> 15.9 us
    all_to_all x1, waiting for transfers between devices: 23.1 us -> 0.01 us  [per_device(): recv = lax.all_to_all(zsend, 'zp', 0, 0, tiled=True)]
    ppermute x0 -> x1, waiting for transfers between devices: none -> 7.66 us  [per_device(): relayed = lax.ppermute(recv, 'zl', [(0, 1), (1, 0)])]
    ppermute x0 -> x1, starting transfers between devices: none -> 3.09 us  [per_device(): relayed = lax.ppermute(recv, 'zl', [(0, 1), (1, 0)])]
    all_to_all x1, blocking collectives: 14.1 us -> 16.8 us  [per_device(): yrecv = lax.all_to_all(ysend, 'y', 0, 0, tiled=True)]
    pallas_call x1 -> x2, Pallas kernels: 8.87 us -> 11.5 us  [the longest x1 5.82 us: per_device(): ysend, = second(place, relayed, grp, *sums)]
  transfers between devices with their start and end apart: 1 -> 2, of which waited for: 1 -> 1; matrix products, arithmetic and copies ran while one was open for 0% -> 0% of each run, Pallas kernels for 0% -> 5%
where the time goes in v3:
time: 116 us; the launch traced here: 115 us
  blocking collectives  70.4 us (61%)
  starting transfers between devices  18.3 us (16%)
  Pallas kernels  15.9 us (14%)
  waiting for transfers between devices  7.67 us (7%)
  other arithmetic  1.24 us (1%)
    all_to_all x1, blocking collectives, per_device(): back = lax.all_to_all(zs, ('zp', 'zl'), 0, 0, tiled=True)  25.5 us
    all_to_all x1, blocking collectives, per_device(): yrecv = lax.all_to_all(ysend, 'y', 0, 0, tiled=True)  16.8 us
    all_to_all x1, starting transfers between devices, per_device(): recv = lax.all_to_all(zsend, 'zp', 0, 0, tiled=True)  15.2 us
    all_gather x1, blocking collectives, per_device(): xt = lax.all_gather(jnp.concatenate(part, axis=1), TP, axis=0, tiled=False)  14.2 us
    all_gather x1, blocking collectives, per_device(): grp = lax.all_gather(own, 'y', axis=0, tiled=False)  13.9 us
    ppermute x1, waiting for transfers between devices, per_device(): relayed = lax.ppermute(recv, 'zl', [(0, 1), (1, 0)])  7.66 us
    pallas_call x1, Pallas kernels, per_device(): ysend, = second(place, relayed, grp, *sums)  5.82 us
    pallas_call x1, Pallas kernels, per_device(): sums = first(place, recv, grp)  5.63 us
  transfers between devices with their start and end apart: 2, of which 1 were waited for; matrix products, arithmetic and copies ran while one was open for 0% of the time, Pallas kernels for 5%

profile of v3, /device:TPU:6, one launch (start us, length us, event | category | flops | bytes accessed | tf_op | source)
XLA Modules:
  0.0 115.0 jit_solution(13803053779400844813)
XLA Ops:
  0.6 0.6 pad_add_fusion.place
  1.2 2.1 %pack.1 = (bf16[8,264,128]{2,1,0:T(8,128)(2,1)}, bf16[784,128]{1,0:T(8,128)(2,1)}) custom-call(s32[3]{0:T(128)} %pad_add_fusion.place, bf16[128,128]{1,0:T(8,128)(2,1)} %q.1, bf16[128,128]{1,0:T(8,128)(2,1)} %k.1, bf16[128,128]{1,0:T(8,128)(2,1)} %v.1, f32[1,128]{1,0:T(1,128)} %bitcast.11, f32[1,128]{1,0:T(1,128)} %bitcast.12, bf16[128,128]{1,0:T(8,128)(2,1)} %o.1, ...), custom_call_target="tpu_custom_call" | custom-call | tf_op jit(solution)/shard_map/pack/pallas_call | solution.py:203
  3.4 0.0 copy-start.3
  3.4 15.2 %all-to-all-start = ((bf16[8,264,128]{2,1,0:T(8,128)(2,1)}), bf16[8,264,128]{2,1,0:T(8,128)(2,1)S(1)}, u32[]{:S(2)}, u32[]{:S(2)}) async-start(bf16[8,264,128]{2,1,0:T(8,128)(2,1)} %get-tuple-element.15), calls=%async_computation | async-start | bytes 1081344 | tf_op jit(solution)/shard_map/all_to_all | solution.py:204
  18.6 0.0 copy-done.3
  18.6 13.9 %all-gather = bf16[3136,128]{1,0:T(8,128)(2,1)S(1)} all-gather(bf16[784,128]{1,0:T(8,128)(2,1)S(1)} %copy-done.3), channel_id=2, replica_groups=mesh['zp'=8,'zl'=2,'y'=4,'x'=4,'c'=2] {'y'}, dimensions={0}, use_global_device_ids=true | all-gather | bytes 1003520 | tf_op jit(solution)/shard_map/all_gather | solution.py:205
  32.5 0.0 copy-start
  32.5 14.2 %all-gather.1 = bf16[32,64,128]{2,1,0:T(8,128)(2,1)} all-gather(bf16[4,64,128]{2,1,0:T(8,128)(2,1)S(1)} %pad_maximum_fusion), channel_id=3, replica_groups=mesh['zp'=8,'zl'=2,'y'=4,'x'=4,'c'=2] {'x','c'}, dimensions={0}, use_global_device_ids=true | all-gather | bytes 589824 | tf_op jit(solution)/shard_map/all_gather | solution.py:207
  46.7 0.0 all-to-all-done.recv
  46.7 0.0 copy-start.1
  46.7 3.1 %collective-permute-start = (bf16[8,264,128]{2,1,0:T(8,128)(2,1)S(1)}, bf16[8,264,128]{2,1,0:T(8,128)(2,1)S(1)}, u32[]{:S(2)}, u32[]{:S(2)}) collective-permute-start(bf16[8,264,128]{2,1,0:T(8,128)(2,1)S(1)} %all-to-all-done.recv), channel_id=1, source_target_pairs={{0,32},{32,0},{1,33},{33,1},{2,34},{34,2},{3,35},{35,3},{4,36},{36... | collective-permute-start | bytes 1622024 | tf_op jit(solution)/shard_map/ppermute | solution.py:209
  49.8 0.0 copy-done
  49.8 0.0 copy-done.1
  49.8 5.6 %first.1 = (f32[512,128]{1,0:T(8,128)}, f32[512,128]{1,0:T(8,128)}, f32[512,128]{1,0:T(8,128)}) custom-call(s32[3]{0:T(128)} %pad_add_fusion.place, bf16[8,264,128]{2,1,0:T(8,128)(2,1)} %copy-done.1, bf16[4,784,128]{2,1,0:T(8,128)(2,1)} %bitcast.8), custom_call_target="tpu_custom_call" | custom-call | tf_op jit(solution)/shard_map/first/pallas_call | solution.py:212
  55.4 7.7 %collective-permute-done.recv = bf16[8,264,128]{2,1,0:T(8,128)(2,1)S(1)} collective-permute-done((bf16[8,264,128]{2,1,0:T(8,128)(2,1)S(1)}, bf16[8,264,128]{2,1,0:T(8,128)(2,1)S(1)}, u32[]{:S(2)}, u32[]{:S(2)}) %collective-permute-start) | collective-permute-done | bytes 540704 | tf_op jit(solution)/shard_map/ppermute | solution.py:209
  63.1 0.0 copy-start.2
  63.1 0.8 copy-done.2
  63.9 5.8 %second.1 = bf16[4,768,128]{2,1,0:T(8,128)(2,1)} custom-call(s32[3]{0:T(128)} %pad_add_fusion.place, bf16[8,264,128]{2,1,0:T(8,128)(2,1)} %copy-done.2, bf16[4,784,128]{2,1,0:T(8,128)(2,1)} %bitcast.9, f32[512,128]{1,0:T(8,128)} %get-tuple-element.18.dq0, f32[512,128]{1,0:T(8,128)} %get-tuple-element.19.dk0, f32[512,128]{1,0:T(8,128)} %get-tuple-element.20.dv0), custom_call_target="tpu_custom_call" | custom-call | tf_op jit(solution)/shard_map/second/pallas_call | solution.py:214
  69.7 16.8 %all_to_all.15.yrecv = bf16[4,768,128]{2,1,0:T(8,128)(2,1)} all-to-all(bf16[4,768,128]{2,1,0:T(8,128)(2,1)} %second.1), channel_id=1, replica_groups=mesh['zp'=8,'zl'=2,'y'=4,'x'=4,'c'=2] {'y'}, dimensions={0} | all-to-all | bytes 1572864 | tf_op jit(solution)/shard_map/all_to_all | solution.py:215
  86.6 2.3 %finish.1 = (bf16[128,128]{1,0:T(8,128)(2,1)}, bf16[128,128]{1,0:T(8,128)(2,1)}, bf16[128,128]{1,0:T(8,128)(2,1)}, bf16[16,32,128]{2,1,0:T(8,128)(2,1)}) custom-call(s32[3]{0:T(128)} %pad_add_fusion.place, bf16[4,768,128]{2,1,0:T(8,128)(2,1)} %all_to_all.15.yrecv, bf16[8,4,64,128]{3,2,1,0:T(8,128)(2,1)} %bitcast.10), custom_call_target="tpu_custom_call" | custom-call | tf_op jit(solution)/shard_map/finish/pallas_call | solution.py:218
  88.8 25.5 %all_to_all.16 = bf16[16,32,128]{2,1,0:T(8,128)(2,1)S(1)} all-to-all(bf16[16,32,128]{2,1,0:T(8,128)(2,1)} %get-tuple-element.25), channel_id=1, replica_groups=mesh['zp'=8,'zl'=2,'y'=4,'x'=4,'c'=2] {'zp','zl'}, dimensions={0} | all-to-all | bytes 262144 | tf_op jit(solution)/shard_map/all_to_all | solution.py:219
  114.3 0.6 convert_reduce_fusion
  (2 shorter events, 0.0 us)
Async XLA Ops:
  3.4 15.2 %copy-start.3 = (bf16[784,128]{1,0:T(8,128)(2,1)S(1)}, bf16[784,128]{1,0:T(8,128)(2,1)}, u32[]{:S(2)}) copy-start(bf16[784,128]{1,0:T(8,128)(2,1)} %get-tuple-element.16) | copy-start | bytes 602116
  3.4 43.3 %all-to-all-start = ((bf16[8,264,128]{2,1,0:T(8,128)(2,1)}), bf16[8,264,128]{2,1,0:T(8,128)(2,1)S(1)}, u32[]{:S(2)}, u32[]{:S(2)}) async-start(bf16[8,264,128]{2,1,0:T(8,128)(2,1)} %get-tuple-element.15), calls=%async_computation | async-start | bytes 1081344 | tf_op jit(solution)/shard_map/all_to_all | solution.py:204
  32.5 17.3 %copy-start = (bf16[3136,128]{1,0:T(8,128)(2,1)}, bf16[3136,128]{1,0:T(8,128)(2,1)S(1)}, u32[]{:S(2)}) copy-start(bf16[3136,128]{1,0:T(8,128)(2,1)S(1)} %all-gather) | copy-start | bytes 2408452
  46.7 3.1 %copy-start.1 = (bf16[8,264,128]{2,1,0:T(8,128)(2,1)}, bf16[8,264,128]{2,1,0:T(8,128)(2,1)S(1)}, u32[]{:S(2)}) copy-start(bf16[8,264,128]{2,1,0:T(8,128)(2,1)S(1)} %all-to-all-done.recv) | copy-start | bytes 1622020
  46.7 16.4 %collective-permute-start = (bf16[8,264,128]{2,1,0:T(8,128)(2,1)S(1)}, bf16[8,264,128]{2,1,0:T(8,128)(2,1)S(1)}, u32[]{:S(2)}, u32[]{:S(2)}) collective-permute-start(bf16[8,264,128]{2,1,0:T(8,128)(2,1)S(1)} %all-to-all-done.recv), channel_id=1, source_target_pairs={{0,32},{32,0},{1,33},{33,1},{2,34},{34,2},{3,35},{35,3},{4,36},{36... | collective-permute-start | bytes 1622024 | tf_op jit(solution)/shard_map/ppermute | solution.py:209
  63.1 0.8 copy-start.2

commit v4 on v3

--- a/solution.py
+++ b/solution.py
@@ -8,7 +8,7 @@
 
 SP = ("zp", "zl", "y")
 TP = ("x", "c")
-NZ, NP, NY, NX, NC = 16, 8, 4, 4, 2
+NP, NY, NX, NC = 8, 4, 4, 2
 T = 128
 H = 128
 SCALE = H**-0.5
@@ -16,7 +16,6 @@
 ST = 4 * T
 XB = ST + 16
 YB = XB + 2 * T
-RB = 4 * T + 2 * T
 f32 = jnp.float32
 bf16 = jnp.bfloat16
 
@@ -149,46 +148,45 @@
     received(recv, query_part, key_part, zp, zp + 1, dq, dk, dv)
 
 
-def second_body(place, recv, grp, dq0, dk0, dv0, ysend, dq, dk, dv):
+def second_body(place, recv, grp, dq0, dk0, dv0, q_sums, *rest):
+    kv_sums, (dq, dk, dv) = rest[:NY], rest[NY:]
     border = place[0] + place[1]
+    y = place[2]
     query_part, key_part = parts_of(grp)
     dq[...] = dq0[...]
     dk[...] = dk0[...]
     dv[...] = dv0[...]
     received(recv, query_part, key_part, border, border, dq, dk, dv)
     sums = dq[...].astype(bf16)
-    for i in range(NY):
-        ysend[i, 0 : 4 * T] = sums
-        ysend[i, 4 * T : 5 * T] = dk[i * T : (i + 1) * T].astype(bf16)
-        ysend[i, 5 * T : 6 * T] = dv[i * T : (i + 1) * T].astype(bf16)
-
-
-def finish_body(place, yrecv, xt, q_out, k_out, v_out, zs, dq):
+    for d in range(NY):
+        at = pl.ds(pl.multiple_of(((y + d) % NY) * T, T), T)
+        q_sums[d] = sums
+        kv_sums[d][0:T] = dk[at].astype(bf16)
+        kv_sums[d][T : 2 * T] = dv[at].astype(bf16)
+
+
+def finish_body(place, q_sums, xt, q_out, keep, send, dq, wg):
+    zl = place[1]
     y = place[2]
-
-    def total(lo, hi):
-        w = [yrecv[i, lo:hi].astype(f32) for i in range(NY)]
-        return (w[0] + w[1]) + (w[2] + w[3])
-
-    dq[...] = (total(0, 4 * T) * SCALE).astype(bf16)
+    w = [q_sums[i].astype(f32) for i in range(NY)]
+    dq[...] = (((w[0] + w[1]) + (w[2] + w[3])) * SCALE).astype(bf16)
     q_out[...] = dq[pl.ds(pl.multiple_of(y * T, T), T)]
-    k_out[...] = (total(4 * T, 5 * T) * SCALE).astype(bf16)
-    v_out[...] = total(5 * T, 6 * T).astype(bf16)
     acc = None
     for i in range(NY):
-        part = nn(xt[:, i].reshape(NX * NC * 64, T), dq[i * T : (i + 1) * T])
+        part = nn(xt[:, i].reshape(NP * 64, T), dq[i * T : (i + 1) * T])
         acc = part if acc is None else acc + part
-    zs[...] = acc.astype(bf16).reshape(NZ, 32, H)
+    wg[...] = acc.reshape(NP, 2, 32, H)
+    keep[...] = wg[:, pl.ds(zl, 1)].reshape(NP, 32, H)
+    send[...] = wg[:, pl.ds(1 - zl, 1)].reshape(NP, 32, H).astype(bf16)
 
 
 def vmem(count):
     return [pl.BlockSpec(memory_space=pltpu.VMEM)] * count
 
 
-def call(body, name, out_shape, scratch, count):
+def call(body, out_shape, scratch, count):
     return pl.pallas_call(
         body,
-        name=name,
         in_specs=[pl.BlockSpec(memory_space=pltpu.SMEM)] + vmem(count),
         out_specs=tuple(vmem(len(out_shape))),
         out_shape=tuple(jax.ShapeDtypeStruct(s, d) for s, d in out_shape),
@@ -199,7 +197,7 @@
 def per_device(q, k, v, g, lse, o, do, x):
     y = lax.axis_index("y")
     place = jnp.stack([lax.axis_index("zp"), lax.axis_index("zl"), y]).astype(jnp.int32)
-    pack = call(pack_body, "pack", [((NP, ZB, H), bf16), ((YB, H), bf16)], [], 8)
+    pack = call(pack_body, [((NP, ZB, H), bf16), ((YB, H), bf16)], [], 8)
     zsend, own = pack(place, q, k, v, g.reshape(1, T), lse.reshape(1, T), o, do, x)
     recv = lax.all_to_all(zsend, "zp", 0, 0, tiled=True)
     grp = lax.all_gather(own, "y", axis=0, tiled=False)
@@ -208,15 +206,33 @@
     recv, xt = lax.optimization_barrier((recv, xt))
     relayed = lax.ppermute(recv, "zl", [(0, 1), (1, 0)])
     block = (NY * T, H)
-    first = call(first_body, "first", [(block, f32)] * 3, [], 2)
+    first = call(first_body, [(block, f32)] * 3, [], 2)
     sums = first(place, recv, grp)
-    second = call(second_body, "second", [((NY, RB, H), bf16)], [pltpu.VMEM(block, f32)] * 3, 5)
-    (ysend,) = second(place, relayed, grp, *sums)
-    yrecv = lax.all_to_all(ysend, "y", 0, 0, tiled=True)
-    one = ((T, H), bf16)
-    finish = call(finish_body, "finish", [one, one, one, ((NZ, 32, H), bf16)], [pltpu.VMEM(block, bf16)], 2)
-    q_grad, k_grad, v_grad, zs = finish(place, yrecv, xt)
-    back = lax.all_to_all(zs, ("zp", "zl"), 0, 0, tiled=True)
+    kv_block = ((2 * T, H), bf16)
+    second = call(
+        second_body, [((NY, NY * T, H), bf16)] + [kv_block] * NY, [pltpu.VMEM(block, f32)] * 3, 5
+    )
+    q_sums, *kv = second(place, relayed, grp, *sums)
+    q_sums = lax.all_to_all(q_sums, "y", 0, 0, tiled=True)
+    part = (NP, 32, H)
+    finish = call(
+        finish_body,
+        [((T, H), bf16), (part, f32), (part, bf16)],
+        [pltpu.VMEM(block, bf16), pltpu.VMEM((NP, 2, 32, H), f32)],
+        2,
+    )
+    q_grad, keep, send = finish(place, q_sums, xt)
+    other = lax.ppermute(send, "zl", [(0, 1), (1, 0)])
+    pair = (keep + other.astype(f32)).astype(bf16)
+    pair, *kv = lax.optimization_barrier((pair, *kv))
+    back = lax.all_to_all(pair, "zp", 0, 0, tiled=True)
+    total = kv[0].astype(f32)
+    for d in range(1, NY):
+        turn = [(i, (i + d) % NY) for i in range(NY)]
+        turned = lax.ppermute(kv[d], "y", turn)
+        total = total + turned.astype(f32)
+    k_grad = (total[0:T] * SCALE).astype(bf16)
+    v_grad = total[T : 2 * T].astype(bf16)
     return q_grad, k_grad, v_grad, jnp.sum(back.astype(f32), axis=0)
 
 

time: 116 us -> 130 us (1.12)
  blocking collectives: 70.4 us -> 42.1 us
  starting transfers between devices: 18.3 us -> 42.8 us
  waiting for transfers between devices: 7.67 us -> 23.2 us
  other arithmetic: 1.24 us -> 3.43 us
    all_to_all x2 -> x1, blocking collectives: 42.4 us -> 14 us  [per_device(): q_sums = lax.all_to_all(q_sums, 'y', 0, 0, tiled=True)]
    ppermute x0 -> x4, starting transfers between devices: none -> 12.4 us  [the longest x3 9.46 us: per_device(): turned = lax.ppermute(kv[d], 'y', turn)]
    all_to_all x0 -> x1, waiting for transfers between devices: none -> 12.1 us  [per_device(): back = lax.all_to_all(pair, 'zp', 0, 0, tiled=True)]
    all_to_all x0 -> x1, starting transfers between devices: none -> 12.1 us  [per_device(): back = lax.all_to_all(pair, 'zp', 0, 0, tiled=True)]
    ppermute x0 -> x4, waiting for transfers between devices: none -> 3.42 us  [the longest x1 3.41 us: per_device(): other = lax.ppermute(send, 'zl', [(0, 1), (1, 0)])]
    convert_element_type x0 -> x2, other arithmetic: none -> 2.21 us  [the longest x1 1.59 us: per_device(): pair = (keep + other.astype(f32)).astype(bf16)]
  transfers between devices with their start and end apart: 2 -> 7, of which waited for: 1 -> 3; matrix products, arithmetic and copies ran while one was open for 0% -> 1% of each run, Pallas kernels for 5% -> 4%
where the time goes in v4:
time: 130 us; the launch traced here: 129 us
  starting transfers between devices  42.8 us (33%)
  blocking collectives  42.1 us (32%)
  waiting for transfers between devices  23.2 us (18%)
  Pallas kernels  15.7 us (12%)
  other arithmetic  3.43 us (3%)
  local copies, waits for them, and re-layouts  1.46 us (1%)
    all_to_all x1, starting transfers between devices, per_device(): recv = lax.all_to_all(zsend, 'zp', 0, 0, tiled=True)  15.2 us
    all_gather x1, blocking collectives, per_device(): xt = lax.all_gather(jnp.concatenate(part, axis=1), TP, axis=0, tiled=False)  14.2 us
    all_to_all x1, blocking collectives, per_device(): q_sums = lax.all_to_all(q_sums, 'y', 0, 0, tiled=True)  14 us
    all_gather x1, blocking collectives, per_device(): grp = lax.all_gather(own, 'y', axis=0, tiled=False)  13.9 us
    all_to_all x1, waiting for transfers between devices, per_device(): back = lax.all_to_all(pair, 'zp', 0, 0, tiled=True)  12.1 us
    all_to_all x1, starting transfers between devices, per_device(): back = lax.all_to_all(pair, 'zp', 0, 0, tiled=True)  12.1 us
    ppermute x3, starting transfers between devices, per_device(): turned = lax.ppermute(kv[d], 'y', turn)  9.46 us
    ppermute x1, waiting for transfers between devices, per_device(): relayed = lax.ppermute(recv, 'zl', [(0, 1), (1, 0)])  7.65 us
  transfers between devices with their start and end apart: 7, of which 3 were waited for; matrix products, arithmetic and copies ran while one was open for 1% of the time, Pallas kernels for 4%

profile of v4, /device:TPU:6, one launch (start us, length us, event | category | flops | bytes accessed | tf_op | source)
XLA Modules:
  0.0 129.4 jit_solution(6053979697378650852)
XLA Ops:
  0.6 0.6 pad_add_fusion.place
  1.2 2.1 %shard_map.111 = (bf16[8,264,128]{2,1,0:T(8,128)(2,1)}, bf16[784,128]{1,0:T(8,128)(2,1)}) custom-call(s32[3]{0:T(128)} %pad_add_fusion.place, bf16[128,128]{1,0:T(8,128)(2,1)} %q.1, bf16[128,128]{1,0:T(8,128)(2,1)} %k.1, bf16[128,128]{1,0:T(8,128)(2,1)} %v.1, f32[1,128]{1,0:T(1,128)} %bitcast.11, f32[1,128]{1,0:T(1,128)} %bitcast.12, bf16[128,128]{1,0:T(8,128)(2,1)} %o.1, ...), custom_call_target="tpu_custom_call" | custom-call | tf_op jit(solution)/shard_map/pallas_call | solution.py:201
  3.3 15.2 %all-to-all-start = ((bf16[8,264,128]{2,1,0:T(8,128)(2,1)}), bf16[8,264,128]{2,1,0:T(8,128)(2,1)S(1)}, u32[]{:S(2)}, u32[]{:S(2)}) async-start(bf16[8,264,128]{2,1,0:T(8,128)(2,1)} %get-tuple-element.24), calls=%async_computation | async-start | bytes 1081344 | tf_op jit(solution)/shard_map/all_to_all | solution.py:202
  18.5 0.0 copy-done.3
  18.5 13.9 %all-gather = bf16[3136,128]{1,0:T(8,128)(2,1)S(1)} all-gather(bf16[784,128]{1,0:T(8,128)(2,1)S(1)} %copy-done.3), channel_id=2, replica_groups=mesh['zp'=8,'zl'=2,'y'=4,'x'=4,'c'=2] {'y'}, dimensions={0}, use_global_device_ids=true | all-gather | bytes 1003520 | tf_op jit(solution)/shard_map/all_gather | solution.py:203
  32.4 14.2 %all-gather.1 = bf16[32,64,128]{2,1,0:T(8,128)(2,1)} all-gather(bf16[4,64,128]{2,1,0:T(8,128)(2,1)S(1)} %pad_maximum_fusion), channel_id=3, replica_groups=mesh['zp'=8,'zl'=2,'y'=4,'x'=4,'c'=2] {'x','c'}, dimensions={0}, use_global_device_ids=true | all-gather | bytes 589824 | tf_op jit(solution)/shard_map/all_gather | solution.py:205
  46.6 0.0 all-to-all-done.recv
  46.6 3.1 %collective-permute-start = (bf16[8,264,128]{2,1,0:T(8,128)(2,1)S(1)}, bf16[8,264,128]{2,1,0:T(8,128)(2,1)S(1)}, u32[]{:S(2)}, u32[]{:S(2)}) collective-permute-start(bf16[8,264,128]{2,1,0:T(8,128)(2,1)S(1)} %all-to-all-done.recv), channel_id=1, source_target_pairs={{0,32},{32,0},{1,33},{33,1},{2,34},{34,2},{3,35},{35,3},{4,36},{36... | collective-permute-start | bytes 1622024 | tf_op jit(solution)/shard_map/ppermute | solution.py:207
  49.7 0.0 copy-done
  49.7 0.0 copy-done.1
  49.7 5.6 %shard_map.112 = (f32[512,128]{1,0:T(8,128)}, f32[512,128]{1,0:T(8,128)}, f32[512,128]{1,0:T(8,128)}) custom-call(s32[3]{0:T(128)} %pad_add_fusion.place, bf16[8,264,128]{2,1,0:T(8,128)(2,1)} %copy-done.1, bf16[4,784,128]{2,1,0:T(8,128)(2,1)} %bitcast.8), custom_call_target="tpu_custom_call" | custom-call | tf_op jit(solution)/shard_map/pallas_call | solution.py:210
  55.3 7.7 %collective-permute-done.recv = bf16[8,264,128]{2,1,0:T(8,128)(2,1)S(1)} collective-permute-done((bf16[8,264,128]{2,1,0:T(8,128)(2,1)S(1)}, bf16[8,264,128]{2,1,0:T(8,128)(2,1)S(1)}, u32[]{:S(2)}, u32[]{:S(2)}) %collective-permute-start) | collective-permute-done | bytes 540704 | tf_op jit(solution)/shard_map/ppermute | solution.py:207
  63.0 0.8 copy-done.2
  63.8 5.8 %shard_map.113 = (bf16[4,512,128]{2,1,0:T(8,128)(2,1)}, bf16[256,128]{1,0:T(8,128)(2,1)}, bf16[256,128]{1,0:T(8,128)(2,1)}, bf16[256,128]{1,0:T(8,128)(2,1)}, bf16[256,128]{1,0:T(8,128)(2,1)}) custom-call(s32[3]{0:T(128)} %pad_add_fusion.place, bf16[8,264,128]{2,1,0:T(8,128)(2,1)} %copy-done.2, bf16[4,784,128]{2,1,0:T(8,128)(2,1)} %bitcast.9, ...), custom_call_target="tpu_custom_call" | custom-call | tf_op jit(solution)/shard_map/pallas_call | solution.py:215
  69.6 14.0 %all_to_all.15.q_sums = bf16[4,512,128]{2,1,0:T(8,128)(2,1)} all-to-all(bf16[4,512,128]{2,1,0:T(8,128)(2,1)} %get-tuple-element.30), channel_id=1, replica_groups=mesh['zp'=8,'zl'=2,'y'=4,'x'=4,'c'=2] {'y'}, dimensions={0} | all-to-all | bytes 1048576 | tf_op jit(solution)/shard_map/all_to_all | solution.py:216
  83.6 2.2 %shard_map.114 = (bf16[128,128]{1,0:T(8,128)(2,1)}, f32[8,32,128]{2,1,0:T(8,128)}, bf16[8,32,128]{2,1,0:T(8,128)(2,1)}) custom-call(s32[3]{0:T(128)} %pad_add_fusion.place, bf16[4,512,128]{2,1,0:T(8,128)(2,1)} %all_to_all.15.q_sums, bf16[8,4,64,128]{3,2,1,0:T(8,128)(2,1)} %bitcast.10), custom_call_target="tpu_custom_call" | custom-call | tf_op jit(solution)/shard_map/pallas_call | solution.py:224
  85.9 2.9 %collective-permute-start.1 = (bf16[8,32,128]{2,1,0:T(8,128)(2,1)}, bf16[8,32,128]{2,1,0:T(8,128)(2,1)S(1)}, u32[]{:S(2)}, u32[]{:S(2)}) collective-permute-start(bf16[8,32,128]{2,1,0:T(8,128)(2,1)} %get-tuple-element.34), channel_id=1, source_target_pairs={{0,32},{32,0},{1,33},{33,1},{2,34},{34,2},{3,35},{35,3},{4,36},{36... | collective-permute-start | bytes 196616 | tf_op jit(solution)/shard_map/ppermute | solution.py:225
  88.8 3.4 %collective-permute-done.1 = bf16[8,32,128]{2,1,0:T(8,128)(2,1)S(1)} collective-permute-done((bf16[8,32,128]{2,1,0:T(8,128)(2,1)}, bf16[8,32,128]{2,1,0:T(8,128)(2,1)S(1)}, u32[]{:S(2)}, u32[]{:S(2)}) %collective-permute-start.1) | collective-permute-done | bytes 65568 | tf_op jit(solution)/shard_map/ppermute | solution.py:225
  92.2 1.6 %add_convert_fusion = bf16[8,32,128]{2,1,0:T(8,128)(2,1)} fusion(f32[8,32,128]{2,1,0:T(8,128)} %get-tuple-element.33, bf16[8,32,128]{2,1,0:T(8,128)(2,1)S(1)} %collective-permute-done.1), kind=kLoop, calls=%fused_computation.2 | loop fusion | flops 98304 | bytes 262144 | tf_op jit(solution)/shard_map/convert_element_type | solution.py:226
  93.8 0.0 copy-done.7
  93.8 2.8 %collective-permute-start.2 = (bf16[256,128]{1,0:T(8,128)(2,1)S(1)}, bf16[256,128]{1,0:T(8,128)(2,1)S(1)}, u32[]{:S(2)}, u32[]{:S(2)}) collective-permute-start(bf16[256,128]{1,0:T(8,128)(2,1)S(1)} %copy-done.7), channel_id=1, source_target_pairs={{0,8},{8,16},{16,24},{24,0},{1,9},{9,17},{17,25},{25,1},{2,10},{10... | collective-permute-start | bytes 196616 | tf_op jit(solution)/shard_map/ppermute | solution.py:232
  96.6 4.0 %collective-permute-start.3 = (bf16[256,128]{1,0:T(8,128)(2,1)S(1)}, bf16[256,128]{1,0:T(8,128)(2,1)S(1)}, u32[]{:S(2)}, u32[]{:S(2)}) collective-permute-start(bf16[256,128]{1,0:T(8,128)(2,1)S(1)} %copy-done.6), channel_id=1, source_target_pairs={{0,16},{8,24},{16,0},{24,8},{1,17},{9,25},{17,1},{25,9},{2,18},{10... | collective-permute-start | bytes 196616 | tf_op jit(solution)/shard_map/ppermute | solution.py:232
  100.6 0.0 copy-done.5
  100.6 2.7 %collective-permute-start.4 = (bf16[256,128]{1,0:T(8,128)(2,1)S(1)}, bf16[256,128]{1,0:T(8,128)(2,1)S(1)}, u32[]{:S(2)}, u32[]{:S(2)}) collective-permute-start(bf16[256,128]{1,0:T(8,128)(2,1)S(1)} %copy-done.5), channel_id=1, source_target_pairs={{0,24},{8,0},{16,8},{24,16},{1,25},{9,1},{17,9},{25,17},{2,26},{10... | collective-permute-start | bytes 196616 | tf_op jit(solution)/shard_map/ppermute | solution.py:232
  103.3 12.1 %all-to-all-start.2 = ((bf16[8,32,128]{2,1,0:T(8,128)(2,1)}), bf16[8,32,128]{2,1,0:T(8,128)(2,1)S(1)}, u32[]{:S(2)}, u32[]{:S(2)}) async-start(bf16[8,32,128]{2,1,0:T(8,128)(2,1)} %add_convert_fusion), calls=%async_computation.2 | async-start | bytes 131072 | tf_op jit(solution)/shard_map/all_to_all | solution.py:228
  115.4 0.0 collective-permute-done.2
  115.4 0.0 collective-permute-done.3
  115.4 0.0 collective-permute-done.4
  115.5 0.6 slice.15
  116.1 0.6 fusion
  116.7 12.1 %all-to-all-done.2 = bf16[8,32,128]{2,1,0:T(8,128)(2,1)S(1)} async-done(((bf16[8,32,128]{2,1,0:T(8,128)(2,1)}), bf16[8,32,128]{2,1,0:T(8,128)(2,1)S(1)}, u32[]{:S(2)}, u32[]{:S(2)}) %all-to-all-start.2) | async-done | bytes 65568 | tf_op jit(solution)/shard_map/all_to_all | solution.py:228
  128.8 0.6 convert_reduce_fusion
  (13 shorter events, 0.1 us)
Async XLA Ops:
  3.3 15.2 %copy-start.3 = (bf16[784,128]{1,0:T(8,128)(2,1)S(1)}, bf16[784,128]{1,0:T(8,128)(2,1)}, u32[]{:S(2)}) copy-start(bf16[784,128]{1,0:T(8,128)(2,1)} %get-tuple-element.25) | copy-start | bytes 602116
  3.3 43.3 %all-to-all-start = ((bf16[8,264,128]{2,1,0:T(8,128)(2,1)}), bf16[8,264,128]{2,1,0:T(8,128)(2,1)S(1)}, u32[]{:S(2)}, u32[]{:S(2)}) async-start(bf16[8,264,128]{2,1,0:T(8,128)(2,1)} %get-tuple-element.24), calls=%async_computation | async-start | bytes 1081344 | tf_op jit(solution)/shard_map/all_to_all | solution.py:202
  32.4 17.3 %copy-start = (bf16[3136,128]{1,0:T(8,128)(2,1)}, bf16[3136,128]{1,0:T(8,128)(2,1)S(1)}, u32[]{:S(2)}) copy-start(bf16[3136,128]{1,0:T(8,128)(2,1)S(1)} %all-gather) | copy-start | bytes 2408452
  46.6 3.1 %copy-start.1 = (bf16[8,264,128]{2,1,0:T(8,128)(2,1)}, bf16[8,264,128]{2,1,0:T(8,128)(2,1)S(1)}, u32[]{:S(2)}) copy-start(bf16[8,264,128]{2,1,0:T(8,128)(2,1)S(1)} %all-to-all-done.recv) | copy-start | bytes 1622020
  46.6 16.4 %collective-permute-start = (bf16[8,264,128]{2,1,0:T(8,128)(2,1)S(1)}, bf16[8,264,128]{2,1,0:T(8,128)(2,1)S(1)}, u32[]{:S(2)}, u32[]{:S(2)}) collective-permute-start(bf16[8,264,128]{2,1,0:T(8,128)(2,1)S(1)} %all-to-all-done.recv), channel_id=1, source_target_pairs={{0,32},{32,0},{1,33},{33,1},{2,34},{34,2},{3,35},{35,3},{4,36},{36... | collective-permute-start | bytes 1622024 | tf_op jit(solution)/shard_map/ppermute | solution.py:207
  63.0 0.8 copy-start.2
  85.9 6.4 %collective-permute-start.1 = (bf16[8,32,128]{2,1,0:T(8,128)(2,1)}, bf16[8,32,128]{2,1,0:T(8,128)(2,1)S(1)}, u32[]{:S(2)}, u32[]{:S(2)}) collective-permute-start(bf16[8,32,128]{2,1,0:T(8,128)(2,1)} %get-tuple-element.34), channel_id=1, source_target_pairs={{0,32},{32,0},{1,33},{33,1},{2,34},{34,2},{3,35},{35,3},{4,36},{36... | collective-permute-start | bytes 196616 | tf_op jit(solution)/shard_map/ppermute | solution.py:225
  92.2 1.6 %copy-start.7 = (bf16[256,128]{1,0:T(8,128)(2,1)S(1)}, bf16[256,128]{1,0:T(8,128)(2,1)}, u32[]{:S(2)}) copy-start(bf16[256,128]{1,0:T(8,128)(2,1)} %get-tuple-element.40) | copy-start | bytes 196612
  92.2 4.4 %copy-start.6 = (bf16[256,128]{1,0:T(8,128)(2,1)S(1)}, bf16[256,128]{1,0:T(8,128)(2,1)}, u32[]{:S(2)}) copy-start(bf16[256,128]{1,0:T(8,128)(2,1)} %get-tuple-element.41) | copy-start | bytes 196612
  92.2 8.4 %copy-start.5 = (bf16[256,128]{1,0:T(8,128)(2,1)S(1)}, bf16[256,128]{1,0:T(8,128)(2,1)}, u32[]{:S(2)}) copy-start(bf16[256,128]{1,0:T(8,128)(2,1)} %get-tuple-element.42) | copy-start | bytes 196612
  93.8 21.6 %copy-start.4 = (bf16[256,128]{1,0:T(8,128)(2,1)S(1)}, bf16[256,128]{1,0:T(8,128)(2,1)}, u32[]{:S(2)}) copy-start(bf16[256,128]{1,0:T(8,128)(2,1)} %get-tuple-element.39) | copy-start | bytes 196612
  93.8 21.6 %collective-permute-start.2 = (bf16[256,128]{1,0:T(8,128)(2,1)S(1)}, bf16[256,128]{1,0:T(8,128)(2,1)S(1)}, u32[]{:S(2)}, u32[]{:S(2)}) collective-permute-start(bf16[256,128]{1,0:T(8,128)(2,1)S(1)} %copy-done.7), channel_id=1, source_target_pairs={{0,8},{8,16},{16,24},{24,0},{1,9},{9,17},{17,25},{25,1},{2,10},{10... | collective-permute-start | bytes 196616 | tf_op jit(solution)/shard_map/ppermute | solution.py:232
  96.6 18.8 %collective-permute-start.3 = (bf16[256,128]{1,0:T(8,128)(2,1)S(1)}, bf16[256,128]{1,0:T(8,128)(2,1)S(1)}, u32[]{:S(2)}, u32[]{:S(2)}) collective-permute-start(bf16[256,128]{1,0:T(8,128)(2,1)S(1)} %copy-done.6), channel_id=1, source_target_pairs={{0,16},{8,24},{16,0},{24,8},{1,17},{9,25},{17,1},{25,9},{2,18},{10... | collective-permute-start | bytes 196616 | tf_op jit(solution)/shard_map/ppermute | solution.py:232
  100.6 14.8 %collective-permute-start.4 = (bf16[256,128]{1,0:T(8,128)(2,1)S(1)}, bf16[256,128]{1,0:T(8,128)(2,1)S(1)}, u32[]{:S(2)}, u32[]{:S(2)}) collective-permute-start(bf16[256,128]{1,0:T(8,128)(2,1)S(1)} %copy-done.5), channel_id=1, source_target_pairs={{0,24},{8,0},{16,8},{24,16},{1,25},{9,1},{17,9},{25,17},{2,26},{10... | collective-permute-start | bytes 196616 | tf_op jit(solution)/shard_map/ppermute | solution.py:232
  103.3 25.5 %all-to-all-start.2 = ((bf16[8,32,128]{2,1,0:T(8,128)(2,1)}), bf16[8,32,128]{2,1,0:T(8,128)(2,1)S(1)}, u32[]{:S(2)}, u32[]{:S(2)}) async-start(bf16[8,32,128]{2,1,0:T(8,128)(2,1)} %add_convert_fusion), calls=%async_computation.2 | async-start | bytes 131072 | tf_op jit(solution)/shard_map/all_to_all | solution.py:228

commit v5 on v3

--- a/solution.py
+++ b/solution.py
@@ -16,7 +16,6 @@
 ST = 4 * T
 XB = ST + 16
 YB = XB + 2 * T
-RB = 4 * T + 2 * T
 f32 = jnp.float32
 bf16 = jnp.bfloat16
 
@@ -119,20 +118,36 @@
 
 
 def received(recv, query_part, key_part, below_end, above_start, dq, dk, dv):
-    def below(j, carry):
-        rows = recv[j, 2 * T : ZB]
-        dq[...] += query_part(recv[j, 0:T], recv[j, T : 2 * T], joined(rows[0:3]))
-        return carry
-
-    def above(j, carry):
-        rows = recv[j, 2 * T : ZB]
-        more = key_part(recv[j, 0:T], recv[j, T : 2 * T], joined(rows[0:3]), joined(rows[3:6]))
+    def block(j, count, at):
+        return recv[pl.ds(j, count), at * T : (at + 1) * T].reshape(count * T, H)
+
+    def stat(j, count, at):
+        rows = [joined(recv[j + i, 2 * T : ZB][at : at + 3]) for i in range(count)]
+        return jnp.concatenate(rows, axis=1)
+
+    def below(j, count):
+        dq[...] += query_part(block(j, count, 0), block(j, count, 1), stat(j, count, 0))
+
+    def above(j, count):
+        more = key_part(block(j, count, 0), block(j, count, 1), stat(j, count, 0), stat(j, count, 3))
         dk[...] += more[0]
         dv[...] += more[1]
-        return carry
-
-    lax.fori_loop(0, below_end, below, 0)
-    lax.fori_loop(above_start, NP, above, 0)
+
+    def over(step, start, end):
+        twos = (end - start) // 2
+
+        def two(i, carry):
+            step(start + 2 * i, 2)
+            return carry
+
+        lax.fori_loop(0, twos, two, 0)
+
+        @pl.when(start + 2 * twos < end)
+        def _():
+            step(end - 1, 1)
+
+    over(below, 0, below_end)
+    over(above, above_start, NP)
 
 
 def first_body(place, recv, grp, dq, dk, dv):
@@ -163,11 +178,12 @@
         ysend[i, 5 * T : 6 * T] = dv[i * T : (i + 1) * T].astype(bf16)
 
 
-def finish_body(place, yrecv, xt, q_out, k_out, v_out, zs, dq):
+def finish_body(place, sums, xt, q_out, k_out, v_out, keep, send, dq, wg):
+    zl = place[1]
     y = place[2]
 
     def total(lo, hi):
-        w = [yrecv[i, lo:hi].astype(f32) for i in range(NY)]
+        w = [sums[i, lo:hi].astype(f32) for i in range(NY)]
         return (w[0] + w[1]) + (w[2] + w[3])
 
     dq[...] = (total(0, 4 * T) * SCALE).astype(bf16)
@@ -176,9 +192,11 @@
     v_out[...] = total(5 * T, 6 * T).astype(bf16)
     acc = None
     for i in range(NY):
-        part = nn(xt[:, i].reshape(NX * NC * 64, T), dq[i * T : (i + 1) * T])
+        part = nn(xt[:, i].reshape(NP * 64, T), dq[i * T : (i + 1) * T])
         acc = part if acc is None else acc + part
-    zs[...] = acc.astype(bf16).reshape(NZ, 32, H)
+    wg[...] = acc.reshape(NP, 2, 32, H)
+    keep[...] = wg[:, pl.ds(zl, 1)].reshape(NP, 32, H)
+    send[...] = wg[:, pl.ds(1 - zl, 1)].reshape(NP, 32, H).astype(bf16)
 
 
 def vmem(count):
@@ -210,13 +228,21 @@
     block = (NY * T, H)
     first = call(first_body, "first", [(block, f32)] * 3, [], 2)
     sums = first(place, recv, grp)
-    second = call(second_body, "second", [((NY, RB, H), bf16)], [pltpu.VMEM(block, f32)] * 3, 5)
+    second = call(second_body, "second", [((NY, 6 * T, H), bf16)], [pltpu.VMEM(block, f32)] * 3, 5)
     (ysend,) = second(place, relayed, grp, *sums)
-    yrecv = lax.all_to_all(ysend, "y", 0, 0, tiled=True)
-    one = ((T, H), bf16)
-    finish = call(finish_body, "finish", [one, one, one, ((NZ, 32, H), bf16)], [pltpu.VMEM(block, bf16)], 2)
-    q_grad, k_grad, v_grad, zs = finish(place, yrecv, xt)
-    back = lax.all_to_all(zs, ("zp", "zl"), 0, 0, tiled=True)
+    sums = lax.all_to_all(ysend, "y", 0, 0, tiled=True)
+    one, part = ((T, H), bf16), (NP, 32, H)
+    finish = call(
+        finish_body,
+        "finish",
+        [one, one, one, (part, f32), (part, bf16)],
+        [pltpu.VMEM(block, bf16), pltpu.VMEM((NP, 2, 32, H), f32)],
+        2,
+    )
+    q_grad, k_grad, v_grad, keep, send = finish(place, sums, xt)
+    other = lax.ppermute(send, "zl", [(0, 1), (1, 0)])
+    pair = (keep + other.astype(f32)).astype(bf16)
+    back = lax.all_to_all(pair, "zp", 0, 0, tiled=True)
     return q_grad, k_grad, v_grad, jnp.sum(back.astype(f32), axis=0)
 
 

time: 116 us -> 122 us (1.052)
  waiting for transfers between devices: 7.67 us -> 11.7 us
  starting transfers between devices: 18.3 us -> 21.5 us
  Pallas kernels: 15.9 us -> 13.7 us
    ppermute x0 -> x1, starting transfers between devices: none -> 3.23 us  [per_device(): other = lax.ppermute(send, 'zl', [(0, 1), (1, 0)])]
    ppermute x0 -> x1, waiting for transfers between devices: none -> 3.12 us  [per_device(): other = lax.ppermute(send, 'zl', [(0, 1), (1, 0)])]
    pallas_call x1, Pallas kernels: 5.82 us -> 4.59 us  [per_device(): ysend, = second(place, relayed, grp, *sums)]
  transfers between devices with their start and end apart: 2 -> 3, of which waited for: 1 -> 2; matrix products, arithmetic and copies ran while one was open for 0% -> 0% of each run, Pallas kernels for 5% -> 4%
where the time goes in v5:
time: 122 us; the launch traced here: 121 us
  blocking collectives  70.5 us (58%)
  starting transfers between devices  21.5 us (18%)
  Pallas kernels  13.7 us (11%)
  waiting for transfers between devices  11.7 us (10%)
  other arithmetic  2.15 us (2%)
    all_to_all x1, blocking collectives, per_device(): back = lax.all_to_all(pair, 'zp', 0, 0, tiled=True)  25.6 us
    all_to_all x1, blocking collectives, per_device(): sums = lax.all_to_all(ysend, 'y', 0, 0, tiled=True)  16.8 us
    all_to_all x1, starting transfers between devices, per_device(): recv = lax.all_to_all(zsend, 'zp', 0, 0, tiled=True)  15.2 us
    all_gather x1, blocking collectives, per_device(): xt = lax.all_gather(jnp.concatenate(part, axis=1), TP, axis=0, tiled=False)  14.2 us
    all_gather x1, blocking collectives, per_device(): grp = lax.all_gather(own, 'y', axis=0, tiled=False)  13.9 us
    ppermute x1, waiting for transfers between devices, per_device(): relayed = lax.ppermute(recv, 'zl', [(0, 1), (1, 0)])  8.57 us
    pallas_call x1, Pallas kernels, per_device(): sums = first(place, recv, grp)  4.72 us
    pallas_call x1, Pallas kernels, per_device(): ysend, = second(place, relayed, grp, *sums)  4.59 us
  transfers between devices with their start and end apart: 3, of which 2 were waited for; matrix products, arithmetic and copies ran while one was open for 0% of the time, Pallas kernels for 4%

profile of v5, /device:TPU:6, one launch (start us, length us, event | category | flops | bytes accessed | tf_op | source)
XLA Modules:
  0.0 121.2 jit_solution(12907147480298317962)
XLA Ops:
  0.6 0.6 pad_add_fusion.place
  1.2 2.1 %pack.1 = (bf16[8,264,128]{2,1,0:T(8,128)(2,1)}, bf16[784,128]{1,0:T(8,128)(2,1)}) custom-call(s32[3]{0:T(128)} %pad_add_fusion.place, bf16[128,128]{1,0:T(8,128)(2,1)} %q.1, bf16[128,128]{1,0:T(8,128)(2,1)} %k.1, bf16[128,128]{1,0:T(8,128)(2,1)} %v.1, f32[1,128]{1,0:T(1,128)} %bitcast.11, f32[1,128]{1,0:T(1,128)} %bitcast.12, bf16[128,128]{1,0:T(8,128)(2,1)} %o.1, ...), custom_call_target="tpu_custom_call" | custom-call | tf_op jit(solution)/shard_map/pack/pallas_call | solution.py:221
  3.4 0.0 copy-start.3
  3.4 15.2 %all-to-all-start = ((bf16[8,264,128]{2,1,0:T(8,128)(2,1)}), bf16[8,264,128]{2,1,0:T(8,128)(2,1)S(1)}, u32[]{:S(2)}, u32[]{:S(2)}) async-start(bf16[8,264,128]{2,1,0:T(8,128)(2,1)} %get-tuple-element.16), calls=%async_computation | async-start | bytes 1081344 | tf_op jit(solution)/shard_map/all_to_all | solution.py:222
  18.6 0.0 copy-done.3
  18.6 13.9 %all-gather = bf16[3136,128]{1,0:T(8,128)(2,1)S(1)} all-gather(bf16[784,128]{1,0:T(8,128)(2,1)S(1)} %copy-done.3), channel_id=2, replica_groups=mesh['zp'=8,'zl'=2,'y'=4,'x'=4,'c'=2] {'y'}, dimensions={0}, use_global_device_ids=true | all-gather | bytes 1003520 | tf_op jit(solution)/shard_map/all_gather | solution.py:223
  32.5 0.0 copy-start
  32.5 14.2 %all-gather.1 = bf16[32,64,128]{2,1,0:T(8,128)(2,1)} all-gather(bf16[4,64,128]{2,1,0:T(8,128)(2,1)S(1)} %pad_maximum_fusion), channel_id=3, replica_groups=mesh['zp'=8,'zl'=2,'y'=4,'x'=4,'c'=2] {'x','c'}, dimensions={0}, use_global_device_ids=true | all-gather | bytes 589824 | tf_op jit(solution)/shard_map/all_gather | solution.py:225
  46.7 0.0 all-to-all-done.recv
  46.7 0.0 copy-start.1
  46.7 3.1 %collective-permute-start = (bf16[8,264,128]{2,1,0:T(8,128)(2,1)S(1)}, bf16[8,264,128]{2,1,0:T(8,128)(2,1)S(1)}, u32[]{:S(2)}, u32[]{:S(2)}) collective-permute-start(bf16[8,264,128]{2,1,0:T(8,128)(2,1)S(1)} %all-to-all-done.recv), channel_id=1, source_target_pairs={{0,32},{32,0},{1,33},{33,1},{2,34},{34,2},{3,35},{35,3},{4,36},{36... | collective-permute-start | bytes 1622024 | tf_op jit(solution)/shard_map/ppermute | solution.py:227
  49.8 0.0 copy-done
  49.8 0.0 copy-done.1
  49.8 4.7 %first.1 = (f32[512,128]{1,0:T(8,128)}, f32[512,128]{1,0:T(8,128)}, f32[512,128]{1,0:T(8,128)}) custom-call(s32[3]{0:T(128)} %pad_add_fusion.place, bf16[8,264,128]{2,1,0:T(8,128)(2,1)} %copy-done.1, bf16[4,784,128]{2,1,0:T(8,128)(2,1)} %bitcast.8), custom_call_target="tpu_custom_call" | custom-call | tf_op jit(solution)/shard_map/first/pallas_call | solution.py:230
  54.5 8.6 %collective-permute-done.recv = bf16[8,264,128]{2,1,0:T(8,128)(2,1)S(1)} collective-permute-done((bf16[8,264,128]{2,1,0:T(8,128)(2,1)S(1)}, bf16[8,264,128]{2,1,0:T(8,128)(2,1)S(1)}, u32[]{:S(2)}, u32[]{:S(2)}) %collective-permute-start) | collective-permute-done | bytes 540704 | tf_op jit(solution)/shard_map/ppermute | solution.py:227
  63.1 0.0 copy-start.2
  63.1 0.8 copy-done.2
  63.9 4.6 %second.1 = bf16[4,768,128]{2,1,0:T(8,128)(2,1)} custom-call(s32[3]{0:T(128)} %pad_add_fusion.place, bf16[8,264,128]{2,1,0:T(8,128)(2,1)} %copy-done.2, bf16[4,784,128]{2,1,0:T(8,128)(2,1)} %bitcast.9, f32[512,128]{1,0:T(8,128)} %get-tuple-element.19.dq0, f32[512,128]{1,0:T(8,128)} %get-tuple-element.20.dk0, f32[512,128]{1,0:T(8,128)} %get-tuple-element.21.dv0), custom_call_target="tpu_custom_call" | custom-call | tf_op jit(solution)/shard_map/second/pallas_call | solution.py:232
  68.5 16.8 %all_to_all.15.sums = bf16[4,768,128]{2,1,0:T(8,128)(2,1)} all-to-all(bf16[4,768,128]{2,1,0:T(8,128)(2,1)} %second.1), channel_id=1, replica_groups=mesh['zp'=8,'zl'=2,'y'=4,'x'=4,'c'=2] {'y'}, dimensions={0} | all-to-all | bytes 1572864 | tf_op jit(solution)/shard_map/all_to_all | solution.py:233
  85.3 2.3 %finish.1 = (bf16[128,128]{1,0:T(8,128)(2,1)}, bf16[128,128]{1,0:T(8,128)(2,1)}, bf16[128,128]{1,0:T(8,128)(2,1)}, f32[8,32,128]{2,1,0:T(8,128)}, bf16[8,32,128]{2,1,0:T(8,128)(2,1)}) custom-call(s32[3]{0:T(128)} %pad_add_fusion.place, bf16[4,768,128]{2,1,0:T(8,128)(2,1)} %all_to_all.15.sums, bf16[8,4,64,128]{3,2,1,0:T(8,128)(2,1)} %bitcast.10), custom_call_target="tpu_custom_call" | custom-call | tf_op jit(solution)/shard_map/finish/pallas_call | solution.py:242
  87.6 3.2 %collective-permute-start.1 = (bf16[8,32,128]{2,1,0:T(8,128)(2,1)}, bf16[8,32,128]{2,1,0:T(8,128)(2,1)S(1)}, u32[]{:S(2)}, u32[]{:S(2)}) collective-permute-start(bf16[8,32,128]{2,1,0:T(8,128)(2,1)} %get-tuple-element.27), channel_id=1, source_target_pairs={{0,32},{32,0},{1,33},{33,1},{2,34},{34,2},{3,35},{35,3},{4,36},{36... | collective-permute-start | bytes 196616 | tf_op jit(solution)/shard_map/ppermute | solution.py:243
  90.9 3.1 %collective-permute-done.1 = bf16[8,32,128]{2,1,0:T(8,128)(2,1)S(1)} collective-permute-done((bf16[8,32,128]{2,1,0:T(8,128)(2,1)}, bf16[8,32,128]{2,1,0:T(8,128)(2,1)S(1)}, u32[]{:S(2)}, u32[]{:S(2)}) %collective-permute-start.1) | collective-permute-done | bytes 65568 | tf_op jit(solution)/shard_map/ppermute | solution.py:243
  94.0 0.9 add_convert_fusion
  94.9 25.6 %all_to_all.16 = bf16[8,32,128]{2,1,0:T(8,128)(2,1)S(1)} all-to-all(bf16[8,32,128]{2,1,0:T(8,128)(2,1)S(1)} %add_convert_fusion), channel_id=1, replica_groups=mesh['zp'=8,'zl'=2,'y'=4,'x'=4,'c'=2] {'zp'}, dimensions={0} | all-to-all | bytes 131072 | tf_op jit(solution)/shard_map/all_to_all | solution.py:245
  120.5 0.6 convert_reduce_fusion
  (2 shorter events, 0.0 us)
Async XLA Ops:
  3.4 15.2 %copy-start.3 = (bf16[784,128]{1,0:T(8,128)(2,1)S(1)}, bf16[784,128]{1,0:T(8,128)(2,1)}, u32[]{:S(2)}) copy-start(bf16[784,128]{1,0:T(8,128)(2,1)} %get-tuple-element.17) | copy-start | bytes 602116
  3.4 43.3 %all-to-all-start = ((bf16[8,264,128]{2,1,0:T(8,128)(2,1)}), bf16[8,264,128]{2,1,0:T(8,128)(2,1)S(1)}, u32[]{:S(2)}, u32[]{:S(2)}) async-start(bf16[8,264,128]{2,1,0:T(8,128)(2,1)} %get-tuple-element.16), calls=%async_computation | async-start | bytes 1081344 | tf_op jit(solution)/shard_map/all_to_all | solution.py:222
  32.5 17.3 %copy-start = (bf16[3136,128]{1,0:T(8,128)(2,1)}, bf16[3136,128]{1,0:T(8,128)(2,1)S(1)}, u32[]{:S(2)}) copy-start(bf16[3136,128]{1,0:T(8,128)(2,1)S(1)} %all-gather) | copy-start | bytes 2408452
  46.7 3.1 %copy-start.1 = (bf16[8,264,128]{2,1,0:T(8,128)(2,1)}, bf16[8,264,128]{2,1,0:T(8,128)(2,1)S(1)}, u32[]{:S(2)}) copy-start(bf16[8,264,128]{2,1,0:T(8,128)(2,1)S(1)} %all-to-all-done.recv) | copy-start | bytes 1622020
  46.7 16.4 %collective-permute-start = (bf16[8,264,128]{2,1,0:T(8,128)(2,1)S(1)}, bf16[8,264,128]{2,1,0:T(8,128)(2,1)S(1)}, u32[]{:S(2)}, u32[]{:S(2)}) collective-permute-start(bf16[8,264,128]{2,1,0:T(8,128)(2,1)S(1)} %all-to-all-done.recv), channel_id=1, source_target_pairs={{0,32},{32,0},{1,33},{33,1},{2,34},{34,2},{3,35},{35,3},{4,36},{36... | collective-permute-start | bytes 1622024 | tf_op jit(solution)/shard_map/ppermute | solution.py:227
  63.1 0.8 copy-start.2
  87.6 6.4 %collective-permute-start.1 = (bf16[8,32,128]{2,1,0:T(8,128)(2,1)}, bf16[8,32,128]{2,1,0:T(8,128)(2,1)S(1)}, u32[]{:S(2)}, u32[]{:S(2)}) collective-permute-start(bf16[8,32,128]{2,1,0:T(8,128)(2,1)} %get-tuple-element.27), channel_id=1, source_target_pairs={{0,32},{32,0},{1,33},{33,1},{2,34},{34,2},{3,35},{35,3},{4,36},{36... | collective-permute-start | bytes 196616 | tf_op jit(solution)/shard_map/ppermute | solution.py:243

commit v6 on v5

--- a/solution.py
+++ b/solution.py
@@ -164,49 +164,45 @@
     received(recv, query_part, key_part, zp, zp + 1, dq, dk, dv)
 
 
-def second_body(place, recv, grp, dq0, dk0, dv0, ysend, dq, dk, dv):
+def second_body(place, recv, grp, dq0, dk0, dv0, q_sums, *rest):
+    kv_sums, (dq, dk, dv) = rest[:NY], rest[NY:]
     border = place[0] + place[1]
+    y = place[2]
     query_part, key_part = parts_of(grp)
     dq[...] = dq0[...]
     dk[...] = dk0[...]
     dv[...] = dv0[...]
     received(recv, query_part, key_part, border, border, dq, dk, dv)
     sums = dq[...].astype(bf16)
-    for i in range(NY):
-        ysend[i, 0 : 4 * T] = sums
-        ysend[i, 4 * T : 5 * T] = dk[i * T : (i + 1) * T].astype(bf16)
-        ysend[i, 5 * T : 6 * T] = dv[i * T : (i + 1) * T].astype(bf16)
-
-
-def finish_body(place, sums, xt, q_out, k_out, v_out, keep, send, dq, wg):
-    zl = place[1]
+    for d in range(NY):
+        at = pl.ds(pl.multiple_of(((y + d) % NY) * T, T), T)
+        q_sums[d] = sums
+        kv_sums[d][0:T] = dk[at].astype(bf16)
+        kv_sums[d][T : 2 * T] = dv[at].astype(bf16)
+
+
+def finish_body(place, sums, *rest):
+    xt, (q_out, zs, dq) = rest[:NX], rest[NX:]
     y = place[2]
-
-    def total(lo, hi):
-        w = [sums[i, lo:hi].astype(f32) for i in range(NY)]
-        return (w[0] + w[1]) + (w[2] + w[3])
-
-    dq[...] = (total(0, 4 * T) * SCALE).astype(bf16)
+    x = place[3]
+    w = [sums[i].astype(f32) for i in range(NY)]
+    dq[...] = (((w[0] + w[1]) + (w[2] + w[3])) * SCALE).astype(bf16)
     q_out[...] = dq[pl.ds(pl.multiple_of(y * T, T), T)]
-    k_out[...] = (total(4 * T, 5 * T) * SCALE).astype(bf16)
-    v_out[...] = total(5 * T, 6 * T).astype(bf16)
-    acc = None
-    for i in range(NY):
-        part = nn(xt[:, i].reshape(NP * 64, T), dq[i * T : (i + 1) * T])
-        acc = part if acc is None else acc + part
-    wg[...] = acc.reshape(NP, 2, 32, H)
-    keep[...] = wg[:, pl.ds(zl, 1)].reshape(NP, 32, H)
-    send[...] = wg[:, pl.ds(1 - zl, 1)].reshape(NP, 32, H).astype(bf16)
+    for d in range(NX):
+        acc = None
+        for i in range(NY):
+            part = nn(xt[d][:, i].reshape(NC * 64, T), dq[i * T : (i + 1) * T])
+            acc = part if acc is None else acc + part
+        zs[pl.ds(((x - d) % NX) * 4, 4)] = acc.astype(bf16).reshape(4, 32, H)
 
 
 def vmem(count):
     return [pl.BlockSpec(memory_space=pltpu.VMEM)] * count
 
 
-def call(body, name, out_shape, scratch, count):
+def call(body, out_shape, scratch, count):
     return pl.pallas_call(
         body,
-        name=name,
         in_specs=[pl.BlockSpec(memory_space=pltpu.SMEM)] + vmem(count),
         out_specs=tuple(vmem(len(out_shape))),
         out_shape=tuple(jax.ShapeDtypeStruct(s, d) for s, d in out_shape),
@@ -216,33 +212,40 @@
 
 def per_device(q, k, v, g, lse, o, do, x):
     y = lax.axis_index("y")
-    place = jnp.stack([lax.axis_index("zp"), lax.axis_index("zl"), y]).astype(jnp.int32)
-    pack = call(pack_body, "pack", [((NP, ZB, H), bf16), ((YB, H), bf16)], [], 8)
+    place = [lax.axis_index("zp"), lax.axis_index("zl"), y, lax.axis_index("x")]
+    place = jnp.stack(place).astype(jnp.int32)
+    pack = call(pack_body, [((NP, ZB, H), bf16), ((YB, H), bf16)], [], 8)
     zsend, own = pack(place, q, k, v, g.reshape(1, T), lse.reshape(1, T), o, do, x)
     recv = lax.all_to_all(zsend, "zp", 0, 0, tiled=True)
     grp = lax.all_gather(own, "y", axis=0, tiled=False)
     part = [lax.dynamic_slice_in_dim(grp, XB + half * T + y * 32, 32, 1) for half in range(2)]
-    xt = lax.all_gather(jnp.concatenate(part, axis=1), TP, axis=0, tiled=False)
+    xt = lax.all_gather(jnp.concatenate(part, axis=1), "c", axis=0, tiled=False)
     recv, xt = lax.optimization_barrier((recv, xt))
+    xts = [xt]
     relayed = lax.ppermute(recv, "zl", [(0, 1), (1, 0)])
+    for d in range(1, NX):
+        xts.append(lax.ppermute(xt, "x", [(i, (i + d) % NX) for i in range(NX)]))
     block = (NY * T, H)
-    first = call(first_body, "first", [(block, f32)] * 3, [], 2)
-    sums = first(place, recv, grp)
-    second = call(second_body, "second", [((NY, 6 * T, H), bf16)], [pltpu.VMEM(block, f32)] * 3, 5)
-    (ysend,) = second(place, relayed, grp, *sums)
-    sums = lax.all_to_all(ysend, "y", 0, 0, tiled=True)
-    one, part = ((T, H), bf16), (NP, 32, H)
-    finish = call(
-        finish_body,
-        "finish",
-        [one, one, one, (part, f32), (part, bf16)],
-        [pltpu.VMEM(block, bf16), pltpu.VMEM((NP, 2, 32, H), f32)],
-        2,
-    )
-    q_grad, k_grad, v_grad, keep, send = finish(place, sums, xt)
-    other = lax.ppermute(send, "zl", [(0, 1), (1, 0)])
-    pair = (keep + other.astype(f32)).astype(bf16)
-    back = lax.all_to_all(pair, "zp", 0, 0, tiled=True)
+    sums = call(first_body, [(block, f32)] * 3, [], 2)(place, recv, grp)
+    second = call(
+        second_body,
+        [((NY, NY * T, H), bf16)] + [((2 * T, H), bf16)] * NY,
+        [pltpu.VMEM(block, f32)] * 3,
+        5,
+    )
+    q_sums, *kv = second(place, relayed, grp, *sums)
+    q_sums = lax.all_to_all(q_sums, "y", 0, 0, tiled=True)
+    outs = [((T, H), bf16), ((NZ, 32, H), bf16)]
+    finish = call(finish_body, outs, [pltpu.VMEM(block, bf16)], 1 + NX)
+    q_grad, zs = finish(place, q_sums, *xts)
+    zs, *kv = lax.optimization_barrier((zs, *kv))
+    back = lax.all_to_all(zs, ("zp", "zl"), 0, 0, tiled=True)
+    total = kv[0].astype(f32)
+    for d in range(1, NY):
+        turned = lax.ppermute(kv[d], "y", [(i, (i + d) % NY) for i in range(NY)])
+        total = total + turned.astype(f32)
+    k_grad = (total[0:T] * SCALE).astype(bf16)
+    v_grad = total[T : 2 * T].astype(bf16)
     return q_grad, k_grad, v_grad, jnp.sum(back.astype(f32), axis=0)
 
 

time: 122 us -> 126 us (1.033)
  blocking collectives: 70.5 us -> 15.8 us
  starting transfers between devices: 21.5 us -> 54 us
  waiting for transfers between devices: 11.7 us -> 36 us
  local copies, waits for them, and re-layouts: 0.82 us -> 2.95 us
    all_to_all x2 -> x0, blocking collectives: 42.5 us -> none  [the longest x1 25.6 us: per_device(): back = lax.all_to_all(pair, 'zp', 0, 0, tiled=True)]
    ppermute x1 -> x6, starting transfers between devices: 3.23 us -> 20.7 us  [the longest x3 12 us: per_device(): turned = lax.ppermute(kv[d], 'y', [(i, (i + d) % NY) for i in range(NY)])]
    all_to_all x0 -> x2, starting transfers between devices: none -> 14.1 us  [the longest x1 9.68 us: per_device(): back = lax.all_to_all(zs, ('zp', 'zl'), 0, 0, tiled=True)]
    all_gather x1, blocking collectives: 14.2 us -> 1.9 us  [per_device(): xt = lax.all_gather(jnp.concatenate(part, axis=1), 'c', axis=0, tiled=False)]
    all_to_all x0 -> x2, waiting for transfers between devices: none -> 11.8 us  [the longest x1 11.8 us: per_device(): back = lax.all_to_all(zs, ('zp', 'zl'), 0, 0, tiled=True)]
    all_to_all x1, waiting for transfers between devices: 0.01 us -> 11.5 us  [per_device(): recv = lax.all_to_all(zsend, 'zp', 0, 0, tiled=True)]
    ppermute x1 -> x6, waiting for transfers between devices: 3.12 us -> 6.13 us  [the longest x3 6.12 us: per_device(): xts.append(lax.ppermute(xt, 'x', [(i, (i + d) % NX) for i in range(NX)]))]
    ppermute x1, waiting for transfers between devices: 8.57 us -> 6.52 us  [per_device(): relayed = lax.ppermute(recv, 'zl', [(0, 1), (1, 0)])]
  transfers between devices with their start and end apart: 3 -> 10, of which waited for: 2 -> 5; matrix products, arithmetic and copies ran while one was open for 0% -> 1% of each run, Pallas kernels for 4% -> 4%
where the time goes in v6:
time: 126 us; the launch traced here: 125 us
  starting transfers between devices  54 us (43%)
  waiting for transfers between devices  36 us (29%)
  blocking collectives  15.8 us (13%)
  Pallas kernels  13.6 us (11%)
  local copies, waits for them, and re-layouts  2.95 us (2%)
  other arithmetic  1.9 us (2%)
    all_to_all x1, starting transfers between devices, per_device(): recv = lax.all_to_all(zsend, 'zp', 0, 0, tiled=True)  15.2 us
    all_gather x1, blocking collectives, per_device(): grp = lax.all_gather(own, 'y', axis=0, tiled=False)  13.9 us
    ppermute x3, starting transfers between devices, per_device(): turned = lax.ppermute(kv[d], 'y', [(i, (i + d) % NY) for i in range(NY)])  12 us
    all_to_all x1, waiting for transfers between devices, per_device(): back = lax.all_to_all(zs, ('zp', 'zl'), 0, 0, tiled=True)  11.8 us
    all_to_all x1, waiting for transfers between devices, per_device(): recv = lax.all_to_all(zsend, 'zp', 0, 0, tiled=True)  11.5 us
    all_to_all x1, starting transfers between devices, per_device(): back = lax.all_to_all(zs, ('zp', 'zl'), 0, 0, tiled=True)  9.68 us
    ppermute x3, starting transfers between devices, per_device(): xts.append(lax.ppermute(xt, 'x', [(i, (i + d) % NX) for i in range(NX)]))  8.76 us
    ppermute x1, waiting for transfers between devices, per_device(): relayed = lax.ppermute(recv, 'zl', [(0, 1), (1, 0)])  6.52 us
  transfers between devices with their start and end apart: 10, of which 5 were waited for; matrix products, arithmetic and copies ran while one was open for 1% of the time, Pallas kernels for 4%

profile of v6, /device:TPU:6, one launch (start us, length us, event | category | flops | bytes accessed | tf_op | source)
XLA Modules:
  0.0 125.0 jit_solution(13449368790574777545)
XLA Ops:
  0.6 0.6 pad_add_fusion.place
  1.2 2.1 %shard_map.111 = (bf16[8,264,128]{2,1,0:T(8,128)(2,1)}, bf16[784,128]{1,0:T(8,128)(2,1)}) custom-call(s32[4]{0:T(128)} %pad_add_fusion.place, bf16[128,128]{1,0:T(8,128)(2,1)} %q.1, bf16[128,128]{1,0:T(8,128)(2,1)} %k.1, bf16[128,128]{1,0:T(8,128)(2,1)} %v.1, f32[1,128]{1,0:T(1,128)} %bitcast.15, f32[1,128]{1,0:T(1,128)} %bitcast.16, bf16[128,128]{1,0:T(8,128)(2,1)} %o.1, ...), custom_call_target="tpu_custom_call" | custom-call | tf_op jit(solution)/shard_map/pallas_call | solution.py:218
  3.4 15.2 %all-to-all-start = ((bf16[8,264,128]{2,1,0:T(8,128)(2,1)}), bf16[8,264,128]{2,1,0:T(8,128)(2,1)S(1)}, u32[]{:S(2)}, u32[]{:S(2)}) async-start(bf16[8,264,128]{2,1,0:T(8,128)(2,1)} %get-tuple-element.23), calls=%async_computation | async-start | bytes 1081344 | tf_op jit(solution)/shard_map/all_to_all | solution.py:219
  18.6 13.9 %all-gather = bf16[3136,128]{1,0:T(8,128)(2,1)S(1)} all-gather(bf16[784,128]{1,0:T(8,128)(2,1)S(1)} %copy-done.5), channel_id=2, replica_groups=mesh['zp'=8,'zl'=2,'y'=4,'x'=4,'c'=2] {'y'}, dimensions={0}, use_global_device_ids=true | all-gather | bytes 1003520 | tf_op jit(solution)/shard_map/all_gather | solution.py:220
  32.5 1.9 %all-gather.1 = bf16[8,64,128]{2,1,0:T(8,128)(2,1)S(1)} all-gather(bf16[4,64,128]{2,1,0:T(8,128)(2,1)S(1)} %pad_maximum_fusion), channel_id=3, replica_groups=mesh['zp'=8,'zl'=2,'y'=4,'x'=4,'c'=2] {'c'}, dimensions={0}, use_global_device_ids=true | all-gather | bytes 196608 | tf_op jit(solution)/shard_map/all_gather | solution.py:222
  34.4 11.5 %all-to-all-done.recv = bf16[8,264,128]{2,1,0:T(8,128)(2,1)S(1)} async-done(((bf16[8,264,128]{2,1,0:T(8,128)(2,1)}), bf16[8,264,128]{2,1,0:T(8,128)(2,1)S(1)}, u32[]{:S(2)}, u32[]{:S(2)}) %all-to-all-start) | async-done | bytes 540704 | tf_op jit(solution)/shard_map/all_to_all | solution.py:219
  45.9 3.8 %collective-permute-start = (bf16[8,264,128]{2,1,0:T(8,128)(2,1)S(1)}, bf16[8,264,128]{2,1,0:T(8,128)(2,1)S(1)}, u32[]{:S(2)}, u32[]{:S(2)}) collective-permute-start(bf16[8,264,128]{2,1,0:T(8,128)(2,1)S(1)} %all-to-all-done.recv), channel_id=1, source_target_pairs={{0,32},{32,0},{1,33},{33,1},{2,34},{34,2},{3,35},{35,3},{4,36},{36... | collective-permute-start | bytes 1622024 | tf_op jit(solution)/shard_map/ppermute | solution.py:225
  49.8 4.7 %shard_map.112 = (f32[512,128]{1,0:T(8,128)}, f32[512,128]{1,0:T(8,128)}, f32[512,128]{1,0:T(8,128)}) custom-call(s32[4]{0:T(128)} %pad_add_fusion.place, bf16[8,264,128]{2,1,0:T(8,128)(2,1)} %copy-done.1, bf16[4,784,128]{2,1,0:T(8,128)(2,1)} %bitcast.9), custom_call_target="tpu_custom_call" | custom-call | tf_op jit(solution)/shard_map/pallas_call | solution.py:229
  54.5 6.5 %collective-permute-done.recv = bf16[8,264,128]{2,1,0:T(8,128)(2,1)S(1)} collective-permute-done((bf16[8,264,128]{2,1,0:T(8,128)(2,1)S(1)}, bf16[8,264,128]{2,1,0:T(8,128)(2,1)S(1)}, u32[]{:S(2)}, u32[]{:S(2)}) %collective-permute-start) | collective-permute-done | bytes 540704 | tf_op jit(solution)/shard_map/ppermute | solution.py:225
  61.1 0.8 copy-done.3
  61.9 4.5 %shard_map.113 = (bf16[4,512,128]{2,1,0:T(8,128)(2,1)}, bf16[256,128]{1,0:T(8,128)(2,1)}, bf16[256,128]{1,0:T(8,128)(2,1)}, bf16[256,128]{1,0:T(8,128)(2,1)}, bf16[256,128]{1,0:T(8,128)(2,1)}) custom-call(s32[4]{0:T(128)} %pad_add_fusion.place, bf16[8,264,128]{2,1,0:T(8,128)(2,1)} %copy-done.3, bf16[4,784,128]{2,1,0:T(8,128)(2,1)} %bitcast.10, ...), custom_call_target="tpu_custom_call" | custom-call | tf_op jit(solution)/shard_map/pallas_call | solution.py:236
  66.4 4.5 %all-to-all-start.1 = ((bf16[4,512,128]{2,1,0:T(8,128)(2,1)}), bf16[4,512,128]{2,1,0:T(8,128)(2,1)S(1)}, u32[]{:S(2)}, u32[]{:S(2)}) async-start(bf16[4,512,128]{2,1,0:T(8,128)(2,1)} %get-tuple-element.29), calls=%async_computation.1 | async-start | bytes 1048576 | tf_op jit(solution)/shard_map/all_to_all | solution.py:237
  70.9 2.5 %collective-permute-start.1 = (bf16[2,4,64,128]{3,2,1,0:T(8,128)(2,1)S(1)}, bf16[2,4,64,128]{3,2,1,0:T(8,128)(2,1)S(1)}, u32[]{:S(2)}, u32[]{:S(2)}) collective-permute-start(bf16[2,4,64,128]{3,2,1,0:T(8,128)(2,1)S(1)} %bitcast.11), channel_id=1, source_target_pairs={{0,2},{2,4},{4,6},{6,0},{1,3},{3,5},{5,7},{7,1},{8,10},{10,12},{12... | collective-permute-start | bytes 393224 | tf_op jit(solution)/shard_map/ppermute | solution.py:227
  73.4 4.3 %collective-permute-start.2 = (bf16[2,4,64,128]{3,2,1,0:T(8,128)(2,1)S(1)}, bf16[2,4,64,128]{3,2,1,0:T(8,128)(2,1)S(1)}, u32[]{:S(2)}, u32[]{:S(2)}) collective-permute-start(bf16[2,4,64,128]{3,2,1,0:T(8,128)(2,1)S(1)} %bitcast.12), channel_id=1, source_target_pairs={{0,4},{2,6},{4,0},{6,2},{1,5},{3,7},{5,1},{7,3},{8,12},{10,14},{12... | collective-permute-start | bytes 393224 | tf_op jit(solution)/shard_map/ppermute | solution.py:227
  77.8 1.9 %collective-permute-start.3 = (bf16[2,4,64,128]{3,2,1,0:T(8,128)(2,1)S(1)}, bf16[2,4,64,128]{3,2,1,0:T(8,128)(2,1)S(1)}, u32[]{:S(2)}, u32[]{:S(2)}) collective-permute-start(bf16[2,4,64,128]{3,2,1,0:T(8,128)(2,1)S(1)} %bitcast.13), channel_id=1, source_target_pairs={{0,6},{2,0},{4,2},{6,4},{1,7},{3,1},{5,3},{7,5},{8,14},{10,8},{12,... | collective-permute-start | bytes 393224 | tf_op jit(solution)/shard_map/ppermute | solution.py:227
  79.7 0.0 collective-permute-done.1.rest_1_
  79.7 3.0 %collective-permute-done.2.rest_2_ = bf16[2,4,64,128]{3,2,1,0:T(8,128)(2,1)S(1)} collective-permute-done((bf16[2,4,64,128]{3,2,1,0:T(8,128)(2,1)S(1)}, bf16[2,4,64,128]{3,2,1,0:T(8,128)(2,1)S(1)}, u32[]{:S(2)}, u32[]{:S(2)}) %collective-permute-start.2) | collective-permute-done | bytes 131104 | tf_op jit(solution)/shard_map/ppermute | solution.py:227
  82.7 3.1 %collective-permute-done.3.rest_3_ = bf16[2,4,64,128]{3,2,1,0:T(8,128)(2,1)S(1)} collective-permute-done((bf16[2,4,64,128]{3,2,1,0:T(8,128)(2,1)S(1)}, bf16[2,4,64,128]{3,2,1,0:T(8,128)(2,1)S(1)}, u32[]{:S(2)}, u32[]{:S(2)}) %collective-permute-start.3) | collective-permute-done | bytes 131104 | tf_op jit(solution)/shard_map/ppermute | solution.py:227
  85.8 0.0 all-to-all-done.1.sums
  85.9 0.6 copy-done.8
  86.5 0.8 copy-done.2
  87.3 2.2 %shard_map.114 = (bf16[128,128]{1,0:T(8,128)(2,1)}, bf16[16,32,128]{2,1,0:T(8,128)(2,1)}) custom-call(s32[4]{0:T(128)} %pad_add_fusion.place, bf16[4,512,128]{2,1,0:T(8,128)(2,1)} %copy-done.2, bf16[2,4,64,128]{3,2,1,0:T(8,128)(2,1)} %bitcast.14, bf16[2,4,64,128]{3,2,1,0:T(8,128)(2,1)} %copy-done.6, bf16[2,4,64,128]{3,2,1,0:T(8,128)(2,1)} %copy-done.7, ...), custom_call_target="tpu_custom_call" | custom-call | tf_op jit(solution)/shard_map/pallas_call | solution.py:240
  89.5 4.0 %collective-permute-start.4 = (bf16[256,128]{1,0:T(8,128)(2,1)S(1)}, bf16[256,128]{1,0:T(8,128)(2,1)S(1)}, u32[]{:S(2)}, u32[]{:S(2)}) collective-permute-start(bf16[256,128]{1,0:T(8,128)(2,1)S(1)} %copy-done.12), channel_id=1, source_target_pairs={{0,8},{8,16},{16,24},{24,0},{1,9},{9,17},{17,25},{25,1},{2,10},{10... | collective-permute-start | bytes 196616 | tf_op jit(solution)/shard_map/ppermute | solution.py:245
  93.6 4.6 %collective-permute-start.5 = (bf16[256,128]{1,0:T(8,128)(2,1)S(1)}, bf16[256,128]{1,0:T(8,128)(2,1)S(1)}, u32[]{:S(2)}, u32[]{:S(2)}) collective-permute-start(bf16[256,128]{1,0:T(8,128)(2,1)S(1)} %copy-done.11), channel_id=1, source_target_pairs={{0,16},{8,24},{16,0},{24,8},{1,17},{9,25},{17,1},{25,9},{2,18},{10... | collective-permute-start | bytes 196616 | tf_op jit(solution)/shard_map/ppermute | solution.py:245
  98.2 3.4 %collective-permute-start.6 = (bf16[256,128]{1,0:T(8,128)(2,1)S(1)}, bf16[256,128]{1,0:T(8,128)(2,1)S(1)}, u32[]{:S(2)}, u32[]{:S(2)}) collective-permute-start(bf16[256,128]{1,0:T(8,128)(2,1)S(1)} %copy-done.10), channel_id=1, source_target_pairs={{0,24},{8,0},{16,8},{24,16},{1,25},{9,1},{17,9},{25,17},{2,26},{10... | collective-permute-start | bytes 196616 | tf_op jit(solution)/shard_map/ppermute | solution.py:245
  101.6 9.7 %all-to-all-start.2 = ((bf16[16,32,128]{2,1,0:T(8,128)(2,1)}), bf16[16,32,128]{2,1,0:T(8,128)(2,1)S(1)}, u32[]{:S(2)}, u32[]{:S(2)}) async-start(bf16[16,32,128]{2,1,0:T(8,128)(2,1)} %get-tuple-element.41), calls=%async_computation.2 | async-start | bytes 262144 | tf_op jit(solution)/shard_map/all_to_all | solution.py:242
  111.3 0.0 collective-permute-done.4
  111.3 0.0 collective-permute-done.5
  111.3 0.6 slice.15
  112.0 0.6 fusion
  112.6 11.8 %all-to-all-done.2 = bf16[16,32,128]{2,1,0:T(8,128)(2,1)S(1)} async-done(((bf16[16,32,128]{2,1,0:T(8,128)(2,1)}), bf16[16,32,128]{2,1,0:T(8,128)(2,1)S(1)}, u32[]{:S(2)}, u32[]{:S(2)}) %all-to-all-start.2) | async-done | bytes 131104 | tf_op jit(solution)/shard_map/all_to_all | solution.py:242
  124.3 0.6 convert_reduce_fusion
  (27 shorter events, 0.1 us)
Async XLA Ops:
  3.4 15.2 %copy-start.5 = (bf16[784,128]{1,0:T(8,128)(2,1)S(1)}, bf16[784,128]{1,0:T(8,128)(2,1)}, u32[]{:S(2)}) copy-start(bf16[784,128]{1,0:T(8,128)(2,1)} %get-tuple-element.24) | copy-start | bytes 602116
  3.4 42.6 %all-to-all-start = ((bf16[8,264,128]{2,1,0:T(8,128)(2,1)}), bf16[8,264,128]{2,1,0:T(8,128)(2,1)S(1)}, u32[]{:S(2)}, u32[]{:S(2)}) async-start(bf16[8,264,128]{2,1,0:T(8,128)(2,1)} %get-tuple-element.23), calls=%async_computation | async-start | bytes 1081344 | tf_op jit(solution)/shard_map/all_to_all | solution.py:219
  32.5 17.3 %copy-start = (bf16[3136,128]{1,0:T(8,128)(2,1)}, bf16[3136,128]{1,0:T(8,128)(2,1)S(1)}, u32[]{:S(2)}) copy-start(bf16[3136,128]{1,0:T(8,128)(2,1)S(1)} %all-gather) | copy-start | bytes 2408452
  34.4 43.4 %copy-start.4 = (bf16[8,64,128]{2,1,0:T(8,128)(2,1)}, bf16[8,64,128]{2,1,0:T(8,128)(2,1)S(1)}, u32[]{:S(2)}) copy-start(bf16[8,64,128]{2,1,0:T(8,128)(2,1)S(1)} %all-gather.1) | copy-start | bytes 393220
  45.9 3.9 %copy-start.1 = (bf16[8,264,128]{2,1,0:T(8,128)(2,1)}, bf16[8,264,128]{2,1,0:T(8,128)(2,1)S(1)}, u32[]{:S(2)}) copy-start(bf16[8,264,128]{2,1,0:T(8,128)(2,1)S(1)} %all-to-all-done.recv) | copy-start | bytes 1622020
  45.9 15.1 %collective-permute-start = (bf16[8,264,128]{2,1,0:T(8,128)(2,1)S(1)}, bf16[8,264,128]{2,1,0:T(8,128)(2,1)S(1)}, u32[]{:S(2)}, u32[]{:S(2)}) collective-permute-start(bf16[8,264,128]{2,1,0:T(8,128)(2,1)S(1)} %all-to-all-done.recv), channel_id=1, source_target_pairs={{0,32},{32,0},{1,33},{33,1},{2,34},{34,2},{3,35},{35,3},{4,36},{36... | collective-permute-start | bytes 1622024 | tf_op jit(solution)/shard_map/ppermute | solution.py:225
  61.1 0.8 copy-start.3
  66.4 19.4 %all-to-all-start.1 = ((bf16[4,512,128]{2,1,0:T(8,128)(2,1)}), bf16[4,512,128]{2,1,0:T(8,128)(2,1)S(1)}, u32[]{:S(2)}, u32[]{:S(2)}) async-start(bf16[4,512,128]{2,1,0:T(8,128)(2,1)} %get-tuple-element.29), calls=%async_computation.1 | async-start | bytes 1048576 | tf_op jit(solution)/shard_map/all_to_all | solution.py:237
  70.9 18.6 %copy-start.12 = (bf16[256,128]{1,0:T(8,128)(2,1)S(1)}, bf16[256,128]{1,0:T(8,128)(2,1)}, u32[]{:S(2)}) copy-start(bf16[256,128]{1,0:T(8,128)(2,1)} %get-tuple-element.38) | copy-start | bytes 196612
  70.9 22.7 %copy-start.11 = (bf16[256,128]{1,0:T(8,128)(2,1)S(1)}, bf16[256,128]{1,0:T(8,128)(2,1)}, u32[]{:S(2)}) copy-start(bf16[256,128]{1,0:T(8,128)(2,1)} %get-tuple-element.39) | copy-start | bytes 196612
  70.9 27.3 %copy-start.10 = (bf16[256,128]{1,0:T(8,128)(2,1)S(1)}, bf16[256,128]{1,0:T(8,128)(2,1)}, u32[]{:S(2)}) copy-start(bf16[256,128]{1,0:T(8,128)(2,1)} %get-tuple-element.40) | copy-start | bytes 196612
  70.9 8.8 %collective-permute-start.1 = (bf16[2,4,64,128]{3,2,1,0:T(8,128)(2,1)S(1)}, bf16[2,4,64,128]{3,2,1,0:T(8,128)(2,1)S(1)}, u32[]{:S(2)}, u32[]{:S(2)}) collective-permute-start(bf16[2,4,64,128]{3,2,1,0:T(8,128)(2,1)S(1)} %bitcast.11), channel_id=1, source_target_pairs={{0,2},{2,4},{4,6},{6,0},{1,3},{3,5},{5,7},{7,1},{8,10},{10,12},{12... | collective-permute-start | bytes 393224 | tf_op jit(solution)/shard_map/ppermute | solution.py:227
  73.4 9.3 %collective-permute-start.2 = (bf16[2,4,64,128]{3,2,1,0:T(8,128)(2,1)S(1)}, bf16[2,4,64,128]{3,2,1,0:T(8,128)(2,1)S(1)}, u32[]{:S(2)}, u32[]{:S(2)}) collective-permute-start(bf16[2,4,64,128]{3,2,1,0:T(8,128)(2,1)S(1)} %bitcast.12), channel_id=1, source_target_pairs={{0,4},{2,6},{4,0},{6,2},{1,5},{3,7},{5,1},{7,3},{8,12},{10,14},{12... | collective-permute-start | bytes 393224 | tf_op jit(solution)/shard_map/ppermute | solution.py:227
  77.8 8.1 %collective-permute-start.3 = (bf16[2,4,64,128]{3,2,1,0:T(8,128)(2,1)S(1)}, bf16[2,4,64,128]{3,2,1,0:T(8,128)(2,1)S(1)}, u32[]{:S(2)}, u32[]{:S(2)}) collective-permute-start(bf16[2,4,64,128]{3,2,1,0:T(8,128)(2,1)S(1)} %bitcast.13), channel_id=1, source_target_pairs={{0,6},{2,0},{4,2},{6,4},{1,7},{3,1},{5,3},{7,5},{8,14},{10,8},{12,... | collective-permute-start | bytes 393224 | tf_op jit(solution)/shard_map/ppermute | solution.py:227
  79.7 6.1 %copy-start.6 = (bf16[2,4,64,128]{3,2,1,0:T(8,128)(2,1)}, bf16[2,4,64,128]{3,2,1,0:T(8,128)(2,1)S(1)}, u32[]{:S(2)}) copy-start(bf16[2,4,64,128]{3,2,1,0:T(8,128)(2,1)S(1)} %collective-permute-done.1.rest_1_) | copy-start | bytes 393220
  82.7 3.1 %copy-start.7 = (bf16[2,4,64,128]{3,2,1,0:T(8,128)(2,1)}, bf16[2,4,64,128]{3,2,1,0:T(8,128)(2,1)S(1)}, u32[]{:S(2)}) copy-start(bf16[2,4,64,128]{3,2,1,0:T(8,128)(2,1)S(1)} %collective-permute-done.2.rest_2_) | copy-start | bytes 393220
  85.8 0.7 copy-start.8
  86.5 0.8 copy-start.2
  89.5 21.8 %copy-start.9 = (bf16[256,128]{1,0:T(8,128)(2,1)S(1)}, bf16[256,128]{1,0:T(8,128)(2,1)}, u32[]{:S(2)}) copy-start(bf16[256,128]{1,0:T(8,128)(2,1)} %get-tuple-element.37) | copy-start | bytes 196612
  89.5 21.7 %collective-permute-start.4 = (bf16[256,128]{1,0:T(8,128)(2,1)S(1)}, bf16[256,128]{1,0:T(8,128)(2,1)S(1)}, u32[]{:S(2)}, u32[]{:S(2)}) collective-permute-start(bf16[256,128]{1,0:T(8,128)(2,1)S(1)} %copy-done.12), channel_id=1, source_target_pairs={{0,8},{8,16},{16,24},{24,0},{1,9},{9,17},{17,25},{25,1},{2,10},{10... | collective-permute-start | bytes 196616 | tf_op jit(solution)/shard_map/ppermute | solution.py:245
  93.6 17.7 %collective-permute-start.5 = (bf16[256,128]{1,0:T(8,128)(2,1)S(1)}, bf16[256,128]{1,0:T(8,128)(2,1)S(1)}, u32[]{:S(2)}, u32[]{:S(2)}) collective-permute-start(bf16[256,128]{1,0:T(8,128)(2,1)S(1)} %copy-done.11), channel_id=1, source_target_pairs={{0,16},{8,24},{16,0},{24,8},{1,17},{9,25},{17,1},{25,9},{2,18},{10... | collective-permute-start | bytes 196616 | tf_op jit(solution)/shard_map/ppermute | solution.py:245
  98.2 13.1 %collective-permute-start.6 = (bf16[256,128]{1,0:T(8,128)(2,1)S(1)}, bf16[256,128]{1,0:T(8,128)(2,1)S(1)}, u32[]{:S(2)}, u32[]{:S(2)}) collective-permute-start(bf16[256,128]{1,0:T(8,128)(2,1)S(1)} %copy-done.10), channel_id=1, source_target_pairs={{0,24},{8,0},{16,8},{24,16},{1,25},{9,1},{17,9},{25,17},{2,26},{10... | collective-permute-start | bytes 196616 | tf_op jit(solution)/shard_map/ppermute | solution.py:245
  101.6 22.8 %all-to-all-start.2 = ((bf16[16,32,128]{2,1,0:T(8,128)(2,1)}), bf16[16,32,128]{2,1,0:T(8,128)(2,1)S(1)}, u32[]{:S(2)}, u32[]{:S(2)}) async-start(bf16[16,32,128]{2,1,0:T(8,128)(2,1)} %get-tuple-element.41), calls=%async_computation.2 | async-start | bytes 262144 | tf_op jit(solution)/shard_map/all_to_all | solution.py:242

commit v7 on v6

--- a/solution.py
+++ b/solution.py
@@ -1,3 +1,5 @@
+import functools
+
 import jax
 import jax.numpy as jnp
 from jax import lax
@@ -9,6 +11,7 @@
 SP = ("zp", "zl", "y")
 TP = ("x", "c")
 NZ, NP, NY, NX, NC = 16, 8, 4, 4, 2
+CUT = 5
 T = 128
 H = 128
 SCALE = H**-0.5
@@ -36,9 +39,8 @@
     return [hi, mid, low]
 
 
-def pack_body(place, q, k, v, g, lse, o, do, x, zsend, own):
-    zp = place[0]
-    zl = place[1]
+def pack_body(q, k, v, g, lse, o, do, x, zsend, own):
+    zp, zl, _, _ = position()
     terms = o[...].astype(f32) * do[...].astype(f32)
     r = jnp.sum(terms.T, axis=0, keepdims=True)
     gate = g[...]
@@ -117,7 +119,7 @@
     return query_part, key_part
 
 
-def received(recv, query_part, key_part, below_end, above_start, dq, dk, dv):
+def received(recv, query_part, key_part, below_end, above_start, end, dq, dk, dv):
     def block(j, count, at):
         return recv[pl.ds(j, count), at * T : (at + 1) * T].reshape(count * T, H)
 
@@ -147,12 +149,11 @@
             step(end - 1, 1)
 
     over(below, 0, below_end)
-    over(above, above_start, NP)
-
-
-def first_body(place, recv, grp, dq, dk, dv):
-    zp = place[0]
-    y = place[2]
+    over(above, above_start, end)
+
+
+def first_body(recv, grp, dq, dk, dv):
+    zp, _, y, _ = position()
     query_part, key_part = parts_of(grp)
     big = lax.broadcasted_iota(jnp.int32, (NY * T, T), 0)
     small = lax.broadcasted_iota(jnp.int32, (NY * T, T), 1) + y * T
@@ -161,18 +162,24 @@
     dk[...], dv[...] = key_part(
         grp[y, 0:T], grp[y, T : 2 * T], joined(st[0:3]), joined(st[3:6]), big <= small
     )
-    received(recv, query_part, key_part, zp, zp + 1, dq, dk, dv)
-
-
-def second_body(place, recv, grp, dq0, dk0, dv0, q_sums, *rest):
-    kv_sums, (dq, dk, dv) = rest[:NY], rest[NY:]
-    border = place[0] + place[1]
-    y = place[2]
+    received(recv, query_part, key_part, zp, zp + 1, NP, dq, dk, dv)
+
+
+def more_body(low, recv, grp, dq0, dk0, dv0, dq, dk, dv):
+    size = recv.shape[0]
+    zp, zl, _, _ = position()
+    border = jnp.clip(zp + zl - low, 0, size)
     query_part, key_part = parts_of(grp)
     dq[...] = dq0[...]
     dk[...] = dk0[...]
     dv[...] = dv0[...]
-    received(recv, query_part, key_part, border, border, dq, dk, dv)
+    received(recv, query_part, key_part, border, border, size, dq, dk, dv)
+
+
+def last_body(recv, grp, dq0, dk0, dv0, q_sums, *rest):
+    kv_sums, (dq, dk, dv) = rest[:NY], rest[NY:]
+    y = position()[2]
+    more_body(CUT, recv, grp, dq0, dk0, dv0, dq, dk, dv)
     sums = dq[...].astype(bf16)
     for d in range(NY):
         at = pl.ds(pl.multiple_of(((y + d) % NY) * T, T), T)
@@ -181,29 +188,33 @@
         kv_sums[d][T : 2 * T] = dv[at].astype(bf16)
 
 
-def finish_body(place, sums, *rest):
+def finish_body(sums, *rest):
     xt, (q_out, zs, dq) = rest[:NX], rest[NX:]
-    y = place[2]
-    x = place[3]
+    _, _, y, x = position()
     w = [sums[i].astype(f32) for i in range(NY)]
     dq[...] = (((w[0] + w[1]) + (w[2] + w[3])) * SCALE).astype(bf16)
     q_out[...] = dq[pl.ds(pl.multiple_of(y * T, T), T)]
+    acc = None
+    for i in range(0, NY, 2):
+        cols = [jnp.concatenate([xt[d][:, i + e].reshape(T, T) for d in range(NX)], axis=0) for e in range(2)]
+        part = nn(jnp.concatenate(cols, axis=1), dq[i * T : (i + 2) * T])
+        acc = part if acc is None else acc + part
     for d in range(NX):
-        acc = None
-        for i in range(NY):
-            part = nn(xt[d][:, i].reshape(NC * 64, T), dq[i * T : (i + 1) * T])
-            acc = part if acc is None else acc + part
-        zs[pl.ds(((x - d) % NX) * 4, 4)] = acc.astype(bf16).reshape(4, 32, H)
+        zs[pl.ds(((x - d) % NX) * 4, 4)] = acc[d * T : (d + 1) * T].astype(bf16).reshape(4, 32, H)
 
 
 def vmem(count):
     return [pl.BlockSpec(memory_space=pltpu.VMEM)] * count
+
+
+def position():
+    return [lax.axis_index(n) for n in ("zp", "zl", "y", "x")]
 
 
 def call(body, out_shape, scratch, count):
     return pl.pallas_call(
         body,
-        in_specs=[pl.BlockSpec(memory_space=pltpu.SMEM)] + vmem(count),
+        in_specs=vmem(count),
         out_specs=tuple(vmem(len(out_shape))),
         out_shape=tuple(jax.ShapeDtypeStruct(s, d) for s, d in out_shape),
         scratch_shapes=scratch,
@@ -212,32 +223,34 @@
 
 def per_device(q, k, v, g, lse, o, do, x):
     y = lax.axis_index("y")
-    place = [lax.axis_index("zp"), lax.axis_index("zl"), y, lax.axis_index("x")]
-    place = jnp.stack(place).astype(jnp.int32)
     pack = call(pack_body, [((NP, ZB, H), bf16), ((YB, H), bf16)], [], 8)
-    zsend, own = pack(place, q, k, v, g.reshape(1, T), lse.reshape(1, T), o, do, x)
+    zsend, own = pack(q, k, v, g.reshape(1, T), lse.reshape(1, T), o, do, x)
     recv = lax.all_to_all(zsend, "zp", 0, 0, tiled=True)
     grp = lax.all_gather(own, "y", axis=0, tiled=False)
     part = [lax.dynamic_slice_in_dim(grp, XB + half * T + y * 32, 32, 1) for half in range(2)]
     xt = lax.all_gather(jnp.concatenate(part, axis=1), "c", axis=0, tiled=False)
-    recv, xt = lax.optimization_barrier((recv, xt))
     xts = [xt]
-    relayed = lax.ppermute(recv, "zl", [(0, 1), (1, 0)])
     for d in range(1, NX):
         xts.append(lax.ppermute(xt, "x", [(i, (i + d) % NX) for i in range(NX)]))
+    recv, *xts[:3] = lax.optimization_barrier((recv, *xts[:3]))
+    swap = [(0, 1), (1, 0)]
+    relayed = lax.ppermute(recv[:CUT], "zl", swap)
+    rest = lax.ppermute(recv[CUT:], "zl", swap)
     block = (NY * T, H)
-    sums = call(first_body, [(block, f32)] * 3, [], 2)(place, recv, grp)
+    sums = call(first_body, [(block, f32)] * 3, [], 2)(recv, grp)
+    more = call(functools.partial(more_body, 0), [(block, f32)] * 3, [], 5)
+    sums = more(relayed, grp, *sums)
     second = call(
-        second_body,
+        last_body,
         [((NY, NY * T, H), bf16)] + [((2 * T, H), bf16)] * NY,
         [pltpu.VMEM(block, f32)] * 3,
         5,
     )
-    q_sums, *kv = second(place, relayed, grp, *sums)
+    q_sums, *kv = second(rest, grp, *sums)
     q_sums = lax.all_to_all(q_sums, "y", 0, 0, tiled=True)
     outs = [((T, H), bf16), ((NZ, 32, H), bf16)]
     finish = call(finish_body, outs, [pltpu.VMEM(block, bf16)], 1 + NX)
-    q_grad, zs = finish(place, q_sums, *xts)
+    q_grad, zs = finish(q_sums, *xts)
     zs, *kv = lax.optimization_barrier((zs, *kv))
     back = lax.all_to_all(zs, ("zp", "zl"), 0, 0, tiled=True)
     total = kv[0].astype(f32)

time: 126 us -> 121 us (0.960)
  waiting for transfers between devices: 36 us -> 23.5 us
  starting transfers between devices: 54 us -> 58.6 us
  Pallas kernels: 13.6 us -> 16.6 us
    all_to_all x1, waiting for transfers between devices: 11.5 us -> 0.47 us  [per_device(): recv = lax.all_to_all(zsend, 'zp', 0, 0, tiled=True)]
    ppermute x1 -> x2, waiting for transfers between devices: 6.52 us -> 2.08 us  [the longest x1 2.08 us: per_device(): relayed = lax.ppermute(recv[:CUT], 'zl', swap)]
    pallas_call x4 -> x5, Pallas kernels: 13.6 us -> 16.6 us  [the longest x1 4.69 us: per_device(): sums = call(first_body, [(block, f32)] * 3, [], 2)(recv, grp)]
    ppermute x3, waiting for transfers between devices: 6.12 us -> 9.08 us  [per_device(): xts.append(lax.ppermute(xt, 'x', [(i, (i + d) % NX) for i in range(NX)]))]
    all_to_all x1, starting transfers between devices: 9.68 us -> 12.1 us  [per_device(): back = lax.all_to_all(zs, ('zp', 'zl'), 0, 0, tiled=True)]
    ppermute x1 -> x2, starting transfers between devices: 3.84 us -> 5.84 us  [the longest x1 3.85 us: per_device(): relayed = lax.ppermute(recv[:CUT], 'zl', swap)]
    ppermute x3, starting transfers between devices: 8.76 us -> 10.2 us  [per_device(): xts.append(lax.ppermute(xt, 'x', [(i, (i + d) % NX) for i in range(NX)]))]
    unnamed x26 -> x28, local copies, waits for them, and re-layouts: 2.33 us -> 2.9 us
  transfers between devices with their start and end apart: 10 -> 11, of which waited for: 5 -> 6; matrix products, arithmetic and copies ran while one was open for 1% -> 1% of each run, Pallas kernels for 4% -> 7%
where the time goes in v7:
time: 121 us; the launch traced here: 120 us
  starting transfers between devices  58.6 us (48%)
  waiting for transfers between devices  23.5 us (19%)
  Pallas kernels  16.6 us (14%)
  blocking collectives  15.8 us (13%)
  local copies, waits for them, and re-layouts  3.56 us (3%)
  other arithmetic  1.29 us (1%)
    all_to_all x1, starting transfers between devices, per_device(): recv = lax.all_to_all(zsend, 'zp', 0, 0, tiled=True)  15.2 us
    all_gather x1, blocking collectives, per_device(): grp = lax.all_gather(own, 'y', axis=0, tiled=False)  13.9 us
    all_to_all x1, starting transfers between devices, per_device(): back = lax.all_to_all(zs, ('zp', 'zl'), 0, 0, tiled=True)  12.1 us
    all_to_all x1, waiting for transfers between devices, per_device(): back = lax.all_to_all(zs, ('zp', 'zl'), 0, 0, tiled=True)  11.8 us
    ppermute x3, starting transfers between devices, per_device(): turned = lax.ppermute(kv[d], 'y', [(i, (i + d) % NY) for i in range(NY)])  10.8 us
    ppermute x3, starting transfers between devices, per_device(): xts.append(lax.ppermute(xt, 'x', [(i, (i + d) % NX) for i in range(NX)]))  10.2 us
    ppermute x3, waiting for transfers between devices, per_device(): xts.append(lax.ppermute(xt, 'x', [(i, (i + d) % NX) for i in range(NX)]))  9.08 us
    pallas_call x1, Pallas kernels, per_device(): sums = call(first_body, [(block, f32)] * 3, [], 2)(recv, grp)  4.69 us
  transfers between devices with their start and end apart: 11, of which 6 were waited for; matrix products, arithmetic and copies ran while one was open for 1% of the time, Pallas kernels for 7%

profile of v7, /device:TPU:6, one launch (start us, length us, event | category | flops | bytes accessed | tf_op | source)
XLA Modules:
  0.0 120.1 jit_solution(17842641879777160017)
XLA Ops:
  0.6 2.1 %shard_map.111 = (bf16[8,264,128]{2,1,0:T(8,128)(2,1)}, bf16[784,128]{1,0:T(8,128)(2,1)}) custom-call(bf16[128,128]{1,0:T(8,128)(2,1)} %q.1, bf16[128,128]{1,0:T(8,128)(2,1)} %k.1, bf16[128,128]{1,0:T(8,128)(2,1)} %v.1, f32[1,128]{1,0:T(1,128)} %bitcast.12, f32[1,128]{1,0:T(1,128)} %bitcast.13, bf16[128,128]{1,0:T(8,128)(2,1)} %o.1, bf16[128,128]{1,0:T(8,128)(2,1)} %do.1, ...), custom_call_target="tpu_custom_call" | custom-call | tf_op jit(solution)/shard_map/pallas_call | solution.py:227
  2.7 15.2 %all-to-all-start = ((bf16[8,264,128]{2,1,0:T(8,128)(2,1)}), bf16[8,264,128]{2,1,0:T(8,128)(2,1)S(1)}, u32[]{:S(2)}, u32[]{:S(2)}) async-start(bf16[8,264,128]{2,1,0:T(8,128)(2,1)} %get-tuple-element.28), calls=%async_computation | async-start | bytes 1081344 | tf_op jit(solution)/shard_map/all_to_all | solution.py:228
  18.0 13.9 %all-gather = bf16[3136,128]{1,0:T(8,128)(2,1)S(1)} all-gather(bf16[784,128]{1,0:T(8,128)(2,1)S(1)} %copy-done.6), channel_id=2, replica_groups=mesh['zp'=8,'zl'=2,'y'=4,'x'=4,'c'=2] {'y'}, dimensions={0}, use_global_device_ids=true | all-gather | bytes 1003520 | tf_op jit(solution)/shard_map/all_gather | solution.py:229
  31.9 1.9 %all-gather.1 = bf16[8,64,128]{2,1,0:T(8,128)(2,1)S(1)} all-gather(bf16[4,64,128]{2,1,0:T(8,128)(2,1)S(1)} %pad_maximum_fusion), channel_id=3, replica_groups=mesh['zp'=8,'zl'=2,'y'=4,'x'=4,'c'=2] {'c'}, dimensions={0}, use_global_device_ids=true | all-gather | bytes 196608 | tf_op jit(solution)/shard_map/all_gather | solution.py:231
  33.8 2.4 %collective-permute-start = (bf16[2,4,64,128]{3,2,1,0:T(8,128)(2,1)S(1)}, bf16[2,4,64,128]{3,2,1,0:T(8,128)(2,1)S(1)}, u32[]{:S(2)}, u32[]{:S(2)}) collective-permute-start(bf16[2,4,64,128]{3,2,1,0:T(8,128)(2,1)S(1)} %bitcast.8), channel_id=1, source_target_pairs={{0,2},{2,4},{4,6},{6,0},{1,3},{3,5},{5,7},{7,1},{8,10},{10,12},{12... | collective-permute-start | bytes 393224 | tf_op jit(solution)/shard_map/ppermute | solution.py:234
  36.1 4.3 %collective-permute-start.1 = (bf16[2,4,64,128]{3,2,1,0:T(8,128)(2,1)S(1)}, bf16[2,4,64,128]{3,2,1,0:T(8,128)(2,1)S(1)}, u32[]{:S(2)}, u32[]{:S(2)}) collective-permute-start(bf16[2,4,64,128]{3,2,1,0:T(8,128)(2,1)S(1)} %bitcast.9), channel_id=1, source_target_pairs={{0,4},{2,6},{4,0},{6,2},{1,5},{3,7},{5,1},{7,3},{8,12},{10,14},{12... | collective-permute-start | bytes 393224 | tf_op jit(solution)/shard_map/ppermute | solution.py:234
  40.5 1.1 collective-permute-done.rest_1_
  41.6 3.2 %collective-permute-done.1.rest_2_ = bf16[2,4,64,128]{3,2,1,0:T(8,128)(2,1)S(1)} collective-permute-done((bf16[2,4,64,128]{3,2,1,0:T(8,128)(2,1)S(1)}, bf16[2,4,64,128]{3,2,1,0:T(8,128)(2,1)S(1)}, u32[]{:S(2)}, u32[]{:S(2)}) %collective-permute-start.1) | collective-permute-done | bytes 131104 | tf_op jit(solution)/shard_map/ppermute | solution.py:234
  44.8 0.5 all-to-all-done.recv
  45.3 3.9 %collective-permute-start.3 = (bf16[5,264,128]{2,1,0:T(8,128)(2,1)S(1)}, bf16[5,264,128]{2,1,0:T(8,128)(2,1)S(1)}, u32[]{:S(2)}, u32[]{:S(2)}) collective-permute-start(bf16[5,264,128]{2,1,0:T(8,128)(2,1)S(1)} %slice.14), channel_id=1, source_target_pairs={{0,32},{32,0},{1,33},{33,1},{2,34},{34,2},{3,35},{35,3},{4,36},{36... | collective-permute-start | bytes 1013768 | tf_op jit(solution)/shard_map/ppermute | solution.py:237
  49.2 2.0 %collective-permute-start.2 = (bf16[3,264,128]{2,1,0:T(8,128)(2,1)S(1)}, bf16[3,264,128]{2,1,0:T(8,128)(2,1)S(1)}, u32[]{:S(2)}, u32[]{:S(2)}) collective-permute-start(bf16[3,264,128]{2,1,0:T(8,128)(2,1)S(1)} %slice.13), channel_id=1, source_target_pairs={{0,32},{32,0},{1,33},{33,1},{2,34},{34,2},{3,35},{35,3},{4,36},{36... | collective-permute-start | bytes 608264 | tf_op jit(solution)/shard_map/ppermute | solution.py:238
  51.3 4.7 %shard_map.112 = (f32[512,128]{1,0:T(8,128)}, f32[512,128]{1,0:T(8,128)}, f32[512,128]{1,0:T(8,128)}) custom-call(bf16[8,264,128]{2,1,0:T(8,128)(2,1)} %copy-done.1, bf16[4,784,128]{2,1,0:T(8,128)(2,1)} %bitcast.5), custom_call_target="tpu_custom_call" | custom-call | tf_op jit(solution)/shard_map/pallas_call | solution.py:240
  55.9 2.1 %collective-permute-done.3.recv = bf16[5,264,128]{2,1,0:T(8,128)(2,1)S(1)} collective-permute-done((bf16[5,264,128]{2,1,0:T(8,128)(2,1)S(1)}, bf16[5,264,128]{2,1,0:T(8,128)(2,1)S(1)}, u32[]{:S(2)}, u32[]{:S(2)}) %collective-permute-start.3) | collective-permute-done | bytes 337952 | tf_op jit(solution)/shard_map/ppermute | solution.py:237
  58.0 0.7 copy-done.4
  58.8 4.0 %shard_map.113 = (f32[512,128]{1,0:T(8,128)}, f32[512,128]{1,0:T(8,128)}, f32[512,128]{1,0:T(8,128)}) custom-call(bf16[5,264,128]{2,1,0:T(8,128)(2,1)} %copy-done.4, bf16[4,784,128]{2,1,0:T(8,128)(2,1)} %bitcast.6, f32[512,128]{1,0:T(8,128)} %get-tuple-element.31.dq0, f32[512,128]{1,0:T(8,128)} %get-tuple-element.32.dk0, f32[512,128]{1,0:T(8,128)} %get-tuple-element.33.dv0), custom_call_target="tpu_custom_call" | custom-call | tf_op jit(solution)/shard_map/pallas_call | solution.py:242
  62.7 0.0 collective-permute-done.2.recv
  62.7 0.7 copy-done.5
  63.4 3.5 %shard_map.114 = (bf16[4,512,128]{2,1,0:T(8,128)(2,1)}, bf16[256,128]{1,0:T(8,128)(2,1)}, bf16[256,128]{1,0:T(8,128)(2,1)}, bf16[256,128]{1,0:T(8,128)(2,1)}, bf16[256,128]{1,0:T(8,128)(2,1)}) custom-call(bf16[3,264,128]{2,1,0:T(8,128)(2,1)} %copy-done.5, bf16[4,784,128]{2,1,0:T(8,128)(2,1)} %bitcast.7, f32[512,128]{1,0:T(8,128)} %get-tuple-element.34.dq0, ...), custom_call_target="tpu_custom_call" | custom-call | tf_op jit(solution)/shard_map/pallas_call | solution.py:249
  66.9 4.5 %all-to-all-start.1 = ((bf16[4,512,128]{2,1,0:T(8,128)(2,1)}), bf16[4,512,128]{2,1,0:T(8,128)(2,1)S(1)}, u32[]{:S(2)}, u32[]{:S(2)}) async-start(bf16[4,512,128]{2,1,0:T(8,128)(2,1)} %get-tuple-element.37), calls=%async_computation.1 | async-start | bytes 1048576 | tf_op jit(solution)/shard_map/all_to_all | solution.py:250
  71.4 3.5 %collective-permute-start.4 = (bf16[2,4,64,128]{3,2,1,0:T(8,128)(2,1)S(1)}, bf16[2,4,64,128]{3,2,1,0:T(8,128)(2,1)S(1)}, u32[]{:S(2)}, u32[]{:S(2)}) collective-permute-start(bf16[2,4,64,128]{3,2,1,0:T(8,128)(2,1)S(1)} %bitcast.10), channel_id=1, source_target_pairs={{0,6},{2,0},{4,2},{6,4},{1,7},{3,1},{5,3},{7,5},{8,14},{10,8},{12,... | collective-permute-start | bytes 393224 | tf_op jit(solution)/shard_map/ppermute | solution.py:234
  74.9 4.7 %collective-permute-done.4.rest_3_ = bf16[2,4,64,128]{3,2,1,0:T(8,128)(2,1)S(1)} collective-permute-done((bf16[2,4,64,128]{3,2,1,0:T(8,128)(2,1)S(1)}, bf16[2,4,64,128]{3,2,1,0:T(8,128)(2,1)S(1)}, u32[]{:S(2)}, u32[]{:S(2)}) %collective-permute-start.4) | collective-permute-done | bytes 131104 | tf_op jit(solution)/shard_map/ppermute | solution.py:234
  79.6 0.6 copy-done.9
  80.3 0.8 copy-done.2
  81.1 2.3 %shard_map.115 = (bf16[128,128]{1,0:T(8,128)(2,1)}, bf16[16,32,128]{2,1,0:T(8,128)(2,1)}) custom-call(bf16[4,512,128]{2,1,0:T(8,128)(2,1)} %copy-done.2, bf16[2,4,64,128]{3,2,1,0:T(8,128)(2,1)} %bitcast.11, bf16[2,4,64,128]{3,2,1,0:T(8,128)(2,1)} %copy-done.7, bf16[2,4,64,128]{3,2,1,0:T(8,128)(2,1)} %copy-done.8, bf16[2,4,64,128]{3,2,1,0:T(8,128)(2,1)} %copy-done.9), custom_call_target="tpu_custom_call" | custom-call | tf_op jit(solution)/shard_map/pallas_call | solution.py:253
  83.4 5.3 %collective-permute-start.7 = (bf16[256,128]{1,0:T(8,128)(2,1)S(1)}, bf16[256,128]{1,0:T(8,128)(2,1)S(1)}, u32[]{:S(2)}, u32[]{:S(2)}) collective-permute-start(bf16[256,128]{1,0:T(8,128)(2,1)S(1)} %copy-done.13), channel_id=1, source_target_pairs={{0,24},{8,0},{16,8},{24,16},{1,25},{9,1},{17,9},{25,17},{2,26},{10... | collective-permute-start | bytes 196616 | tf_op jit(solution)/shard_map/ppermute | solution.py:258
  88.6 2.8 %collective-permute-start.6 = (bf16[256,128]{1,0:T(8,128)(2,1)S(1)}, bf16[256,128]{1,0:T(8,128)(2,1)S(1)}, u32[]{:S(2)}, u32[]{:S(2)}) collective-permute-start(bf16[256,128]{1,0:T(8,128)(2,1)S(1)} %copy-done.12), channel_id=1, source_target_pairs={{0,16},{8,24},{16,0},{24,8},{1,17},{9,25},{17,1},{25,9},{2,18},{10... | collective-permute-start | bytes 196616 | tf_op jit(solution)/shard_map/ppermute | solution.py:258
  91.4 2.8 %collective-permute-start.5 = (bf16[256,128]{1,0:T(8,128)(2,1)S(1)}, bf16[256,128]{1,0:T(8,128)(2,1)S(1)}, u32[]{:S(2)}, u32[]{:S(2)}) collective-permute-start(bf16[256,128]{1,0:T(8,128)(2,1)S(1)} %copy-done.11), channel_id=1, source_target_pairs={{0,8},{8,16},{16,24},{24,0},{1,9},{9,17},{17,25},{25,1},{2,10},{10... | collective-permute-start | bytes 196616 | tf_op jit(solution)/shard_map/ppermute | solution.py:258
  94.2 12.1 %all-to-all-start.2 = ((bf16[16,32,128]{2,1,0:T(8,128)(2,1)}), bf16[16,32,128]{2,1,0:T(8,128)(2,1)S(1)}, u32[]{:S(2)}, u32[]{:S(2)}) async-start(bf16[16,32,128]{2,1,0:T(8,128)(2,1)} %get-tuple-element.51), calls=%async_computation.2 | async-start | bytes 262144 | tf_op jit(solution)/shard_map/all_to_all | solution.py:255
  106.4 0.6 slice.23
  107.0 0.6 fusion
  107.6 11.8 %all-to-all-done.2 = bf16[16,32,128]{2,1,0:T(8,128)(2,1)S(1)} async-done(((bf16[16,32,128]{2,1,0:T(8,128)(2,1)}), bf16[16,32,128]{2,1,0:T(8,128)(2,1)S(1)}, u32[]{:S(2)}, u32[]{:S(2)}) %all-to-all-start.2) | async-done | bytes 131104 | tf_op jit(solution)/shard_map/all_to_all | solution.py:255
  119.5 0.6 convert_reduce_fusion
  (33 shorter events, 0.1 us)
Async XLA Ops:
  2.7 15.2 %copy-start.6 = (bf16[784,128]{1,0:T(8,128)(2,1)S(1)}, bf16[784,128]{1,0:T(8,128)(2,1)}, u32[]{:S(2)}) copy-start(bf16[784,128]{1,0:T(8,128)(2,1)} %get-tuple-element.29) | copy-start | bytes 602116
  2.7 42.6 %all-to-all-start = ((bf16[8,264,128]{2,1,0:T(8,128)(2,1)}), bf16[8,264,128]{2,1,0:T(8,128)(2,1)S(1)}, u32[]{:S(2)}, u32[]{:S(2)}) async-start(bf16[8,264,128]{2,1,0:T(8,128)(2,1)} %get-tuple-element.28), calls=%async_computation | async-start | bytes 1081344 | tf_op jit(solution)/shard_map/all_to_all | solution.py:228
  31.8 19.4 %copy-start = (bf16[3136,128]{1,0:T(8,128)(2,1)}, bf16[3136,128]{1,0:T(8,128)(2,1)S(1)}, u32[]{:S(2)}) copy-start(bf16[3136,128]{1,0:T(8,128)(2,1)S(1)} %all-gather) | copy-start | bytes 2408452
  33.8 37.6 %copy-start.3 = (bf16[8,64,128]{2,1,0:T(8,128)(2,1)}, bf16[8,64,128]{2,1,0:T(8,128)(2,1)S(1)}, u32[]{:S(2)}) copy-start(bf16[8,64,128]{2,1,0:T(8,128)(2,1)S(1)} %all-gather.1) | copy-start | bytes 393220
  33.8 7.8 %collective-permute-start = (bf16[2,4,64,128]{3,2,1,0:T(8,128)(2,1)S(1)}, bf16[2,4,64,128]{3,2,1,0:T(8,128)(2,1)S(1)}, u32[]{:S(2)}, u32[]{:S(2)}) collective-permute-start(bf16[2,4,64,128]{3,2,1,0:T(8,128)(2,1)S(1)} %bitcast.8), channel_id=1, source_target_pairs={{0,2},{2,4},{4,6},{6,0},{1,3},{3,5},{5,7},{7,1},{8,10},{10,12},{12... | collective-permute-start | bytes 393224 | tf_op jit(solution)/shard_map/ppermute | solution.py:234
  36.1 8.7 %collective-permute-start.1 = (bf16[2,4,64,128]{3,2,1,0:T(8,128)(2,1)S(1)}, bf16[2,4,64,128]{3,2,1,0:T(8,128)(2,1)S(1)}, u32[]{:S(2)}, u32[]{:S(2)}) collective-permute-start(bf16[2,4,64,128]{3,2,1,0:T(8,128)(2,1)S(1)} %bitcast.9), channel_id=1, source_target_pairs={{0,4},{2,6},{4,0},{6,2},{1,5},{3,7},{5,1},{7,3},{8,12},{10,14},{12... | collective-permute-start | bytes 393224 | tf_op jit(solution)/shard_map/ppermute | solution.py:234
  41.6 7.6 %copy-start.7 = (bf16[2,4,64,128]{3,2,1,0:T(8,128)(2,1)}, bf16[2,4,64,128]{3,2,1,0:T(8,128)(2,1)S(1)}, u32[]{:S(2)}) copy-start(bf16[2,4,64,128]{3,2,1,0:T(8,128)(2,1)S(1)} %collective-permute-done.rest_1_) | copy-start | bytes 393220
  44.8 4.4 %copy-start.8 = (bf16[2,4,64,128]{3,2,1,0:T(8,128)(2,1)}, bf16[2,4,64,128]{3,2,1,0:T(8,128)(2,1)S(1)}, u32[]{:S(2)}) copy-start(bf16[2,4,64,128]{3,2,1,0:T(8,128)(2,1)S(1)} %collective-permute-done.1.rest_2_) | copy-start | bytes 393220
  45.3 3.9 %copy-start.1 = (bf16[8,264,128]{2,1,0:T(8,128)(2,1)}, bf16[8,264,128]{2,1,0:T(8,128)(2,1)S(1)}, u32[]{:S(2)}) copy-start(bf16[8,264,128]{2,1,0:T(8,128)(2,1)S(1)} %all-to-all-done.recv) | copy-start | bytes 1622020
  45.3 12.7 %collective-permute-start.3 = (bf16[5,264,128]{2,1,0:T(8,128)(2,1)S(1)}, bf16[5,264,128]{2,1,0:T(8,128)(2,1)S(1)}, u32[]{:S(2)}, u32[]{:S(2)}) collective-permute-start(bf16[5,264,128]{2,1,0:T(8,128)(2,1)S(1)} %slice.14), channel_id=1, source_target_pairs={{0,32},{32,0},{1,33},{33,1},{2,34},{34,2},{3,35},{35,3},{4,36},{36... | collective-permute-start | bytes 1013768 | tf_op jit(solution)/shard_map/ppermute | solution.py:237
  49.2 13.5 %collective-permute-start.2 = (bf16[3,264,128]{2,1,0:T(8,128)(2,1)S(1)}, bf16[3,264,128]{2,1,0:T(8,128)(2,1)S(1)}, u32[]{:S(2)}, u32[]{:S(2)}) collective-permute-start(bf16[3,264,128]{2,1,0:T(8,128)(2,1)S(1)} %slice.13), channel_id=1, source_target_pairs={{0,32},{32,0},{1,33},{33,1},{2,34},{34,2},{3,35},{35,3},{4,36},{36... | collective-permute-start | bytes 608264 | tf_op jit(solution)/shard_map/ppermute | solution.py:238
  58.0 0.7 copy-start.4
  62.7 0.7 copy-start.5
  66.9 12.7 %all-to-all-start.1 = ((bf16[4,512,128]{2,1,0:T(8,128)(2,1)}), bf16[4,512,128]{2,1,0:T(8,128)(2,1)S(1)}, u32[]{:S(2)}, u32[]{:S(2)}) async-start(bf16[4,512,128]{2,1,0:T(8,128)(2,1)} %get-tuple-element.37), calls=%async_computation.1 | async-start | bytes 1048576 | tf_op jit(solution)/shard_map/all_to_all | solution.py:250
  71.4 12.0 %copy-start.13 = (bf16[256,128]{1,0:T(8,128)(2,1)S(1)}, bf16[256,128]{1,0:T(8,128)(2,1)}, u32[]{:S(2)}) copy-start(bf16[256,128]{1,0:T(8,128)(2,1)} %get-tuple-element.50) | copy-start | bytes 196612
  71.4 17.2 %copy-start.12 = (bf16[256,128]{1,0:T(8,128)(2,1)S(1)}, bf16[256,128]{1,0:T(8,128)(2,1)}, u32[]{:S(2)}) copy-start(bf16[256,128]{1,0:T(8,128)(2,1)} %get-tuple-element.49) | copy-start | bytes 196612
  71.4 20.0 %copy-start.11 = (bf16[256,128]{1,0:T(8,128)(2,1)S(1)}, bf16[256,128]{1,0:T(8,128)(2,1)}, u32[]{:S(2)}) copy-start(bf16[256,128]{1,0:T(8,128)(2,1)} %get-tuple-element.48) | copy-start | bytes 196612
  71.4 8.2 %collective-permute-start.4 = (bf16[2,4,64,128]{3,2,1,0:T(8,128)(2,1)S(1)}, bf16[2,4,64,128]{3,2,1,0:T(8,128)(2,1)S(1)}, u32[]{:S(2)}, u32[]{:S(2)}) collective-permute-start(bf16[2,4,64,128]{3,2,1,0:T(8,128)(2,1)S(1)} %bitcast.10), channel_id=1, source_target_pairs={{0,6},{2,0},{4,2},{6,4},{1,7},{3,1},{5,3},{7,5},{8,14},{10,8},{12,... | collective-permute-start | bytes 393224 | tf_op jit(solution)/shard_map/ppermute | solution.py:234
  79.6 0.6 copy-start.9
  80.3 0.8 copy-start.2
  83.4 23.0 %copy-start.10 = (bf16[256,128]{1,0:T(8,128)(2,1)S(1)}, bf16[256,128]{1,0:T(8,128)(2,1)}, u32[]{:S(2)}) copy-start(bf16[256,128]{1,0:T(8,128)(2,1)} %get-tuple-element.47) | copy-start | bytes 196612
  83.4 23.0 %collective-permute-start.7 = (bf16[256,128]{1,0:T(8,128)(2,1)S(1)}, bf16[256,128]{1,0:T(8,128)(2,1)S(1)}, u32[]{:S(2)}, u32[]{:S(2)}) collective-permute-start(bf16[256,128]{1,0:T(8,128)(2,1)S(1)} %copy-done.13), channel_id=1, source_target_pairs={{0,24},{8,0},{16,8},{24,16},{1,25},{9,1},{17,9},{25,17},{2,26},{10... | collective-permute-start | bytes 196616 | tf_op jit(solution)/shard_map/ppermute | solution.py:258
  88.6 17.7 %collective-permute-start.6 = (bf16[256,128]{1,0:T(8,128)(2,1)S(1)}, bf16[256,128]{1,0:T(8,128)(2,1)S(1)}, u32[]{:S(2)}, u32[]{:S(2)}) collective-permute-start(bf16[256,128]{1,0:T(8,128)(2,1)S(1)} %copy-done.12), channel_id=1, source_target_pairs={{0,16},{8,24},{16,0},{24,8},{1,17},{9,25},{17,1},{25,9},{2,18},{10... | collective-permute-start | bytes 196616 | tf_op jit(solution)/shard_map/ppermute | solution.py:258
  91.4 14.9 %collective-permute-start.5 = (bf16[256,128]{1,0:T(8,128)(2,1)S(1)}, bf16[256,128]{1,0:T(8,128)(2,1)S(1)}, u32[]{:S(2)}, u32[]{:S(2)}) collective-permute-start(bf16[256,128]{1,0:T(8,128)(2,1)S(1)} %copy-done.11), channel_id=1, source_target_pairs={{0,8},{8,16},{16,24},{24,0},{1,9},{9,17},{17,25},{25,1},{2,10},{10... | collective-permute-start | bytes 196616 | tf_op jit(solution)/shard_map/ppermute | solution.py:258
  94.2 25.3 %all-to-all-start.2 = ((bf16[16,32,128]{2,1,0:T(8,128)(2,1)}), bf16[16,32,128]{2,1,0:T(8,128)(2,1)S(1)}, u32[]{:S(2)}, u32[]{:S(2)}) async-start(bf16[16,32,128]{2,1,0:T(8,128)(2,1)} %get-tuple-element.51), calls=%async_computation.2 | async-start | bytes 262144 | tf_op jit(solution)/shard_map/all_to_all | solution.py:255

commit v8 on v7

--- a/solution.py
+++ b/solution.py
@@ -1,5 +1,3 @@
-import functools
-
 import jax
 import jax.numpy as jnp
 from jax import lax
@@ -11,7 +9,7 @@
 SP = ("zp", "zl", "y")
 TP = ("x", "c")
 NZ, NP, NY, NX, NC = 16, 8, 4, 4, 2
-CUT = 5
+GROUPS = [[2 * j + (g ^ (j // 4)) for j in range(NP)] for g in range(2)]
 T = 128
 H = 128
 SCALE = H**-0.5
@@ -119,7 +117,7 @@
     return query_part, key_part
 
 
-def received(recv, query_part, key_part, below_end, above_start, end, dq, dk, dv):
+def received(recv, query_part, key_part, below_end, above_start, dq, dk, dv):
     def block(j, count, at):
         return recv[pl.ds(j, count), at * T : (at + 1) * T].reshape(count * T, H)
 
@@ -149,7 +147,7 @@
             step(end - 1, 1)
 
     over(below, 0, below_end)
-    over(above, above_start, end)
+    over(above, above_start, NP)
 
 
 def first_body(recv, grp, dq, dk, dv):
@@ -162,24 +160,18 @@
     dk[...], dv[...] = key_part(
         grp[y, 0:T], grp[y, T : 2 * T], joined(st[0:3]), joined(st[3:6]), big <= small
     )
-    received(recv, query_part, key_part, zp, zp + 1, NP, dq, dk, dv)
-
-
-def more_body(low, recv, grp, dq0, dk0, dv0, dq, dk, dv):
-    size = recv.shape[0]
-    zp, zl, _, _ = position()
-    border = jnp.clip(zp + zl - low, 0, size)
+    received(recv, query_part, key_part, zp, zp + 1, dq, dk, dv)
+
+
+def last_body(recv, grp, dq0, dk0, dv0, q_sums, *rest):
+    kv_sums, (dq, dk, dv) = rest[:NY], rest[NY:]
+    zp, zl, y, _ = position()
+    border = zp + zl
     query_part, key_part = parts_of(grp)
     dq[...] = dq0[...]
     dk[...] = dk0[...]
     dv[...] = dv0[...]
-    received(recv, query_part, key_part, border, border, size, dq, dk, dv)
-
-
-def last_body(recv, grp, dq0, dk0, dv0, q_sums, *rest):
-    kv_sums, (dq, dk, dv) = rest[:NY], rest[NY:]
-    y = position()[2]
-    more_body(CUT, recv, grp, dq0, dk0, dv0, dq, dk, dv)
+    received(recv, query_part, key_part, border, border, dq, dk, dv)
     sums = dq[...].astype(bf16)
     for d in range(NY):
         at = pl.ds(pl.multiple_of(((y + d) % NY) * T, T), T)
@@ -225,28 +217,24 @@
     y = lax.axis_index("y")
     pack = call(pack_body, [((NP, ZB, H), bf16), ((YB, H), bf16)], [], 8)
     zsend, own = pack(q, k, v, g.reshape(1, T), lse.reshape(1, T), o, do, x)
-    recv = lax.all_to_all(zsend, "zp", 0, 0, tiled=True)
+    recv = lax.all_to_all(zsend, ("zp", "zl"), 0, 0, axis_index_groups=GROUPS, tiled=True)
     grp = lax.all_gather(own, "y", axis=0, tiled=False)
     part = [lax.dynamic_slice_in_dim(grp, XB + half * T + y * 32, 32, 1) for half in range(2)]
     xt = lax.all_gather(jnp.concatenate(part, axis=1), "c", axis=0, tiled=False)
     xts = [xt]
     for d in range(1, NX):
         xts.append(lax.ppermute(xt, "x", [(i, (i + d) % NX) for i in range(NX)]))
-    recv, *xts[:3] = lax.optimization_barrier((recv, *xts[:3]))
-    swap = [(0, 1), (1, 0)]
-    relayed = lax.ppermute(recv[:CUT], "zl", swap)
-    rest = lax.ppermute(recv[CUT:], "zl", swap)
+    recv, *xts[:2] = lax.optimization_barrier((recv, *xts[:2]))
+    relayed = lax.ppermute(recv, "zl", [(0, 1), (1, 0)])
     block = (NY * T, H)
     sums = call(first_body, [(block, f32)] * 3, [], 2)(recv, grp)
-    more = call(functools.partial(more_body, 0), [(block, f32)] * 3, [], 5)
-    sums = more(relayed, grp, *sums)
     second = call(
         last_body,
         [((NY, NY * T, H), bf16)] + [((2 * T, H), bf16)] * NY,
         [pltpu.VMEM(block, f32)] * 3,
         5,
     )
-    q_sums, *kv = second(rest, grp, *sums)
+    q_sums, *kv = second(relayed, grp, *sums)
     q_sums = lax.all_to_all(q_sums, "y", 0, 0, tiled=True)
     outs = [((T, H), bf16), ((NZ, 32, H), bf16)]
     finish = call(finish_body, outs, [pltpu.VMEM(block, bf16)], 1 + NX)

time: 121 us -> 121 us (level)
  waiting for transfers between devices: 23.5 us -> 38 us
  starting transfers between devices: 58.6 us -> 47.9 us
  Pallas kernels: 16.6 us -> 13.7 us
    all_to_all x1, waiting for transfers between devices: 0.47 us -> 8.6 us  [per_device(): lax.all_to_all(zsend, ('zp', 'zl'), 0, 0, axis_index_groups=GROUPS, tiled...]
    all_to_all x1, starting transfers between devices: 12.1 us -> 6.64 us  [per_device(): back = lax.all_to_all(zs, ('zp', 'zl'), 0, 0, tiled=True)]
    ppermute x2 -> x1, waiting for transfers between devices: 2.08 us -> 6.34 us  [per_device(): relayed = lax.ppermute(recv, 'zl', [(0, 1), (1, 0)])]
    ppermute x2 -> x1, starting transfers between devices: 5.84 us -> 2.29 us  [per_device(): relayed = lax.ppermute(recv, 'zl', [(0, 1), (1, 0)])]
    pallas_call x2 -> x1, Pallas kernels: 7.5 us -> 4.6 us  [per_device(): q_sums, *kv = second(relayed, grp, *sums)]
    ppermute x3, starting transfers between devices: 10.2 us -> 7.75 us  [per_device(): xts.append(lax.ppermute(xt, 'x', [(i, (i + d) % NX) for i in range(NX)]))]
    ppermute x3, waiting for transfers between devices: 9.08 us -> 11.2 us  [per_device(): xts.append(lax.ppermute(xt, 'x', [(i, (i + d) % NX) for i in range(NX)]))]
    unnamed x28 -> x26, local copies, waits for them, and re-layouts: 2.9 us -> 2.33 us
  transfers between devices with their start and end apart: 11 -> 10, of which waited for: 6 -> 6; matrix products, arithmetic and copies ran while one was open for 1% -> 1% of each run, Pallas kernels for 7% -> 4%
where the time goes in v8:
time: 121 us; the launch traced here: 120 us
  starting transfers between devices  47.9 us (40%)
  waiting for transfers between devices  38 us (31%)
  blocking collectives  15.8 us (13%)
  Pallas kernels  13.7 us (11%)
  local copies, waits for them, and re-layouts  2.96 us (2%)
  other arithmetic  1.29 us (1%)
    all_to_all x1, starting transfers between devices, per_device(): lax.all_to_all(zsend, ('zp', 'zl'), 0, 0, axis_index_groups=GROUPS, tiled...  14.8 us
    all_gather x1, blocking collectives, per_device(): grp = lax.all_gather(own, 'y', axis=0, tiled=False)  13.9 us
    ppermute x3, starting transfers between devices, per_device(): turned = lax.ppermute(kv[d], 'y', [(i, (i + d) % NY) for i in range(NY)])  12 us
    all_to_all x1, waiting for transfers between devices, per_device(): back = lax.all_to_all(zs, ('zp', 'zl'), 0, 0, tiled=True)  11.9 us
    ppermute x3, waiting for transfers between devices, per_device(): xts.append(lax.ppermute(xt, 'x', [(i, (i + d) % NX) for i in range(NX)]))  11.2 us
    all_to_all x1, waiting for transfers between devices, per_device(): lax.all_to_all(zsend, ('zp', 'zl'), 0, 0, axis_index_groups=GROUPS, tiled...  8.6 us
    ppermute x3, starting transfers between devices, per_device(): xts.append(lax.ppermute(xt, 'x', [(i, (i + d) % NX) for i in range(NX)]))  7.75 us
    all_to_all x1, starting transfers between devices, per_device(): back = lax.all_to_all(zs, ('zp', 'zl'), 0, 0, tiled=True)  6.64 us
  transfers between devices with their start and end apart: 10, of which 6 were waited for; matrix products, arithmetic and copies ran while one was open for 1% of the time, Pallas kernels for 4%

profile of v8, /device:TPU:6, one launch (start us, length us, event | category | flops | bytes accessed | tf_op | source)
XLA Modules:
  0.0 120.4 jit_solution(7024849480129713794)
XLA Ops:
  0.6 2.1 %shard_map.111 = (bf16[8,264,128]{2,1,0:T(8,128)(2,1)}, bf16[784,128]{1,0:T(8,128)(2,1)}) custom-call(bf16[128,128]{1,0:T(8,128)(2,1)} %q.1, bf16[128,128]{1,0:T(8,128)(2,1)} %k.1, bf16[128,128]{1,0:T(8,128)(2,1)} %v.1, f32[1,128]{1,0:T(1,128)} %bitcast.11, f32[1,128]{1,0:T(1,128)} %bitcast.12, bf16[128,128]{1,0:T(8,128)(2,1)} %o.1, bf16[128,128]{1,0:T(8,128)(2,1)} %do.1, ...), custom_call_target="tpu_custom_call" | custom-call | tf_op jit(solution)/shard_map/pallas_call | solution.py:219
  2.8 14.8 %all-to-all-start = ((bf16[8,264,128]{2,1,0:T(8,128)(2,1)}), bf16[8,264,128]{2,1,0:T(8,128)(2,1)S(1)}, u32[]{:S(2)}, u32[]{:S(2)}) async-start(bf16[8,264,128]{2,1,0:T(8,128)(2,1)} %get-tuple-element.24), calls=%async_computation | async-start | bytes 1081344 | tf_op jit(solution)/shard_map/all_to_all | solution.py:220
  17.6 13.9 %all-gather = bf16[3136,128]{1,0:T(8,128)(2,1)S(1)} all-gather(bf16[784,128]{1,0:T(8,128)(2,1)S(1)} %copy-done.5), channel_id=2, replica_groups=mesh['zp'=8,'zl'=2,'y'=4,'x'=4,'c'=2] {'y'}, dimensions={0}, use_global_device_ids=true | all-gather | bytes 1003520 | tf_op jit(solution)/shard_map/all_gather | solution.py:221
  31.4 1.9 %all-gather.1 = bf16[8,64,128]{2,1,0:T(8,128)(2,1)S(1)} all-gather(bf16[4,64,128]{2,1,0:T(8,128)(2,1)S(1)} %pad_maximum_fusion), channel_id=3, replica_groups=mesh['zp'=8,'zl'=2,'y'=4,'x'=4,'c'=2] {'c'}, dimensions={0}, use_global_device_ids=true | all-gather | bytes 196608 | tf_op jit(solution)/shard_map/all_gather | solution.py:223
  33.3 2.4 %collective-permute-start = (bf16[2,4,64,128]{3,2,1,0:T(8,128)(2,1)S(1)}, bf16[2,4,64,128]{3,2,1,0:T(8,128)(2,1)S(1)}, u32[]{:S(2)}, u32[]{:S(2)}) collective-permute-start(bf16[2,4,64,128]{3,2,1,0:T(8,128)(2,1)S(1)} %bitcast.7), channel_id=1, source_target_pairs={{0,2},{2,4},{4,6},{6,0},{1,3},{3,5},{5,7},{7,1},{8,10},{10,12},{12... | collective-permute-start | bytes 393224 | tf_op jit(solution)/shard_map/ppermute | solution.py:226
  35.7 5.1 %collective-permute-done.rest_1_ = bf16[2,4,64,128]{3,2,1,0:T(8,128)(2,1)S(1)} collective-permute-done((bf16[2,4,64,128]{3,2,1,0:T(8,128)(2,1)S(1)}, bf16[2,4,64,128]{3,2,1,0:T(8,128)(2,1)S(1)}, u32[]{:S(2)}, u32[]{:S(2)}) %collective-permute-start) | collective-permute-done | bytes 131104 | tf_op jit(solution)/shard_map/ppermute | solution.py:226
  40.8 8.6 %all-to-all-done.recv = bf16[8,264,128]{2,1,0:T(8,128)(2,1)S(1)} async-done(((bf16[8,264,128]{2,1,0:T(8,128)(2,1)}), bf16[8,264,128]{2,1,0:T(8,128)(2,1)S(1)}, u32[]{:S(2)}, u32[]{:S(2)}) %all-to-all-start) | async-done | bytes 540704 | tf_op jit(solution)/shard_map/all_to_all | solution.py:220
  49.4 2.3 %collective-permute-start.1 = (bf16[8,264,128]{2,1,0:T(8,128)(2,1)S(1)}, bf16[8,264,128]{2,1,0:T(8,128)(2,1)S(1)}, u32[]{:S(2)}, u32[]{:S(2)}) collective-permute-start(bf16[8,264,128]{2,1,0:T(8,128)(2,1)S(1)} %all-to-all-done.recv), channel_id=1, source_target_pairs={{0,32},{32,0},{1,33},{33,1},{2,34},{34,2},{3,35},{35,3},{4,36},{36... | collective-permute-start | bytes 1622024 | tf_op jit(solution)/shard_map/ppermute | solution.py:228
  51.7 4.7 %shard_map.112 = (f32[512,128]{1,0:T(8,128)}, f32[512,128]{1,0:T(8,128)}, f32[512,128]{1,0:T(8,128)}) custom-call(bf16[8,264,128]{2,1,0:T(8,128)(2,1)} %copy-done.1, bf16[4,784,128]{2,1,0:T(8,128)(2,1)} %bitcast.5), custom_call_target="tpu_custom_call" | custom-call | tf_op jit(solution)/shard_map/pallas_call | solution.py:230
  56.4 6.3 %collective-permute-done.1.recv = bf16[8,264,128]{2,1,0:T(8,128)(2,1)S(1)} collective-permute-done((bf16[8,264,128]{2,1,0:T(8,128)(2,1)S(1)}, bf16[8,264,128]{2,1,0:T(8,128)(2,1)S(1)}, u32[]{:S(2)}, u32[]{:S(2)}) %collective-permute-start.1) | collective-permute-done | bytes 540704 | tf_op jit(solution)/shard_map/ppermute | solution.py:228
  62.8 0.8 copy-done.3
  63.6 4.6 %shard_map.113 = (bf16[4,512,128]{2,1,0:T(8,128)(2,1)}, bf16[256,128]{1,0:T(8,128)(2,1)}, bf16[256,128]{1,0:T(8,128)(2,1)}, bf16[256,128]{1,0:T(8,128)(2,1)}, bf16[256,128]{1,0:T(8,128)(2,1)}) custom-call(bf16[8,264,128]{2,1,0:T(8,128)(2,1)} %copy-done.3, bf16[4,784,128]{2,1,0:T(8,128)(2,1)} %bitcast.6, f32[512,128]{1,0:T(8,128)} %get-tuple-element.27.dq0, ...), custom_call_target="tpu_custom_call" | custom-call | tf_op jit(solution)/shard_map/pallas_call | solution.py:237
  68.2 4.5 %all-to-all-start.1 = ((bf16[4,512,128]{2,1,0:T(8,128)(2,1)}), bf16[4,512,128]{2,1,0:T(8,128)(2,1)S(1)}, u32[]{:S(2)}, u32[]{:S(2)}) async-start(bf16[4,512,128]{2,1,0:T(8,128)(2,1)} %get-tuple-element.30), calls=%async_computation.1 | async-start | bytes 1048576 | tf_op jit(solution)/shard_map/all_to_all | solution.py:238
  72.7 3.5 %collective-permute-start.2 = (bf16[2,4,64,128]{3,2,1,0:T(8,128)(2,1)S(1)}, bf16[2,4,64,128]{3,2,1,0:T(8,128)(2,1)S(1)}, u32[]{:S(2)}, u32[]{:S(2)}) collective-permute-start(bf16[2,4,64,128]{3,2,1,0:T(8,128)(2,1)S(1)} %bitcast.8), channel_id=1, source_target_pairs={{0,4},{2,6},{4,0},{6,2},{1,5},{3,7},{5,1},{7,3},{8,12},{10,14},{12... | collective-permute-start | bytes 393224 | tf_op jit(solution)/shard_map/ppermute | solution.py:226
  76.1 1.9 %collective-permute-start.3 = (bf16[2,4,64,128]{3,2,1,0:T(8,128)(2,1)S(1)}, bf16[2,4,64,128]{3,2,1,0:T(8,128)(2,1)S(1)}, u32[]{:S(2)}, u32[]{:S(2)}) collective-permute-start(bf16[2,4,64,128]{3,2,1,0:T(8,128)(2,1)S(1)} %bitcast.9), channel_id=1, source_target_pairs={{0,6},{2,0},{4,2},{6,4},{1,7},{3,1},{5,3},{7,5},{8,14},{10,8},{12,... | collective-permute-start | bytes 393224 | tf_op jit(solution)/shard_map/ppermute | solution.py:226
  78.1 3.1 %collective-permute-done.2.rest_2_ = bf16[2,4,64,128]{3,2,1,0:T(8,128)(2,1)S(1)} collective-permute-done((bf16[2,4,64,128]{3,2,1,0:T(8,128)(2,1)S(1)}, bf16[2,4,64,128]{3,2,1,0:T(8,128)(2,1)S(1)}, u32[]{:S(2)}, u32[]{:S(2)}) %collective-permute-start.2) | collective-permute-done | bytes 131104 | tf_op jit(solution)/shard_map/ppermute | solution.py:226
  81.2 3.0 %collective-permute-done.3.rest_3_ = bf16[2,4,64,128]{3,2,1,0:T(8,128)(2,1)S(1)} collective-permute-done((bf16[2,4,64,128]{3,2,1,0:T(8,128)(2,1)S(1)}, bf16[2,4,64,128]{3,2,1,0:T(8,128)(2,1)S(1)}, u32[]{:S(2)}, u32[]{:S(2)}) %collective-permute-start.3) | collective-permute-done | bytes 131104 | tf_op jit(solution)/shard_map/ppermute | solution.py:226
  84.2 0.0 all-to-all-done.1.sums
  84.2 0.6 copy-done.8
  84.9 0.8 copy-done.2
  85.7 2.3 %shard_map.114 = (bf16[128,128]{1,0:T(8,128)(2,1)}, bf16[16,32,128]{2,1,0:T(8,128)(2,1)}) custom-call(bf16[4,512,128]{2,1,0:T(8,128)(2,1)} %copy-done.2, bf16[2,4,64,128]{3,2,1,0:T(8,128)(2,1)} %bitcast.10, bf16[2,4,64,128]{3,2,1,0:T(8,128)(2,1)} %copy-done.6, bf16[2,4,64,128]{3,2,1,0:T(8,128)(2,1)} %copy-done.7, bf16[2,4,64,128]{3,2,1,0:T(8,128)(2,1)} %copy-done.8), custom_call_target="tpu_custom_call" | custom-call | tf_op jit(solution)/shard_map/pallas_call | solution.py:241
  87.9 4.0 %collective-permute-start.4 = (bf16[256,128]{1,0:T(8,128)(2,1)S(1)}, bf16[256,128]{1,0:T(8,128)(2,1)S(1)}, u32[]{:S(2)}, u32[]{:S(2)}) collective-permute-start(bf16[256,128]{1,0:T(8,128)(2,1)S(1)} %copy-done.12), channel_id=1, source_target_pairs={{0,8},{8,16},{16,24},{24,0},{1,9},{9,17},{17,25},{25,1},{2,10},{10... | collective-permute-start | bytes 196616 | tf_op jit(solution)/shard_map/ppermute | solution.py:246
  92.0 4.6 %collective-permute-start.5 = (bf16[256,128]{1,0:T(8,128)(2,1)S(1)}, bf16[256,128]{1,0:T(8,128)(2,1)S(1)}, u32[]{:S(2)}, u32[]{:S(2)}) collective-permute-start(bf16[256,128]{1,0:T(8,128)(2,1)S(1)} %copy-done.11), channel_id=1, source_target_pairs={{0,16},{8,24},{16,0},{24,8},{1,17},{9,25},{17,1},{25,9},{2,18},{10... | collective-permute-start | bytes 196616 | tf_op jit(solution)/shard_map/ppermute | solution.py:246
  96.6 3.4 %collective-permute-start.6 = (bf16[256,128]{1,0:T(8,128)(2,1)S(1)}, bf16[256,128]{1,0:T(8,128)(2,1)S(1)}, u32[]{:S(2)}, u32[]{:S(2)}) collective-permute-start(bf16[256,128]{1,0:T(8,128)(2,1)S(1)} %copy-done.10), channel_id=1, source_target_pairs={{0,24},{8,0},{16,8},{24,16},{1,25},{9,1},{17,9},{25,17},{2,26},{10... | collective-permute-start | bytes 196616 | tf_op jit(solution)/shard_map/ppermute | solution.py:246
  100.0 6.6 %all-to-all-start.2 = ((bf16[16,32,128]{2,1,0:T(8,128)(2,1)}), bf16[16,32,128]{2,1,0:T(8,128)(2,1)S(1)}, u32[]{:S(2)}, u32[]{:S(2)}) async-start(bf16[16,32,128]{2,1,0:T(8,128)(2,1)} %get-tuple-element.43), calls=%async_computation.2 | async-start | bytes 262144 | tf_op jit(solution)/shard_map/all_to_all | solution.py:243
  106.6 0.0 collective-permute-done.4
  106.6 0.0 collective-permute-done.5
  106.6 0.0 collective-permute-done.6
  106.7 0.6 slice.15
  107.3 0.6 fusion
  108.0 11.9 %all-to-all-done.2 = bf16[16,32,128]{2,1,0:T(8,128)(2,1)S(1)} async-done(((bf16[16,32,128]{2,1,0:T(8,128)(2,1)}), bf16[16,32,128]{2,1,0:T(8,128)(2,1)S(1)}, u32[]{:S(2)}, u32[]{:S(2)}) %all-to-all-start.2) | async-done | bytes 131104 | tf_op jit(solution)/shard_map/all_to_all | solution.py:243
  119.8 0.6 convert_reduce_fusion
  (26 shorter events, 0.1 us)
Async XLA Ops:
  2.8 14.8 %copy-start.5 = (bf16[784,128]{1,0:T(8,128)(2,1)S(1)}, bf16[784,128]{1,0:T(8,128)(2,1)}, u32[]{:S(2)}) copy-start(bf16[784,128]{1,0:T(8,128)(2,1)} %get-tuple-element.25) | copy-start | bytes 602116
  2.8 46.6 %all-to-all-start = ((bf16[8,264,128]{2,1,0:T(8,128)(2,1)}), bf16[8,264,128]{2,1,0:T(8,128)(2,1)S(1)}, u32[]{:S(2)}, u32[]{:S(2)}) async-start(bf16[8,264,128]{2,1,0:T(8,128)(2,1)} %get-tuple-element.24), calls=%async_computation | async-start | bytes 1081344 | tf_op jit(solution)/shard_map/all_to_all | solution.py:220
  31.4 20.3 %copy-start = (bf16[3136,128]{1,0:T(8,128)(2,1)}, bf16[3136,128]{1,0:T(8,128)(2,1)S(1)}, u32[]{:S(2)}) copy-start(bf16[3136,128]{1,0:T(8,128)(2,1)S(1)} %all-gather) | copy-start | bytes 2408452
  33.3 42.8 %copy-start.4 = (bf16[8,64,128]{2,1,0:T(8,128)(2,1)}, bf16[8,64,128]{2,1,0:T(8,128)(2,1)S(1)}, u32[]{:S(2)}) copy-start(bf16[8,64,128]{2,1,0:T(8,128)(2,1)S(1)} %all-gather.1) | copy-start | bytes 393220
  33.3 7.4 %collective-permute-start = (bf16[2,4,64,128]{3,2,1,0:T(8,128)(2,1)S(1)}, bf16[2,4,64,128]{3,2,1,0:T(8,128)(2,1)S(1)}, u32[]{:S(2)}, u32[]{:S(2)}) collective-permute-start(bf16[2,4,64,128]{3,2,1,0:T(8,128)(2,1)S(1)} %bitcast.7), channel_id=1, source_target_pairs={{0,2},{2,4},{4,6},{6,0},{1,3},{3,5},{5,7},{7,1},{8,10},{10,12},{12... | collective-permute-start | bytes 393224 | tf_op jit(solution)/shard_map/ppermute | solution.py:226
  40.8 15.6 %copy-start.6 = (bf16[2,4,64,128]{3,2,1,0:T(8,128)(2,1)}, bf16[2,4,64,128]{3,2,1,0:T(8,128)(2,1)S(1)}, u32[]{:S(2)}) copy-start(bf16[2,4,64,128]{3,2,1,0:T(8,128)(2,1)S(1)} %collective-permute-done.rest_1_) | copy-start | bytes 393220
  49.4 2.3 %copy-start.1 = (bf16[8,264,128]{2,1,0:T(8,128)(2,1)}, bf16[8,264,128]{2,1,0:T(8,128)(2,1)S(1)}, u32[]{:S(2)}) copy-start(bf16[8,264,128]{2,1,0:T(8,128)(2,1)S(1)} %all-to-all-done.recv) | copy-start | bytes 1622020
  49.4 13.4 %collective-permute-start.1 = (bf16[8,264,128]{2,1,0:T(8,128)(2,1)S(1)}, bf16[8,264,128]{2,1,0:T(8,128)(2,1)S(1)}, u32[]{:S(2)}, u32[]{:S(2)}) collective-permute-start(bf16[8,264,128]{2,1,0:T(8,128)(2,1)S(1)} %all-to-all-done.recv), channel_id=1, source_target_pairs={{0,32},{32,0},{1,33},{33,1},{2,34},{34,2},{3,35},{35,3},{4,36},{36... | collective-permute-start | bytes 1622024 | tf_op jit(solution)/shard_map/ppermute | solution.py:228
  62.8 0.8 copy-start.3
  68.2 16.0 %all-to-all-start.1 = ((bf16[4,512,128]{2,1,0:T(8,128)(2,1)}), bf16[4,512,128]{2,1,0:T(8,128)(2,1)S(1)}, u32[]{:S(2)}, u32[]{:S(2)}) async-start(bf16[4,512,128]{2,1,0:T(8,128)(2,1)} %get-tuple-element.30), calls=%async_computation.1 | async-start | bytes 1048576 | tf_op jit(solution)/shard_map/all_to_all | solution.py:238
  72.7 15.3 %copy-start.12 = (bf16[256,128]{1,0:T(8,128)(2,1)S(1)}, bf16[256,128]{1,0:T(8,128)(2,1)}, u32[]{:S(2)}) copy-start(bf16[256,128]{1,0:T(8,128)(2,1)} %get-tuple-element.40) | copy-start | bytes 196612
  72.7 19.3 %copy-start.11 = (bf16[256,128]{1,0:T(8,128)(2,1)S(1)}, bf16[256,128]{1,0:T(8,128)(2,1)}, u32[]{:S(2)}) copy-start(bf16[256,128]{1,0:T(8,128)(2,1)} %get-tuple-element.41) | copy-start | bytes 196612
  72.7 23.9 %copy-start.10 = (bf16[256,128]{1,0:T(8,128)(2,1)S(1)}, bf16[256,128]{1,0:T(8,128)(2,1)}, u32[]{:S(2)}) copy-start(bf16[256,128]{1,0:T(8,128)(2,1)} %get-tuple-element.42) | copy-start | bytes 196612
  72.7 8.5 %collective-permute-start.2 = (bf16[2,4,64,128]{3,2,1,0:T(8,128)(2,1)S(1)}, bf16[2,4,64,128]{3,2,1,0:T(8,128)(2,1)S(1)}, u32[]{:S(2)}, u32[]{:S(2)}) collective-permute-start(bf16[2,4,64,128]{3,2,1,0:T(8,128)(2,1)S(1)} %bitcast.8), channel_id=1, source_target_pairs={{0,4},{2,6},{4,0},{6,2},{1,5},{3,7},{5,1},{7,3},{8,12},{10,14},{12... | collective-permute-start | bytes 393224 | tf_op jit(solution)/shard_map/ppermute | solution.py:226
  76.1 8.1 %collective-permute-start.3 = (bf16[2,4,64,128]{3,2,1,0:T(8,128)(2,1)S(1)}, bf16[2,4,64,128]{3,2,1,0:T(8,128)(2,1)S(1)}, u32[]{:S(2)}, u32[]{:S(2)}) collective-permute-start(bf16[2,4,64,128]{3,2,1,0:T(8,128)(2,1)S(1)} %bitcast.9), channel_id=1, source_target_pairs={{0,6},{2,0},{4,2},{6,4},{1,7},{3,1},{5,3},{7,5},{8,14},{10,8},{12,... | collective-permute-start | bytes 393224 | tf_op jit(solution)/shard_map/ppermute | solution.py:226
  81.2 3.1 %copy-start.7 = (bf16[2,4,64,128]{3,2,1,0:T(8,128)(2,1)}, bf16[2,4,64,128]{3,2,1,0:T(8,128)(2,1)S(1)}, u32[]{:S(2)}) copy-start(bf16[2,4,64,128]{3,2,1,0:T(8,128)(2,1)S(1)} %collective-permute-done.2.rest_2_) | copy-start | bytes 393220
  84.2 0.6 copy-start.8
  84.9 0.8 copy-start.2
  87.9 18.7 %copy-start.9 = (bf16[256,128]{1,0:T(8,128)(2,1)S(1)}, bf16[256,128]{1,0:T(8,128)(2,1)}, u32[]{:S(2)}) copy-start(bf16[256,128]{1,0:T(8,128)(2,1)} %get-tuple-element.39) | copy-start | bytes 196612
  87.9 18.7 %collective-permute-start.4 = (bf16[256,128]{1,0:T(8,128)(2,1)S(1)}, bf16[256,128]{1,0:T(8,128)(2,1)S(1)}, u32[]{:S(2)}, u32[]{:S(2)}) collective-permute-start(bf16[256,128]{1,0:T(8,128)(2,1)S(1)} %copy-done.12), channel_id=1, source_target_pairs={{0,8},{8,16},{16,24},{24,0},{1,9},{9,17},{17,25},{25,1},{2,10},{10... | collective-permute-start | bytes 196616 | tf_op jit(solution)/shard_map/ppermute | solution.py:246
  92.0 14.6 %collective-permute-start.5 = (bf16[256,128]{1,0:T(8,128)(2,1)S(1)}, bf16[256,128]{1,0:T(8,128)(2,1)S(1)}, u32[]{:S(2)}, u32[]{:S(2)}) collective-permute-start(bf16[256,128]{1,0:T(8,128)(2,1)S(1)} %copy-done.11), channel_id=1, source_target_pairs={{0,16},{8,24},{16,0},{24,8},{1,17},{9,25},{17,1},{25,9},{2,18},{10... | collective-permute-start | bytes 196616 | tf_op jit(solution)/shard_map/ppermute | solution.py:246
  96.6 10.1 %collective-permute-start.6 = (bf16[256,128]{1,0:T(8,128)(2,1)S(1)}, bf16[256,128]{1,0:T(8,128)(2,1)S(1)}, u32[]{:S(2)}, u32[]{:S(2)}) collective-permute-start(bf16[256,128]{1,0:T(8,128)(2,1)S(1)} %copy-done.10), channel_id=1, source_target_pairs={{0,24},{8,0},{16,8},{24,16},{1,25},{9,1},{17,9},{25,17},{2,26},{10... | collective-permute-start | bytes 196616 | tf_op jit(solution)/shard_map/ppermute | solution.py:246
  100.0 19.8 %all-to-all-start.2 = ((bf16[16,32,128]{2,1,0:T(8,128)(2,1)}), bf16[16,32,128]{2,1,0:T(8,128)(2,1)S(1)}, u32[]{:S(2)}, u32[]{:S(2)}) async-start(bf16[16,32,128]{2,1,0:T(8,128)(2,1)} %get-tuple-element.43), calls=%async_computation.2 | async-start | bytes 262144 | tf_op jit(solution)/shard_map/all_to_all | solution.py:243

commit v9 on v8

--- a/solution.py
+++ b/solution.py
@@ -224,7 +224,7 @@
     xts = [xt]
     for d in range(1, NX):
         xts.append(lax.ppermute(xt, "x", [(i, (i + d) % NX) for i in range(NX)]))
-    recv, *xts[:2] = lax.optimization_barrier((recv, *xts[:2]))
+    recv, *xts[:3] = lax.optimization_barrier((recv, *xts[:3]))
     relayed = lax.ppermute(recv, "zl", [(0, 1), (1, 0)])
     block = (NY * T, H)
     sums = call(first_body, [(block, f32)] * 3, [], 2)(recv, grp)
@@ -235,18 +235,18 @@
         5,
     )
     q_sums, *kv = second(relayed, grp, *sums)
+    turned = []
     q_sums = lax.all_to_all(q_sums, "y", 0, 0, tiled=True)
+    for d in range(1, NY):
+        turned.append(lax.ppermute(kv[d], "y", [(i, (i + d) % NY) for i in range(NY)]))
+    q_sums, *turned[:2] = lax.optimization_barrier((q_sums, *turned[:2]))
     outs = [((T, H), bf16), ((NZ, 32, H), bf16)]
     finish = call(finish_body, outs, [pltpu.VMEM(block, bf16)], 1 + NX)
     q_grad, zs = finish(q_sums, *xts)
-    zs, *kv = lax.optimization_barrier((zs, *kv))
     back = lax.all_to_all(zs, ("zp", "zl"), 0, 0, tiled=True)
-    total = kv[0].astype(f32)
-    for d in range(1, NY):
-        turned = lax.ppermute(kv[d], "y", [(i, (i + d) % NY) for i in range(NY)])
-        total = total + turned.astype(f32)
-    k_grad = (total[0:T] * SCALE).astype(bf16)
-    v_grad = total[T : 2 * T].astype(bf16)
+    parts = [kv[0], *turned]
+    k_grad = (sum(p[0:T].astype(f32) for p in parts) * SCALE).astype(bf16)
+    v_grad = sum(p[T : 2 * T].astype(f32) for p in parts).astype(bf16)
     return q_grad, k_grad, v_grad, jnp.sum(back.astype(f32), axis=0)
 
 

time: 121 us -> 116 us (0.959)
  waiting for transfers between devices: 38 us -> 28.1 us
  starting transfers between devices: 47.9 us -> 52.4 us
    ppermute x3, waiting for transfers between devices: 11.2 us -> 4.34 us  [per_device(): xts.append(lax.ppermute(xt, 'x', [(i, (i + d) % NX) for i in range(NX)]))]
    ppermute x3, waiting for transfers between devices: 0.01 us -> 6.08 us  [per_device(): lax.ppermute(kv[d], 'y', [(i, (i + d) % NY) for i in range(NY)])]
    all_to_all x1, waiting for transfers between devices: 11.9 us -> 6.32 us  [per_device(): back = lax.all_to_all(zs, ('zp', 'zl'), 0, 0, tiled=True)]
    all_to_all x1, waiting for transfers between devices: 8.6 us -> 4.98 us  [per_device(): lax.all_to_all(zsend, ('zp', 'zl'), 0, 0, axis_index_groups=GROUPS, tiled...]
    all_to_all x1, starting transfers between devices: 6.64 us -> 9.62 us  [per_device(): back = lax.all_to_all(zs, ('zp', 'zl'), 0, 0, tiled=True)]
    ppermute x3, starting transfers between devices: 7.75 us -> 9.42 us  [per_device(): xts.append(lax.ppermute(xt, 'x', [(i, (i + d) % NX) for i in range(NX)]))]
  transfers between devices with their start and end apart: 10 -> 10, of which waited for: 6 -> 7; matrix products, arithmetic and copies ran while one was open for 1% -> 1% of each run, Pallas kernels for 4% -> 4%
where the time goes in v9:
time: 116 us; the launch traced here: 114 us
  starting transfers between devices  52.4 us (45%)
  waiting for transfers between devices  28.1 us (24%)
  blocking collectives  15.8 us (14%)
  Pallas kernels  13.7 us (12%)
  local copies, waits for them, and re-layouts  2.32 us (2%)
  other arithmetic  1.3 us (1%)
    all_to_all x1, starting transfers between devices, per_device(): lax.all_to_all(zsend, ('zp', 'zl'), 0, 0, axis_index_groups=GROUPS, tiled...  14.8 us
    all_gather x1, blocking collectives, per_device(): grp = lax.all_gather(own, 'y', axis=0, tiled=False)  13.9 us
    ppermute x3, starting transfers between devices, per_device(): lax.ppermute(kv[d], 'y', [(i, (i + d) % NY) for i in range(NY)])  11.6 us
    all_to_all x1, starting transfers between devices, per_device(): back = lax.all_to_all(zs, ('zp', 'zl'), 0, 0, tiled=True)  9.62 us
    ppermute x3, starting transfers between devices, per_device(): xts.append(lax.ppermute(xt, 'x', [(i, (i + d) % NX) for i in range(NX)]))  9.42 us
    ppermute x1, waiting for transfers between devices, per_device(): relayed = lax.ppermute(recv, 'zl', [(0, 1), (1, 0)])  6.36 us
    all_to_all x1, waiting for transfers between devices, per_device(): back = lax.all_to_all(zs, ('zp', 'zl'), 0, 0, tiled=True)  6.32 us
    ppermute x3, waiting for transfers between devices, per_device(): lax.ppermute(kv[d], 'y', [(i, (i + d) % NY) for i in range(NY)])  6.08 us
  transfers between devices with their start and end apart: 10, of which 7 were waited for; matrix products, arithmetic and copies ran while one was open for 1% of the time, Pallas kernels for 4%

profile of v9, /device:TPU:6, one launch (start us, length us, event | category | flops | bytes accessed | tf_op | source)
XLA Modules:
  0.0 114.3 jit_solution(810664314371396417)
XLA Ops:
  0.6 2.1 %shard_map.111 = (bf16[8,264,128]{2,1,0:T(8,128)(2,1)}, bf16[784,128]{1,0:T(8,128)(2,1)}) custom-call(bf16[128,128]{1,0:T(8,128)(2,1)} %q.1, bf16[128,128]{1,0:T(8,128)(2,1)} %k.1, bf16[128,128]{1,0:T(8,128)(2,1)} %v.1, f32[1,128]{1,0:T(1,128)} %bitcast.11, f32[1,128]{1,0:T(1,128)} %bitcast.12, bf16[128,128]{1,0:T(8,128)(2,1)} %o.1, bf16[128,128]{1,0:T(8,128)(2,1)} %do.1, ...), custom_call_target="tpu_custom_call" | custom-call | tf_op jit(solution)/shard_map/pallas_call | solution.py:219
  2.8 14.8 %all-to-all-start = ((bf16[8,264,128]{2,1,0:T(8,128)(2,1)}), bf16[8,264,128]{2,1,0:T(8,128)(2,1)S(1)}, u32[]{:S(2)}, u32[]{:S(2)}) async-start(bf16[8,264,128]{2,1,0:T(8,128)(2,1)} %get-tuple-element.23), calls=%async_computation | async-start | bytes 1081344 | tf_op jit(solution)/shard_map/all_to_all | solution.py:220
  17.5 0.0 copy-done.5
  17.6 13.9 %all-gather = bf16[3136,128]{1,0:T(8,128)(2,1)S(1)} all-gather(bf16[784,128]{1,0:T(8,128)(2,1)S(1)} %copy-done.5), channel_id=2, replica_groups=mesh['zp'=8,'zl'=2,'y'=4,'x'=4,'c'=2] {'y'}, dimensions={0}, use_global_device_ids=true | all-gather | bytes 1003520 | tf_op jit(solution)/shard_map/all_gather | solution.py:221
  31.4 1.9 %all-gather.1 = bf16[8,64,128]{2,1,0:T(8,128)(2,1)S(1)} all-gather(bf16[4,64,128]{2,1,0:T(8,128)(2,1)S(1)} %pad_maximum_fusion), channel_id=3, replica_groups=mesh['zp'=8,'zl'=2,'y'=4,'x'=4,'c'=2] {'c'}, dimensions={0}, use_global_device_ids=true | all-gather | bytes 196608 | tf_op jit(solution)/shard_map/all_gather | solution.py:223
  33.3 2.4 %collective-permute-start = (bf16[2,4,64,128]{3,2,1,0:T(8,128)(2,1)S(1)}, bf16[2,4,64,128]{3,2,1,0:T(8,128)(2,1)S(1)}, u32[]{:S(2)}, u32[]{:S(2)}) collective-permute-start(bf16[2,4,64,128]{3,2,1,0:T(8,128)(2,1)S(1)} %bitcast.7), channel_id=1, source_target_pairs={{0,2},{2,4},{4,6},{6,0},{1,3},{3,5},{5,7},{7,1},{8,10},{10,12},{12... | collective-permute-start | bytes 393224 | tf_op jit(solution)/shard_map/ppermute | solution.py:226
  35.7 4.3 %collective-permute-start.1 = (bf16[2,4,64,128]{3,2,1,0:T(8,128)(2,1)S(1)}, bf16[2,4,64,128]{3,2,1,0:T(8,128)(2,1)S(1)}, u32[]{:S(2)}, u32[]{:S(2)}) collective-permute-start(bf16[2,4,64,128]{3,2,1,0:T(8,128)(2,1)S(1)} %bitcast.8), channel_id=1, source_target_pairs={{0,4},{2,6},{4,0},{6,2},{1,5},{3,7},{5,1},{7,3},{8,12},{10,14},{12... | collective-permute-start | bytes 393224 | tf_op jit(solution)/shard_map/ppermute | solution.py:226
  40.1 1.1 collective-permute-done.rest_1_
  41.2 3.2 %collective-permute-done.1.rest_2_ = bf16[2,4,64,128]{3,2,1,0:T(8,128)(2,1)S(1)} collective-permute-done((bf16[2,4,64,128]{3,2,1,0:T(8,128)(2,1)S(1)}, bf16[2,4,64,128]{3,2,1,0:T(8,128)(2,1)S(1)}, u32[]{:S(2)}, u32[]{:S(2)}) %collective-permute-start.1) | collective-permute-done | bytes 131104 | tf_op jit(solution)/shard_map/ppermute | solution.py:226
  44.4 5.0 %all-to-all-done.recv = bf16[8,264,128]{2,1,0:T(8,128)(2,1)S(1)} async-done(((bf16[8,264,128]{2,1,0:T(8,128)(2,1)}), bf16[8,264,128]{2,1,0:T(8,128)(2,1)S(1)}, u32[]{:S(2)}, u32[]{:S(2)}) %all-to-all-start) | async-done | bytes 540704 | tf_op jit(solution)/shard_map/all_to_all | solution.py:220
  49.4 2.3 %collective-permute-start.2 = (bf16[8,264,128]{2,1,0:T(8,128)(2,1)S(1)}, bf16[8,264,128]{2,1,0:T(8,128)(2,1)S(1)}, u32[]{:S(2)}, u32[]{:S(2)}) collective-permute-start(bf16[8,264,128]{2,1,0:T(8,128)(2,1)S(1)} %all-to-all-done.recv), channel_id=1, source_target_pairs={{0,32},{32,0},{1,33},{33,1},{2,34},{34,2},{3,35},{35,3},{4,36},{36... | collective-permute-start | bytes 1622024 | tf_op jit(solution)/shard_map/ppermute | solution.py:228
  51.7 4.7 %shard_map.112 = (f32[512,128]{1,0:T(8,128)}, f32[512,128]{1,0:T(8,128)}, f32[512,128]{1,0:T(8,128)}) custom-call(bf16[8,264,128]{2,1,0:T(8,128)(2,1)} %copy-done.1, bf16[4,784,128]{2,1,0:T(8,128)(2,1)} %bitcast.5), custom_call_target="tpu_custom_call" | custom-call | tf_op jit(solution)/shard_map/pallas_call | solution.py:230
  56.4 6.4 %collective-permute-done.2.recv = bf16[8,264,128]{2,1,0:T(8,128)(2,1)S(1)} collective-permute-done((bf16[8,264,128]{2,1,0:T(8,128)(2,1)S(1)}, bf16[8,264,128]{2,1,0:T(8,128)(2,1)S(1)}, u32[]{:S(2)}, u32[]{:S(2)}) %collective-permute-start.2) | collective-permute-done | bytes 540704 | tf_op jit(solution)/shard_map/ppermute | solution.py:228
  62.8 0.8 copy-done.3
  63.6 4.6 %shard_map.113 = (bf16[4,512,128]{2,1,0:T(8,128)(2,1)}, bf16[256,128]{1,0:T(8,128)(2,1)}, bf16[256,128]{1,0:T(8,128)(2,1)}, bf16[256,128]{1,0:T(8,128)(2,1)}, bf16[256,128]{1,0:T(8,128)(2,1)}) custom-call(bf16[8,264,128]{2,1,0:T(8,128)(2,1)} %copy-done.3, bf16[4,784,128]{2,1,0:T(8,128)(2,1)} %bitcast.6, f32[512,128]{1,0:T(8,128)} %get-tuple-element.26.dq0, ...), custom_call_target="tpu_custom_call" | custom-call | tf_op jit(solution)/shard_map/pallas_call | solution.py:237
  68.2 4.6 %all-to-all-start.1 = ((bf16[4,512,128]{2,1,0:T(8,128)(2,1)}), bf16[4,512,128]{2,1,0:T(8,128)(2,1)S(1)}, u32[]{:S(2)}, u32[]{:S(2)}) async-start(bf16[4,512,128]{2,1,0:T(8,128)(2,1)} %get-tuple-element.29), calls=%async_computation.1 | async-start | bytes 1048576 | tf_op jit(solution)/shard_map/all_to_all | solution.py:239
  72.8 2.7 %collective-permute-start.5 = (bf16[2,4,64,128]{3,2,1,0:T(8,128)(2,1)S(1)}, bf16[2,4,64,128]{3,2,1,0:T(8,128)(2,1)S(1)}, u32[]{:S(2)}, u32[]{:S(2)}) collective-permute-start(bf16[2,4,64,128]{3,2,1,0:T(8,128)(2,1)S(1)} %bitcast.9), channel_id=1, source_target_pairs={{0,6},{2,0},{4,2},{6,4},{1,7},{3,1},{5,3},{7,5},{8,14},{10,8},{12,... | collective-permute-start | bytes 393224 | tf_op jit(solution)/shard_map/ppermute | solution.py:226
  75.5 3.9 %collective-permute-start.3 = (bf16[256,128]{1,0:T(8,128)(2,1)S(1)}, bf16[256,128]{1,0:T(8,128)(2,1)S(1)}, u32[]{:S(2)}, u32[]{:S(2)}) collective-permute-start(bf16[256,128]{1,0:T(8,128)(2,1)S(1)} %copy-done.12), channel_id=1, source_target_pairs={{0,8},{8,16},{16,24},{24,0},{1,9},{9,17},{17,25},{25,1},{2,10},{10... | collective-permute-start | bytes 196616 | tf_op jit(solution)/shard_map/ppermute | solution.py:241
  79.5 4.6 %collective-permute-start.4 = (bf16[256,128]{1,0:T(8,128)(2,1)S(1)}, bf16[256,128]{1,0:T(8,128)(2,1)S(1)}, u32[]{:S(2)}, u32[]{:S(2)}) collective-permute-start(bf16[256,128]{1,0:T(8,128)(2,1)S(1)} %copy-done.11), channel_id=1, source_target_pairs={{0,16},{8,24},{16,0},{24,8},{1,17},{9,25},{17,1},{25,9},{2,18},{10... | collective-permute-start | bytes 196616 | tf_op jit(solution)/shard_map/ppermute | solution.py:241
  84.1 0.0 collective-permute-done.3
  84.1 3.1 %collective-permute-done.4 = bf16[256,128]{1,0:T(8,128)(2,1)S(1)} collective-permute-done((bf16[256,128]{1,0:T(8,128)(2,1)S(1)}, bf16[256,128]{1,0:T(8,128)(2,1)S(1)}, u32[]{:S(2)}, u32[]{:S(2)}) %collective-permute-start.4) | collective-permute-done | bytes 65568 | tf_op jit(solution)/shard_map/ppermute | solution.py:241
  87.1 0.0 all-to-all-done.1.sums
  87.1 0.0 collective-permute-done.5.rest_3_
  87.2 0.8 copy-done.2
  88.0 0.6 copy-done.8
  88.6 2.3 %shard_map.114 = (bf16[128,128]{1,0:T(8,128)(2,1)}, bf16[16,32,128]{2,1,0:T(8,128)(2,1)}) custom-call(bf16[4,512,128]{2,1,0:T(8,128)(2,1)} %copy-done.2, bf16[2,4,64,128]{3,2,1,0:T(8,128)(2,1)} %bitcast.10, bf16[2,4,64,128]{3,2,1,0:T(8,128)(2,1)} %copy-done.6, bf16[2,4,64,128]{3,2,1,0:T(8,128)(2,1)} %copy-done.7, bf16[2,4,64,128]{3,2,1,0:T(8,128)(2,1)} %copy-done.8), custom_call_target="tpu_custom_call" | custom-call | tf_op jit(solution)/shard_map/pallas_call | solution.py:245
  90.9 9.6 %all-to-all-start.2 = ((bf16[16,32,128]{2,1,0:T(8,128)(2,1)}), bf16[16,32,128]{2,1,0:T(8,128)(2,1)S(1)}, u32[]{:S(2)}, u32[]{:S(2)}) async-start(bf16[16,32,128]{2,1,0:T(8,128)(2,1)} %get-tuple-element.41), calls=%async_computation.2 | async-start | bytes 262144 | tf_op jit(solution)/shard_map/all_to_all | solution.py:246
  100.5 3.1 %collective-permute-start.6 = (bf16[256,128]{1,0:T(8,128)(2,1)S(1)}, bf16[256,128]{1,0:T(8,128)(2,1)S(1)}, u32[]{:S(2)}, u32[]{:S(2)}) collective-permute-start(bf16[256,128]{1,0:T(8,128)(2,1)S(1)} %copy-done.10), channel_id=1, source_target_pairs={{0,24},{8,0},{16,8},{24,16},{1,25},{9,1},{17,9},{25,17},{2,26},{10... | collective-permute-start | bytes 196616 | tf_op jit(solution)/shard_map/ppermute | solution.py:241
  103.6 3.0 %collective-permute-done.6 = bf16[256,128]{1,0:T(8,128)(2,1)S(1)} collective-permute-done((bf16[256,128]{1,0:T(8,128)(2,1)S(1)}, bf16[256,128]{1,0:T(8,128)(2,1)S(1)}, u32[]{:S(2)}, u32[]{:S(2)}) %collective-permute-start.6) | collective-permute-done | bytes 65568 | tf_op jit(solution)/shard_map/ppermute | solution.py:241
  106.7 0.7 add_convert_fusion
  107.3 6.3 %all-to-all-done.2 = bf16[16,32,128]{2,1,0:T(8,128)(2,1)S(1)} async-done(((bf16[16,32,128]{2,1,0:T(8,128)(2,1)}), bf16[16,32,128]{2,1,0:T(8,128)(2,1)S(1)}, u32[]{:S(2)}, u32[]{:S(2)}) %all-to-all-start.2) | async-done | bytes 131104 | tf_op jit(solution)/shard_map/all_to_all | solution.py:246
  113.7 0.6 convert_reduce_fusion
  (24 shorter events, 0.1 us)
Async XLA Ops:
  2.8 14.8 %copy-start.5 = (bf16[784,128]{1,0:T(8,128)(2,1)S(1)}, bf16[784,128]{1,0:T(8,128)(2,1)}, u32[]{:S(2)}) copy-start(bf16[784,128]{1,0:T(8,128)(2,1)} %get-tuple-element.24) | copy-start | bytes 602116
  2.8 46.6 %all-to-all-start = ((bf16[8,264,128]{2,1,0:T(8,128)(2,1)}), bf16[8,264,128]{2,1,0:T(8,128)(2,1)S(1)}, u32[]{:S(2)}, u32[]{:S(2)}) async-start(bf16[8,264,128]{2,1,0:T(8,128)(2,1)} %get-tuple-element.23), calls=%async_computation | async-start | bytes 1081344 | tf_op jit(solution)/shard_map/all_to_all | solution.py:220
  31.4 20.3 %copy-start = (bf16[3136,128]{1,0:T(8,128)(2,1)}, bf16[3136,128]{1,0:T(8,128)(2,1)S(1)}, u32[]{:S(2)}) copy-start(bf16[3136,128]{1,0:T(8,128)(2,1)S(1)} %all-gather) | copy-start | bytes 2408452
  33.3 39.4 %copy-start.4 = (bf16[8,64,128]{2,1,0:T(8,128)(2,1)}, bf16[8,64,128]{2,1,0:T(8,128)(2,1)S(1)}, u32[]{:S(2)}) copy-start(bf16[8,64,128]{2,1,0:T(8,128)(2,1)S(1)} %all-gather.1) | copy-start | bytes 393220
  33.3 7.8 %collective-permute-start = (bf16[2,4,64,128]{3,2,1,0:T(8,128)(2,1)S(1)}, bf16[2,4,64,128]{3,2,1,0:T(8,128)(2,1)S(1)}, u32[]{:S(2)}, u32[]{:S(2)}) collective-permute-start(bf16[2,4,64,128]{3,2,1,0:T(8,128)(2,1)S(1)} %bitcast.7), channel_id=1, source_target_pairs={{0,2},{2,4},{4,6},{6,0},{1,3},{3,5},{5,7},{7,1},{8,10},{10,12},{12... | collective-permute-start | bytes 393224 | tf_op jit(solution)/shard_map/ppermute | solution.py:226
  35.7 8.7 %collective-permute-start.1 = (bf16[2,4,64,128]{3,2,1,0:T(8,128)(2,1)S(1)}, bf16[2,4,64,128]{3,2,1,0:T(8,128)(2,1)S(1)}, u32[]{:S(2)}, u32[]{:S(2)}) collective-permute-start(bf16[2,4,64,128]{3,2,1,0:T(8,128)(2,1)S(1)} %bitcast.8), channel_id=1, source_target_pairs={{0,4},{2,6},{4,0},{6,2},{1,5},{3,7},{5,1},{7,3},{8,12},{10,14},{12... | collective-permute-start | bytes 393224 | tf_op jit(solution)/shard_map/ppermute | solution.py:226
  41.2 15.2 %copy-start.6 = (bf16[2,4,64,128]{3,2,1,0:T(8,128)(2,1)}, bf16[2,4,64,128]{3,2,1,0:T(8,128)(2,1)S(1)}, u32[]{:S(2)}) copy-start(bf16[2,4,64,128]{3,2,1,0:T(8,128)(2,1)S(1)} %collective-permute-done.rest_1_) | copy-start | bytes 393220
  44.4 12.0 %copy-start.7 = (bf16[2,4,64,128]{3,2,1,0:T(8,128)(2,1)}, bf16[2,4,64,128]{3,2,1,0:T(8,128)(2,1)S(1)}, u32[]{:S(2)}) copy-start(bf16[2,4,64,128]{3,2,1,0:T(8,128)(2,1)S(1)} %collective-permute-done.1.rest_2_) | copy-start | bytes 393220
  49.4 2.3 %copy-start.1 = (bf16[8,264,128]{2,1,0:T(8,128)(2,1)}, bf16[8,264,128]{2,1,0:T(8,128)(2,1)S(1)}, u32[]{:S(2)}) copy-start(bf16[8,264,128]{2,1,0:T(8,128)(2,1)S(1)} %all-to-all-done.recv) | copy-start | bytes 1622020
  49.4 13.4 %collective-permute-start.2 = (bf16[8,264,128]{2,1,0:T(8,128)(2,1)S(1)}, bf16[8,264,128]{2,1,0:T(8,128)(2,1)S(1)}, u32[]{:S(2)}, u32[]{:S(2)}) collective-permute-start(bf16[8,264,128]{2,1,0:T(8,128)(2,1)S(1)} %all-to-all-done.recv), channel_id=1, source_target_pairs={{0,32},{32,0},{1,33},{33,1},{2,34},{34,2},{3,35},{35,3},{4,36},{36... | collective-permute-start | bytes 1622024 | tf_op jit(solution)/shard_map/ppermute | solution.py:228
  62.8 0.8 copy-start.3
  68.2 7.3 %copy-start.12 = (bf16[256,128]{1,0:T(8,128)(2,1)S(1)}, bf16[256,128]{1,0:T(8,128)(2,1)}, u32[]{:S(2)}) copy-start(bf16[256,128]{1,0:T(8,128)(2,1)} %get-tuple-element.30) | copy-start | bytes 196612
  68.2 11.3 %copy-start.11 = (bf16[256,128]{1,0:T(8,128)(2,1)S(1)}, bf16[256,128]{1,0:T(8,128)(2,1)}, u32[]{:S(2)}) copy-start(bf16[256,128]{1,0:T(8,128)(2,1)} %get-tuple-element.31) | copy-start | bytes 196612
  68.2 19.0 %all-to-all-start.1 = ((bf16[4,512,128]{2,1,0:T(8,128)(2,1)}), bf16[4,512,128]{2,1,0:T(8,128)(2,1)S(1)}, u32[]{:S(2)}, u32[]{:S(2)}) async-start(bf16[4,512,128]{2,1,0:T(8,128)(2,1)} %get-tuple-element.29), calls=%async_computation.1 | async-start | bytes 1048576 | tf_op jit(solution)/shard_map/all_to_all | solution.py:239
  72.8 14.4 %collective-permute-start.5 = (bf16[2,4,64,128]{3,2,1,0:T(8,128)(2,1)S(1)}, bf16[2,4,64,128]{3,2,1,0:T(8,128)(2,1)S(1)}, u32[]{:S(2)}, u32[]{:S(2)}) collective-permute-start(bf16[2,4,64,128]{3,2,1,0:T(8,128)(2,1)S(1)} %bitcast.9), channel_id=1, source_target_pairs={{0,6},{2,0},{4,2},{6,4},{1,7},{3,1},{5,3},{7,5},{8,14},{10,8},{12,... | collective-permute-start | bytes 393224 | tf_op jit(solution)/shard_map/ppermute | solution.py:226
  75.5 8.5 %collective-permute-start.3 = (bf16[256,128]{1,0:T(8,128)(2,1)S(1)}, bf16[256,128]{1,0:T(8,128)(2,1)S(1)}, u32[]{:S(2)}, u32[]{:S(2)}) collective-permute-start(bf16[256,128]{1,0:T(8,128)(2,1)S(1)} %copy-done.12), channel_id=1, source_target_pairs={{0,8},{8,16},{16,24},{24,0},{1,9},{9,17},{17,25},{25,1},{2,10},{10... | collective-permute-start | bytes 196616 | tf_op jit(solution)/shard_map/ppermute | solution.py:241
  79.5 7.7 %collective-permute-start.4 = (bf16[256,128]{1,0:T(8,128)(2,1)S(1)}, bf16[256,128]{1,0:T(8,128)(2,1)S(1)}, u32[]{:S(2)}, u32[]{:S(2)}) collective-permute-start(bf16[256,128]{1,0:T(8,128)(2,1)S(1)} %copy-done.11), channel_id=1, source_target_pairs={{0,16},{8,24},{16,0},{24,8},{1,17},{9,25},{17,1},{25,9},{2,18},{10... | collective-permute-start | bytes 196616 | tf_op jit(solution)/shard_map/ppermute | solution.py:241
  87.1 0.8 copy-start.2
  88.0 0.6 copy-start.8
  90.9 9.6 %copy-start.10 = (bf16[256,128]{1,0:T(8,128)(2,1)S(1)}, bf16[256,128]{1,0:T(8,128)(2,1)}, u32[]{:S(2)}) copy-start(bf16[256,128]{1,0:T(8,128)(2,1)} %get-tuple-element.40) | copy-start | bytes 196612
  90.9 15.8 %copy-start.9 = (bf16[256,128]{1,0:T(8,128)(2,1)S(1)}, bf16[256,128]{1,0:T(8,128)(2,1)}, u32[]{:S(2)}) copy-start(bf16[256,128]{1,0:T(8,128)(2,1)} %get-tuple-element.37) | copy-start | bytes 196612
  90.9 22.8 %all-to-all-start.2 = ((bf16[16,32,128]{2,1,0:T(8,128)(2,1)}), bf16[16,32,128]{2,1,0:T(8,128)(2,1)S(1)}, u32[]{:S(2)}, u32[]{:S(2)}) async-start(bf16[16,32,128]{2,1,0:T(8,128)(2,1)} %get-tuple-element.41), calls=%async_computation.2 | async-start | bytes 262144 | tf_op jit(solution)/shard_map/all_to_all | solution.py:246
  100.5 6.2 %collective-permute-start.6 = (bf16[256,128]{1,0:T(8,128)(2,1)S(1)}, bf16[256,128]{1,0:T(8,128)(2,1)S(1)}, u32[]{:S(2)}, u32[]{:S(2)}) collective-permute-start(bf16[256,128]{1,0:T(8,128)(2,1)S(1)} %copy-done.10), channel_id=1, source_target_pairs={{0,24},{8,0},{16,8},{24,16},{1,25},{9,1},{17,9},{25,17},{2,26},{10... | collective-permute-start | bytes 196616 | tf_op jit(solution)/shard_map/ppermute | solution.py:241

commit v10 on v9

--- a/solution.py
+++ b/solution.py
@@ -221,11 +221,11 @@
     grp = lax.all_gather(own, "y", axis=0, tiled=False)
     part = [lax.dynamic_slice_in_dim(grp, XB + half * T + y * 32, 32, 1) for half in range(2)]
     xt = lax.all_gather(jnp.concatenate(part, axis=1), "c", axis=0, tiled=False)
+    recv, xt = lax.optimization_barrier((recv, xt))
     xts = [xt]
+    relayed = lax.ppermute(recv, "zl", [(0, 1), (1, 0)])
     for d in range(1, NX):
         xts.append(lax.ppermute(xt, "x", [(i, (i + d) % NX) for i in range(NX)]))
-    recv, *xts[:3] = lax.optimization_barrier((recv, *xts[:3]))
-    relayed = lax.ppermute(recv, "zl", [(0, 1), (1, 0)])
     block = (NY * T, H)
     sums = call(first_body, [(block, f32)] * 3, [], 2)(recv, grp)
     second = call(
@@ -235,16 +235,16 @@
         5,
     )
     q_sums, *kv = second(relayed, grp, *sums)
-    turned = []
     q_sums = lax.all_to_all(q_sums, "y", 0, 0, tiled=True)
-    for d in range(1, NY):
-        turned.append(lax.ppermute(kv[d], "y", [(i, (i + d) % NY) for i in range(NY)]))
-    q_sums, *turned[:2] = lax.optimization_barrier((q_sums, *turned[:2]))
+    q_sums, xts[3] = lax.optimization_barrier((q_sums, xts[3]))
     outs = [((T, H), bf16), ((NZ, 32, H), bf16)]
     finish = call(finish_body, outs, [pltpu.VMEM(block, bf16)], 1 + NX)
     q_grad, zs = finish(q_sums, *xts)
+    zs, *kv = lax.optimization_barrier((zs, *kv))
     back = lax.all_to_all(zs, ("zp", "zl"), 0, 0, tiled=True)
-    parts = [kv[0], *turned]
+    parts = [kv[0]]
+    for d in range(1, NY):
+        parts.append(lax.ppermute(kv[d], "y", [(i, (i + d) % NY) for i in range(NY)]))
     k_grad = (sum(p[0:T].astype(f32) for p in parts) * SCALE).astype(bf16)
     v_grad = sum(p[T : 2 * T].astype(f32) for p in parts).astype(bf16)
     return q_grad, k_grad, v_grad, jnp.sum(back.astype(f32), axis=0)

time: 116 us -> 115 us (level)
  waiting for transfers between devices: 28.1 us -> 31.4 us
  starting transfers between devices: 52.4 us -> 49.3 us
    all_to_all x1, waiting for transfers between devices: 4.98 us -> 16 us  [per_device(): lax.all_to_all(zsend, ('zp', 'zl'), 0, 0, axis_index_groups=GROUPS, tiled...]
    all_to_all x1, waiting for transfers between devices: 6.32 us -> 0.01 us  [per_device(): back = lax.all_to_all(zs, ('zp', 'zl'), 0, 0, tiled=True)]
    ppermute x3, waiting for transfers between devices: 6.08 us -> 2.77 us  [per_device(): lax.ppermute(kv[d], 'y', [(i, (i + d) % NY) for i in range(NY)])]
    all_to_all x1, starting transfers between devices: 9.62 us -> 6.77 us  [per_device(): back = lax.all_to_all(zs, ('zp', 'zl'), 0, 0, tiled=True)]
    ppermute x3, waiting for transfers between devices: 4.34 us -> 6.21 us  [per_device(): xts.append(lax.ppermute(xt, 'x', [(i, (i + d) % NX) for i in range(NX)]))]
  transfers between devices with their start and end apart: 10 -> 10, of which waited for: 7 -> 5; matrix products, arithmetic and copies ran while one was open for 1% -> 1% of each run, Pallas kernels for 4% -> 4%
where the time goes in v10:
time: 115 us; the launch traced here: 114 us
  starting transfers between devices  49.3 us (43%)
  waiting for transfers between devices  31.4 us (27%)
  blocking collectives  15.8 us (14%)
  Pallas kernels  13.7 us (12%)
  local copies, waits for them, and re-layouts  1.52 us (1%)
  other arithmetic  1.3 us (1%)
    all_to_all x1, waiting for transfers between devices, per_device(): lax.all_to_all(zsend, ('zp', 'zl'), 0, 0, axis_index_groups=GROUPS, tiled...  16 us
    all_to_all x1, starting transfers between devices, per_device(): lax.all_to_all(zsend, ('zp', 'zl'), 0, 0, axis_index_groups=GROUPS, tiled...  14.8 us
    all_gather x1, blocking collectives, per_device(): grp = lax.all_gather(own, 'y', axis=0, tiled=False)  13.9 us
    ppermute x3, starting transfers between devices, per_device(): lax.ppermute(kv[d], 'y', [(i, (i + d) % NY) for i in range(NY)])  11.9 us
    ppermute x3, starting transfers between devices, per_device(): xts.append(lax.ppermute(xt, 'x', [(i, (i + d) % NX) for i in range(NX)]))  9.14 us
    all_to_all x1, starting transfers between devices, per_device(): back = lax.all_to_all(zs, ('zp', 'zl'), 0, 0, tiled=True)  6.77 us
    ppermute x1, waiting for transfers between devices, per_device(): relayed = lax.ppermute(recv, 'zl', [(0, 1), (1, 0)])  6.37 us
    ppermute x3, waiting for transfers between devices, per_device(): xts.append(lax.ppermute(xt, 'x', [(i, (i + d) % NX) for i in range(NX)]))  6.21 us
  transfers between devices with their start and end apart: 10, of which 5 were waited for; matrix products, arithmetic and copies ran while one was open for 1% of the time, Pallas kernels for 4%

profile of v10, /device:TPU:6, one launch (start us, length us, event | category | flops | bytes accessed | tf_op | source)
XLA Modules:
  0.0 113.8 jit_solution(5835631289247380550)
XLA Ops:
  0.6 2.1 %shard_map.111 = (bf16[8,264,128]{2,1,0:T(8,128)(2,1)}, bf16[784,128]{1,0:T(8,128)(2,1)}) custom-call(bf16[128,128]{1,0:T(8,128)(2,1)} %q.1, bf16[128,128]{1,0:T(8,128)(2,1)} %k.1, bf16[128,128]{1,0:T(8,128)(2,1)} %v.1, f32[1,128]{1,0:T(1,128)} %bitcast.11, f32[1,128]{1,0:T(1,128)} %bitcast.12, bf16[128,128]{1,0:T(8,128)(2,1)} %o.1, bf16[128,128]{1,0:T(8,128)(2,1)} %do.1, ...), custom_call_target="tpu_custom_call" | custom-call | tf_op jit(solution)/shard_map/pallas_call | solution.py:219
  2.8 14.8 %all-to-all-start = ((bf16[8,264,128]{2,1,0:T(8,128)(2,1)}), bf16[8,264,128]{2,1,0:T(8,128)(2,1)S(1)}, u32[]{:S(2)}, u32[]{:S(2)}) async-start(bf16[8,264,128]{2,1,0:T(8,128)(2,1)} %get-tuple-element.25), calls=%async_computation | async-start | bytes 1081344 | tf_op jit(solution)/shard_map/all_to_all | solution.py:220
  17.5 0.0 copy-done.5
  17.6 13.9 %all-gather = bf16[3136,128]{1,0:T(8,128)(2,1)S(1)} all-gather(bf16[784,128]{1,0:T(8,128)(2,1)S(1)} %copy-done.5), channel_id=2, replica_groups=mesh['zp'=8,'zl'=2,'y'=4,'x'=4,'c'=2] {'y'}, dimensions={0}, use_global_device_ids=true | all-gather | bytes 1003520 | tf_op jit(solution)/shard_map/all_gather | solution.py:221
  31.4 1.9 %all-gather.1 = bf16[8,64,128]{2,1,0:T(8,128)(2,1)S(1)} all-gather(bf16[4,64,128]{2,1,0:T(8,128)(2,1)S(1)} %pad_maximum_fusion), channel_id=3, replica_groups=mesh['zp'=8,'zl'=2,'y'=4,'x'=4,'c'=2] {'c'}, dimensions={0}, use_global_device_ids=true | all-gather | bytes 196608 | tf_op jit(solution)/shard_map/all_gather | solution.py:223
  33.3 16.0 %all-to-all-done.recv = bf16[8,264,128]{2,1,0:T(8,128)(2,1)S(1)} async-done(((bf16[8,264,128]{2,1,0:T(8,128)(2,1)}), bf16[8,264,128]{2,1,0:T(8,128)(2,1)S(1)}, u32[]{:S(2)}, u32[]{:S(2)}) %all-to-all-start) | async-done | bytes 540704 | tf_op jit(solution)/shard_map/all_to_all | solution.py:220
  49.4 2.3 %collective-permute-start = (bf16[8,264,128]{2,1,0:T(8,128)(2,1)S(1)}, bf16[8,264,128]{2,1,0:T(8,128)(2,1)S(1)}, u32[]{:S(2)}, u32[]{:S(2)}) collective-permute-start(bf16[8,264,128]{2,1,0:T(8,128)(2,1)S(1)} %all-to-all-done.recv), channel_id=1, source_target_pairs={{0,32},{32,0},{1,33},{33,1},{2,34},{34,2},{3,35},{35,3},{4,36},{36... | collective-permute-start | bytes 1622024 | tf_op jit(solution)/shard_map/ppermute | solution.py:226
  51.7 0.0 copy-done
  51.7 4.7 %shard_map.112 = (f32[512,128]{1,0:T(8,128)}, f32[512,128]{1,0:T(8,128)}, f32[512,128]{1,0:T(8,128)}) custom-call(bf16[8,264,128]{2,1,0:T(8,128)(2,1)} %copy-done.1, bf16[4,784,128]{2,1,0:T(8,128)(2,1)} %bitcast.5), custom_call_target="tpu_custom_call" | custom-call | tf_op jit(solution)/shard_map/pallas_call | solution.py:230
  56.4 6.4 %collective-permute-done.recv = bf16[8,264,128]{2,1,0:T(8,128)(2,1)S(1)} collective-permute-done((bf16[8,264,128]{2,1,0:T(8,128)(2,1)S(1)}, bf16[8,264,128]{2,1,0:T(8,128)(2,1)S(1)}, u32[]{:S(2)}, u32[]{:S(2)}) %collective-permute-start) | collective-permute-done | bytes 540704 | tf_op jit(solution)/shard_map/ppermute | solution.py:226
  62.8 0.8 copy-done.3
  63.6 4.6 %shard_map.113 = (bf16[4,512,128]{2,1,0:T(8,128)(2,1)}, bf16[256,128]{1,0:T(8,128)(2,1)}, bf16[256,128]{1,0:T(8,128)(2,1)}, bf16[256,128]{1,0:T(8,128)(2,1)}, bf16[256,128]{1,0:T(8,128)(2,1)}) custom-call(bf16[8,264,128]{2,1,0:T(8,128)(2,1)} %copy-done.3, bf16[4,784,128]{2,1,0:T(8,128)(2,1)} %bitcast.6, f32[512,128]{1,0:T(8,128)} %get-tuple-element.28.dq0, ...), custom_call_target="tpu_custom_call" | custom-call | tf_op jit(solution)/shard_map/pallas_call | solution.py:237
  68.2 4.5 %all-to-all-start.1 = ((bf16[4,512,128]{2,1,0:T(8,128)(2,1)}), bf16[4,512,128]{2,1,0:T(8,128)(2,1)S(1)}, u32[]{:S(2)}, u32[]{:S(2)}) async-start(bf16[4,512,128]{2,1,0:T(8,128)(2,1)} %get-tuple-element.31), calls=%async_computation.1 | async-start | bytes 1048576 | tf_op jit(solution)/shard_map/all_to_all | solution.py:238
  72.6 2.7 %collective-permute-start.1 = (bf16[2,4,64,128]{3,2,1,0:T(8,128)(2,1)S(1)}, bf16[2,4,64,128]{3,2,1,0:T(8,128)(2,1)S(1)}, u32[]{:S(2)}, u32[]{:S(2)}) collective-permute-start(bf16[2,4,64,128]{3,2,1,0:T(8,128)(2,1)S(1)} %bitcast.7), channel_id=1, source_target_pairs={{0,6},{2,0},{4,2},{6,4},{1,7},{3,1},{5,3},{7,5},{8,14},{10,8},{12,... | collective-permute-start | bytes 393224 | tf_op jit(solution)/shard_map/ppermute | solution.py:228
  75.4 4.3 %collective-permute-start.2 = (bf16[2,4,64,128]{3,2,1,0:T(8,128)(2,1)S(1)}, bf16[2,4,64,128]{3,2,1,0:T(8,128)(2,1)S(1)}, u32[]{:S(2)}, u32[]{:S(2)}) collective-permute-start(bf16[2,4,64,128]{3,2,1,0:T(8,128)(2,1)S(1)} %bitcast.8), channel_id=1, source_target_pairs={{0,2},{2,4},{4,6},{6,0},{1,3},{3,5},{5,7},{7,1},{8,10},{10,12},{12... | collective-permute-start | bytes 393224 | tf_op jit(solution)/shard_map/ppermute | solution.py:228
  79.7 2.1 %collective-permute-start.3 = (bf16[2,4,64,128]{3,2,1,0:T(8,128)(2,1)S(1)}, bf16[2,4,64,128]{3,2,1,0:T(8,128)(2,1)S(1)}, u32[]{:S(2)}, u32[]{:S(2)}) collective-permute-start(bf16[2,4,64,128]{3,2,1,0:T(8,128)(2,1)S(1)} %bitcast.9), channel_id=1, source_target_pairs={{0,4},{2,6},{4,0},{6,2},{1,5},{3,7},{5,1},{7,3},{8,12},{10,14},{12... | collective-permute-start | bytes 393224 | tf_op jit(solution)/shard_map/ppermute | solution.py:228
  81.8 0.0 collective-permute-done.1.rest_3_
  81.8 0.0 all-to-all-done.1.sums
  81.8 0.4 collective-permute-done.2.rest_1_
  82.2 5.8 %collective-permute-done.3.rest_2_ = bf16[2,4,64,128]{3,2,1,0:T(8,128)(2,1)S(1)} collective-permute-done((bf16[2,4,64,128]{3,2,1,0:T(8,128)(2,1)S(1)}, bf16[2,4,64,128]{3,2,1,0:T(8,128)(2,1)S(1)}, u32[]{:S(2)}, u32[]{:S(2)}) %collective-permute-start.3) | collective-permute-done | bytes 131104 | tf_op jit(solution)/shard_map/ppermute | solution.py:228
  88.1 0.6 copy-done.8
  88.7 2.3 %shard_map.114 = (bf16[128,128]{1,0:T(8,128)(2,1)}, bf16[16,32,128]{2,1,0:T(8,128)(2,1)}) custom-call(bf16[4,512,128]{2,1,0:T(8,128)(2,1)} %copy-done.2, bf16[2,4,64,128]{3,2,1,0:T(8,128)(2,1)} %bitcast.10, bf16[2,4,64,128]{3,2,1,0:T(8,128)(2,1)} %copy-done.7, bf16[2,4,64,128]{3,2,1,0:T(8,128)(2,1)} %copy-done.8, bf16[2,4,64,128]{3,2,1,0:T(8,128)(2,1)} %copy-done.6), custom_call_target="tpu_custom_call" | custom-call | tf_op jit(solution)/shard_map/pallas_call | solution.py:242
  91.0 6.8 %all-to-all-start.2 = ((bf16[16,32,128]{2,1,0:T(8,128)(2,1)}), bf16[16,32,128]{2,1,0:T(8,128)(2,1)S(1)}, u32[]{:S(2)}, u32[]{:S(2)}) async-start(bf16[16,32,128]{2,1,0:T(8,128)(2,1)} %get-tuple-element.45), calls=%async_computation.2 | async-start | bytes 262144 | tf_op jit(solution)/shard_map/all_to_all | solution.py:244
  97.8 3.9 %collective-permute-start.4 = (bf16[256,128]{1,0:T(8,128)(2,1)S(1)}, bf16[256,128]{1,0:T(8,128)(2,1)S(1)}, u32[]{:S(2)}, u32[]{:S(2)}) collective-permute-start(bf16[256,128]{1,0:T(8,128)(2,1)S(1)} %copy-done.12), channel_id=1, source_target_pairs={{0,8},{8,16},{16,24},{24,0},{1,9},{9,17},{17,25},{25,1},{2,10},{10... | collective-permute-start | bytes 196616 | tf_op jit(solution)/shard_map/ppermute | solution.py:247
  101.7 4.6 %collective-permute-start.5 = (bf16[256,128]{1,0:T(8,128)(2,1)S(1)}, bf16[256,128]{1,0:T(8,128)(2,1)S(1)}, u32[]{:S(2)}, u32[]{:S(2)}) collective-permute-start(bf16[256,128]{1,0:T(8,128)(2,1)S(1)} %copy-done.11), channel_id=1, source_target_pairs={{0,16},{8,24},{16,0},{24,8},{1,17},{9,25},{17,1},{25,9},{2,18},{10... | collective-permute-start | bytes 196616 | tf_op jit(solution)/shard_map/ppermute | solution.py:247
  106.3 3.4 %collective-permute-start.6 = (bf16[256,128]{1,0:T(8,128)(2,1)S(1)}, bf16[256,128]{1,0:T(8,128)(2,1)S(1)}, u32[]{:S(2)}, u32[]{:S(2)}) collective-permute-start(bf16[256,128]{1,0:T(8,128)(2,1)S(1)} %copy-done.10), channel_id=1, source_target_pairs={{0,24},{8,0},{16,8},{24,16},{1,25},{9,1},{17,9},{25,17},{2,26},{10... | collective-permute-start | bytes 196616 | tf_op jit(solution)/shard_map/ppermute | solution.py:247
  109.7 0.0 collective-permute-done.4
  109.7 0.0 collective-permute-done.5
  109.7 2.8 %collective-permute-done.6 = bf16[256,128]{1,0:T(8,128)(2,1)S(1)} collective-permute-done((bf16[256,128]{1,0:T(8,128)(2,1)S(1)}, bf16[256,128]{1,0:T(8,128)(2,1)S(1)}, u32[]{:S(2)}, u32[]{:S(2)}) %collective-permute-start.6) | collective-permute-done | bytes 65568 | tf_op jit(solution)/shard_map/ppermute | solution.py:247
  112.5 0.7 add_convert_fusion
  113.2 0.0 all-to-all-done.2
  113.2 0.6 convert_reduce_fusion
  (24 shorter events, 0.1 us)
Async XLA Ops:
  2.8 14.8 %copy-start.5 = (bf16[784,128]{1,0:T(8,128)(2,1)S(1)}, bf16[784,128]{1,0:T(8,128)(2,1)}, u32[]{:S(2)}) copy-start(bf16[784,128]{1,0:T(8,128)(2,1)} %get-tuple-element.26) | copy-start | bytes 602116
  2.8 46.6 %all-to-all-start = ((bf16[8,264,128]{2,1,0:T(8,128)(2,1)}), bf16[8,264,128]{2,1,0:T(8,128)(2,1)S(1)}, u32[]{:S(2)}, u32[]{:S(2)}) async-start(bf16[8,264,128]{2,1,0:T(8,128)(2,1)} %get-tuple-element.25), calls=%async_computation | async-start | bytes 1081344 | tf_op jit(solution)/shard_map/all_to_all | solution.py:220
  31.4 20.3 %copy-start = (bf16[3136,128]{1,0:T(8,128)(2,1)}, bf16[3136,128]{1,0:T(8,128)(2,1)S(1)}, u32[]{:S(2)}) copy-start(bf16[3136,128]{1,0:T(8,128)(2,1)S(1)} %all-gather) | copy-start | bytes 2408452
  33.3 46.3 %copy-start.4 = (bf16[8,64,128]{2,1,0:T(8,128)(2,1)}, bf16[8,64,128]{2,1,0:T(8,128)(2,1)S(1)}, u32[]{:S(2)}) copy-start(bf16[8,64,128]{2,1,0:T(8,128)(2,1)S(1)} %all-gather.1) | copy-start | bytes 393220
  49.4 2.3 %copy-start.1 = (bf16[8,264,128]{2,1,0:T(8,128)(2,1)}, bf16[8,264,128]{2,1,0:T(8,128)(2,1)S(1)}, u32[]{:S(2)}) copy-start(bf16[8,264,128]{2,1,0:T(8,128)(2,1)S(1)} %all-to-all-done.recv) | copy-start | bytes 1622020
  49.4 13.4 %collective-permute-start = (bf16[8,264,128]{2,1,0:T(8,128)(2,1)S(1)}, bf16[8,264,128]{2,1,0:T(8,128)(2,1)S(1)}, u32[]{:S(2)}, u32[]{:S(2)}) collective-permute-start(bf16[8,264,128]{2,1,0:T(8,128)(2,1)S(1)} %all-to-all-done.recv), channel_id=1, source_target_pairs={{0,32},{32,0},{1,33},{33,1},{2,34},{34,2},{3,35},{35,3},{4,36},{36... | collective-permute-start | bytes 1622024 | tf_op jit(solution)/shard_map/ppermute | solution.py:226
  62.8 0.8 copy-start.3
  68.2 13.7 %all-to-all-start.1 = ((bf16[4,512,128]{2,1,0:T(8,128)(2,1)}), bf16[4,512,128]{2,1,0:T(8,128)(2,1)S(1)}, u32[]{:S(2)}, u32[]{:S(2)}) async-start(bf16[4,512,128]{2,1,0:T(8,128)(2,1)} %get-tuple-element.31), calls=%async_computation.1 | async-start | bytes 1048576 | tf_op jit(solution)/shard_map/all_to_all | solution.py:238
  72.6 9.2 %collective-permute-start.1 = (bf16[2,4,64,128]{3,2,1,0:T(8,128)(2,1)S(1)}, bf16[2,4,64,128]{3,2,1,0:T(8,128)(2,1)S(1)}, u32[]{:S(2)}, u32[]{:S(2)}) collective-permute-start(bf16[2,4,64,128]{3,2,1,0:T(8,128)(2,1)S(1)} %bitcast.7), channel_id=1, source_target_pairs={{0,6},{2,0},{4,2},{6,4},{1,7},{3,1},{5,3},{7,5},{8,14},{10,8},{12,... | collective-permute-start | bytes 393224 | tf_op jit(solution)/shard_map/ppermute | solution.py:228
  75.4 6.9 %collective-permute-start.2 = (bf16[2,4,64,128]{3,2,1,0:T(8,128)(2,1)S(1)}, bf16[2,4,64,128]{3,2,1,0:T(8,128)(2,1)S(1)}, u32[]{:S(2)}, u32[]{:S(2)}) collective-permute-start(bf16[2,4,64,128]{3,2,1,0:T(8,128)(2,1)S(1)} %bitcast.8), channel_id=1, source_target_pairs={{0,2},{2,4},{4,6},{6,0},{1,3},{3,5},{5,7},{7,1},{8,10},{10,12},{12... | collective-permute-start | bytes 393224 | tf_op jit(solution)/shard_map/ppermute | solution.py:228
  79.7 8.4 %collective-permute-start.3 = (bf16[2,4,64,128]{3,2,1,0:T(8,128)(2,1)S(1)}, bf16[2,4,64,128]{3,2,1,0:T(8,128)(2,1)S(1)}, u32[]{:S(2)}, u32[]{:S(2)}) collective-permute-start(bf16[2,4,64,128]{3,2,1,0:T(8,128)(2,1)S(1)} %bitcast.9), channel_id=1, source_target_pairs={{0,4},{2,6},{4,0},{6,2},{1,5},{3,7},{5,1},{7,3},{8,12},{10,14},{12... | collective-permute-start | bytes 393224 | tf_op jit(solution)/shard_map/ppermute | solution.py:228
  81.8 6.2 %copy-start.6 = (bf16[2,4,64,128]{3,2,1,0:T(8,128)(2,1)}, bf16[2,4,64,128]{3,2,1,0:T(8,128)(2,1)S(1)}, u32[]{:S(2)}) copy-start(bf16[2,4,64,128]{3,2,1,0:T(8,128)(2,1)S(1)} %collective-permute-done.1.rest_3_) | copy-start | bytes 393220
  81.8 6.2 %copy-start.2 = (bf16[4,512,128]{2,1,0:T(8,128)(2,1)}, bf16[4,512,128]{2,1,0:T(8,128)(2,1)S(1)}, u32[]{:S(2)}) copy-start(bf16[4,512,128]{2,1,0:T(8,128)(2,1)S(1)} %all-to-all-done.1.sums) | copy-start | bytes 1572868
  82.2 5.8 %copy-start.7 = (bf16[2,4,64,128]{3,2,1,0:T(8,128)(2,1)}, bf16[2,4,64,128]{3,2,1,0:T(8,128)(2,1)S(1)}, u32[]{:S(2)}) copy-start(bf16[2,4,64,128]{3,2,1,0:T(8,128)(2,1)S(1)} %collective-permute-done.2.rest_1_) | copy-start | bytes 393220
  88.1 0.7 copy-start.8
  91.0 6.8 %copy-start.12 = (bf16[256,128]{1,0:T(8,128)(2,1)S(1)}, bf16[256,128]{1,0:T(8,128)(2,1)}, u32[]{:S(2)}) copy-start(bf16[256,128]{1,0:T(8,128)(2,1)} %get-tuple-element.42) | copy-start | bytes 196612
  91.0 10.7 %copy-start.11 = (bf16[256,128]{1,0:T(8,128)(2,1)S(1)}, bf16[256,128]{1,0:T(8,128)(2,1)}, u32[]{:S(2)}) copy-start(bf16[256,128]{1,0:T(8,128)(2,1)} %get-tuple-element.43) | copy-start | bytes 196612
  91.0 15.3 %copy-start.10 = (bf16[256,128]{1,0:T(8,128)(2,1)S(1)}, bf16[256,128]{1,0:T(8,128)(2,1)}, u32[]{:S(2)}) copy-start(bf16[256,128]{1,0:T(8,128)(2,1)} %get-tuple-element.44) | copy-start | bytes 196612
  91.0 21.5 %copy-start.9 = (bf16[256,128]{1,0:T(8,128)(2,1)S(1)}, bf16[256,128]{1,0:T(8,128)(2,1)}, u32[]{:S(2)}) copy-start(bf16[256,128]{1,0:T(8,128)(2,1)} %get-tuple-element.41) | copy-start | bytes 196612
  91.0 22.2 %all-to-all-start.2 = ((bf16[16,32,128]{2,1,0:T(8,128)(2,1)}), bf16[16,32,128]{2,1,0:T(8,128)(2,1)S(1)}, u32[]{:S(2)}, u32[]{:S(2)}) async-start(bf16[16,32,128]{2,1,0:T(8,128)(2,1)} %get-tuple-element.45), calls=%async_computation.2 | async-start | bytes 262144 | tf_op jit(solution)/shard_map/all_to_all | solution.py:244
  97.8 11.9 %collective-permute-start.4 = (bf16[256,128]{1,0:T(8,128)(2,1)S(1)}, bf16[256,128]{1,0:T(8,128)(2,1)S(1)}, u32[]{:S(2)}, u32[]{:S(2)}) collective-permute-start(bf16[256,128]{1,0:T(8,128)(2,1)S(1)} %copy-done.12), channel_id=1, source_target_pairs={{0,8},{8,16},{16,24},{24,0},{1,9},{9,17},{17,25},{25,1},{2,10},{10... | collective-permute-start | bytes 196616 | tf_op jit(solution)/shard_map/ppermute | solution.py:247
  101.7 8.0 %collective-permute-start.5 = (bf16[256,128]{1,0:T(8,128)(2,1)S(1)}, bf16[256,128]{1,0:T(8,128)(2,1)S(1)}, u32[]{:S(2)}, u32[]{:S(2)}) collective-permute-start(bf16[256,128]{1,0:T(8,128)(2,1)S(1)} %copy-done.11), channel_id=1, source_target_pairs={{0,16},{8,24},{16,0},{24,8},{1,17},{9,25},{17,1},{25,9},{2,18},{10... | collective-permute-start | bytes 196616 | tf_op jit(solution)/shard_map/ppermute | solution.py:247
  106.3 6.2 %collective-permute-start.6 = (bf16[256,128]{1,0:T(8,128)(2,1)S(1)}, bf16[256,128]{1,0:T(8,128)(2,1)S(1)}, u32[]{:S(2)}, u32[]{:S(2)}) collective-permute-start(bf16[256,128]{1,0:T(8,128)(2,1)S(1)} %copy-done.10), channel_id=1, source_target_pairs={{0,24},{8,0},{16,8},{24,16},{1,25},{9,1},{17,9},{25,17},{2,26},{10... | collective-permute-start | bytes 196616 | tf_op jit(solution)/shard_map/ppermute | solution.py:247

commit v11 on v10

--- a/solution.py
+++ b/solution.py
@@ -199,47 +199,52 @@
     return [pl.BlockSpec(memory_space=pltpu.VMEM)] * count
 
 
+def in_vmem(a):
+    return pltpu.with_memory_space_constraint(a, pltpu.VMEM)
+
+
 def position():
     return [lax.axis_index(n) for n in ("zp", "zl", "y", "x")]
 
 
-def call(body, out_shape, scratch, count):
+def call(body, outs, scratch, count, kept=0, limit=16 * 2**20):
+    shapes = [pltpu.VMEM(*o) if i >= kept else jax.ShapeDtypeStruct(*o) for i, o in enumerate(outs)]
     return pl.pallas_call(
         body,
         in_specs=vmem(count),
-        out_specs=tuple(vmem(len(out_shape))),
-        out_shape=tuple(jax.ShapeDtypeStruct(s, d) for s, d in out_shape),
+        out_specs=tuple(vmem(len(outs))),
+        out_shape=tuple(shapes),
         scratch_shapes=scratch,
+        compiler_params=pltpu.CompilerParams(vmem_limit_bytes=limit),
     )
 
 
 def per_device(q, k, v, g, lse, o, do, x):
     y = lax.axis_index("y")
-    pack = call(pack_body, [((NP, ZB, H), bf16), ((YB, H), bf16)], [], 8)
+    pack = call(pack_body, [((NP, ZB, H), bf16), ((YB, H), bf16)], [], 8, limit=60 * 2**20)
     zsend, own = pack(q, k, v, g.reshape(1, T), lse.reshape(1, T), o, do, x)
     recv = lax.all_to_all(zsend, ("zp", "zl"), 0, 0, axis_index_groups=GROUPS, tiled=True)
     grp = lax.all_gather(own, "y", axis=0, tiled=False)
     part = [lax.dynamic_slice_in_dim(grp, XB + half * T + y * 32, 32, 1) for half in range(2)]
     xt = lax.all_gather(jnp.concatenate(part, axis=1), "c", axis=0, tiled=False)
-    recv, xt = lax.optimization_barrier((recv, xt))
     xts = [xt]
-    relayed = lax.ppermute(recv, "zl", [(0, 1), (1, 0)])
     for d in range(1, NX):
         xts.append(lax.ppermute(xt, "x", [(i, (i + d) % NX) for i in range(NX)]))
+    recv, *xts[:2] = lax.optimization_barrier((recv, *xts[:2]))
+    relayed = lax.ppermute(recv, "zl", [(0, 1), (1, 0)])
     block = (NY * T, H)
-    sums = call(first_body, [(block, f32)] * 3, [], 2)(recv, grp)
+    sums = call(first_body, [(block, f32)] * 3, [], 2)(in_vmem(recv), in_vmem(grp))
     second = call(
         last_body,
         [((NY, NY * T, H), bf16)] + [((2 * T, H), bf16)] * NY,
         [pltpu.VMEM(block, f32)] * 3,
         5,
     )
-    q_sums, *kv = second(relayed, grp, *sums)
+    q_sums, *kv = second(*[in_vmem(a) for a in (relayed, grp, *sums)])
     q_sums = lax.all_to_all(q_sums, "y", 0, 0, tiled=True)
-    q_sums, xts[3] = lax.optimization_barrier((q_sums, xts[3]))
     outs = [((T, H), bf16), ((NZ, 32, H), bf16)]
-    finish = call(finish_body, outs, [pltpu.VMEM(block, bf16)], 1 + NX)
-    q_grad, zs = finish(q_sums, *xts)
+    finish = call(finish_body, outs, [pltpu.VMEM(block, bf16)], 1 + NX, kept=1)
+    q_grad, zs = finish(in_vmem(q_sums), *[in_vmem(a) for a in xts])
     zs, *kv = lax.optimization_barrier((zs, *kv))
     back = lax.all_to_all(zs, ("zp", "zl"), 0, 0, tiled=True)
     parts = [kv[0]]

time: 115 us -> 106 us (0.922)
  Pallas kernels: 13.7 us -> 8.5 us
  starting transfers between devices: 49.3 us -> 47.5 us
  local copies, waits for them, and re-layouts: 1.52 us -> 0.01 us
    all_to_all x1, waiting for transfers between devices: 16 us -> 8.62 us  [per_device(): lax.all_to_all(zsend, ('zp', 'zl'), 0, 0, axis_index_groups=GROUPS, tiled...]
    pallas_call x3, Pallas kernels: 11.5 us -> 6.46 us  [the longest x1 2.94 us: per_device(): q_sums, *kv = second(*[in_vmem(a) for a in (relayed, grp, *sums)])]
    ppermute x3, waiting for transfers between devices: 6.21 us -> 11.2 us  [per_device(): xts.append(lax.ppermute(xt, 'x', [(i, (i + d) % NX) for i in range(NX)]))]
    ppermute x1, waiting for transfers between devices: 6.37 us -> 8.58 us  [per_device(): relayed = lax.ppermute(recv, 'zl', [(0, 1), (1, 0)])]
    ppermute x3, starting transfers between devices: 9.14 us -> 7.6 us  [per_device(): xts.append(lax.ppermute(xt, 'x', [(i, (i + d) % NX) for i in range(NX)]))]
    unnamed x26 -> x0, local copies, waits for them, and re-layouts: 1.52 us -> none
  transfers between devices with their start and end apart: 10 -> 10, of which waited for: 5 -> 6; matrix products, arithmetic and copies ran while one was open for 1% -> 1% of each run, Pallas kernels for 4% -> 2%
where the time goes in v11:
time: 106 us; the launch traced here: 105 us
  starting transfers between devices  47.5 us (45%)
  waiting for transfers between devices  31.2 us (29%)
  blocking collectives  15.8 us (15%)
  Pallas kernels  8.5 us (8%)
  other arithmetic  1.3 us (1%)
    all_to_all x1, starting transfers between devices, per_device(): lax.all_to_all(zsend, ('zp', 'zl'), 0, 0, axis_index_groups=GROUPS, tiled...  14.6 us
    all_gather x1, blocking collectives, per_device(): grp = lax.all_gather(own, 'y', axis=0, tiled=False)  13.9 us
    ppermute x3, starting transfers between devices, per_device(): lax.ppermute(kv[d], 'y', [(i, (i + d) % NY) for i in range(NY)])  11.9 us
    ppermute x3, waiting for transfers between devices, per_device(): xts.append(lax.ppermute(xt, 'x', [(i, (i + d) % NX) for i in range(NX)]))  11.2 us
    all_to_all x1, waiting for transfers between devices, per_device(): lax.all_to_all(zsend, ('zp', 'zl'), 0, 0, axis_index_groups=GROUPS, tiled...  8.62 us
    ppermute x1, waiting for transfers between devices, per_device(): relayed = lax.ppermute(recv, 'zl', [(0, 1), (1, 0)])  8.58 us
    ppermute x3, starting transfers between devices, per_device(): xts.append(lax.ppermute(xt, 'x', [(i, (i + d) % NX) for i in range(NX)]))  7.6 us
    all_to_all x1, starting transfers between devices, per_device(): back = lax.all_to_all(zs, ('zp', 'zl'), 0, 0, tiled=True)  6.63 us
  transfers between devices with their start and end apart: 10, of which 6 were waited for; matrix products, arithmetic and copies ran while one was open for 1% of the time, Pallas kernels for 2%

profile of v11, /device:TPU:6, one launch (start us, length us, event | category | flops | bytes accessed | tf_op | source)
XLA Modules:
  0.0 105.0 jit_solution(1114475390994766763)
XLA Ops:
  0.6 2.0 %shard_map.111 = (bf16[8,264,128]{2,1,0:T(8,128)(2,1)}, bf16[784,128]{1,0:T(8,128)(2,1)S(1)}) custom-call(bf16[128,128]{1,0:T(8,128)(2,1)} %q.1, bf16[128,128]{1,0:T(8,128)(2,1)} %k.1, bf16[128,128]{1,0:T(8,128)(2,1)} %v.1, f32[1,128]{1,0:T(1,128)} %bitcast.11, f32[1,128]{1,0:T(1,128)} %bitcast.12, bf16[128,128]{1,0:T(8,128)(2,1)} %o.1, ...), custom_call_target="tpu_custom_call" | custom-call | tf_op jit(solution)/shard_map/pallas_call | solution.py:225
  2.7 14.6 %all-to-all-start = ((bf16[8,264,128]{2,1,0:T(8,128)(2,1)}), bf16[8,264,128]{2,1,0:T(8,128)(2,1)S(1)}, u32[]{:S(2)}, u32[]{:S(2)}) async-start(bf16[8,264,128]{2,1,0:T(8,128)(2,1)} %get-tuple-element.24), calls=%async_computation | async-start | bytes 1081344 | tf_op jit(solution)/shard_map/all_to_all | solution.py:226
  17.3 13.9 %all-gather = bf16[3136,128]{1,0:T(8,128)(2,1)S(1)} all-gather(bf16[784,128]{1,0:T(8,128)(2,1)S(1)} %get-tuple-element.25), channel_id=2, replica_groups=mesh['zp'=8,'zl'=2,'y'=4,'x'=4,'c'=2] {'y'}, dimensions={0}, use_global_device_ids=true | all-gather | bytes 1003520 | tf_op jit(solution)/shard_map/all_gather | solution.py:227
  31.2 1.9 %all-gather.1 = bf16[8,64,128]{2,1,0:T(8,128)(2,1)S(1)} all-gather(bf16[4,64,128]{2,1,0:T(8,128)(2,1)S(1)} %pad_maximum_fusion), channel_id=3, replica_groups=mesh['zp'=8,'zl'=2,'y'=4,'x'=4,'c'=2] {'c'}, dimensions={0}, use_global_device_ids=true | all-gather | bytes 196608 | tf_op jit(solution)/shard_map/all_gather | solution.py:229
  33.1 2.4 %collective-permute-start = (bf16[2,4,64,128]{3,2,1,0:T(8,128)(2,1)S(1)}, bf16[2,4,64,128]{3,2,1,0:T(8,128)(2,1)S(1)}, u32[]{:S(2)}, u32[]{:S(2)}) collective-permute-start(bf16[2,4,64,128]{3,2,1,0:T(8,128)(2,1)S(1)} %bitcast.7), channel_id=1, source_target_pairs={{0,2},{2,4},{4,6},{6,0},{1,3},{3,5},{5,7},{7,1},{8,10},{10,12},{12... | collective-permute-start | bytes 393224 | tf_op jit(solution)/shard_map/ppermute | solution.py:232
  35.5 5.1 %collective-permute-done.rest_1_ = bf16[2,4,64,128]{3,2,1,0:T(8,128)(2,1)S(1)} collective-permute-done((bf16[2,4,64,128]{3,2,1,0:T(8,128)(2,1)S(1)}, bf16[2,4,64,128]{3,2,1,0:T(8,128)(2,1)S(1)}, u32[]{:S(2)}, u32[]{:S(2)}) %collective-permute-start) | collective-permute-done | bytes 131104 | tf_op jit(solution)/shard_map/ppermute | solution.py:232
  40.5 8.6 %all-to-all-done.recv = bf16[8,264,128]{2,1,0:T(8,128)(2,1)S(1)} async-done(((bf16[8,264,128]{2,1,0:T(8,128)(2,1)}), bf16[8,264,128]{2,1,0:T(8,128)(2,1)S(1)}, u32[]{:S(2)}, u32[]{:S(2)}) %all-to-all-start) | async-done | bytes 540704 | tf_op jit(solution)/shard_map/all_to_all | solution.py:226
  49.2 2.3 %collective-permute-start.1 = (bf16[8,264,128]{2,1,0:T(8,128)(2,1)S(1)}, bf16[8,264,128]{2,1,0:T(8,128)(2,1)S(1)}, u32[]{:S(2)}, u32[]{:S(2)}) collective-permute-start(bf16[8,264,128]{2,1,0:T(8,128)(2,1)S(1)} %all-to-all-done.recv), channel_id=1, source_target_pairs={{0,32},{32,0},{1,33},{33,1},{2,34},{34,2},{3,35},{35,3},{4,36},{36... | collective-permute-start | bytes 1622024 | tf_op jit(solution)/shard_map/ppermute | solution.py:234
  51.5 2.5 %shard_map.112 = (f32[512,128]{1,0:T(8,128)S(1)}, f32[512,128]{1,0:T(8,128)S(1)}, f32[512,128]{1,0:T(8,128)S(1)}) custom-call(bf16[8,264,128]{2,1,0:T(8,128)(2,1)S(1)} %all-to-all-done.recv, bf16[4,784,128]{2,1,0:T(8,128)(2,1)S(1)} %bitcast.5), custom_call_target="tpu_custom_call" | custom-call | tf_op jit(solution)/shard_map/pallas_call | solution.py:236
  53.9 8.6 %collective-permute-done.1.recv = bf16[8,264,128]{2,1,0:T(8,128)(2,1)S(1)} collective-permute-done((bf16[8,264,128]{2,1,0:T(8,128)(2,1)S(1)}, bf16[8,264,128]{2,1,0:T(8,128)(2,1)S(1)}, u32[]{:S(2)}, u32[]{:S(2)}) %collective-permute-start.1) | collective-permute-done | bytes 540704 | tf_op jit(solution)/shard_map/ppermute | solution.py:234
  62.5 2.9 %shard_map.113 = (bf16[4,512,128]{2,1,0:T(8,128)(2,1)}, bf16[256,128]{1,0:T(8,128)(2,1)S(1)}, bf16[256,128]{1,0:T(8,128)(2,1)S(1)}, bf16[256,128]{1,0:T(8,128)(2,1)S(1)}, bf16[256,128]{1,0:T(8,128)(2,1)S(1)}) custom-call(bf16[8,264,128]{2,1,0:T(8,128)(2,1)S(1)} %collective-permute-done.1.recv, bf16[4,784,128]{2,1,0:T(8,128)(2,1)S(1)} %bitcast.6, ...), custom_call_target="tpu_custom_call" | custom-call | tf_op jit(solution)/shard_map/pallas_call | solution.py:243
  65.5 4.5 %all-to-all-start.1 = ((bf16[4,512,128]{2,1,0:T(8,128)(2,1)}), bf16[4,512,128]{2,1,0:T(8,128)(2,1)S(1)}, u32[]{:S(2)}, u32[]{:S(2)}) async-start(bf16[4,512,128]{2,1,0:T(8,128)(2,1)} %get-tuple-element.30), calls=%async_computation.1 | async-start | bytes 1048576 | tf_op jit(solution)/shard_map/all_to_all | solution.py:244
  69.9 3.3 %collective-permute-start.2 = (bf16[2,4,64,128]{3,2,1,0:T(8,128)(2,1)S(1)}, bf16[2,4,64,128]{3,2,1,0:T(8,128)(2,1)S(1)}, u32[]{:S(2)}, u32[]{:S(2)}) collective-permute-start(bf16[2,4,64,128]{3,2,1,0:T(8,128)(2,1)S(1)} %bitcast.8), channel_id=1, source_target_pairs={{0,4},{2,6},{4,0},{6,2},{1,5},{3,7},{5,1},{7,3},{8,12},{10,14},{12... | collective-permute-start | bytes 393224 | tf_op jit(solution)/shard_map/ppermute | solution.py:232
  73.2 1.9 %collective-permute-start.3 = (bf16[2,4,64,128]{3,2,1,0:T(8,128)(2,1)S(1)}, bf16[2,4,64,128]{3,2,1,0:T(8,128)(2,1)S(1)}, u32[]{:S(2)}, u32[]{:S(2)}) collective-permute-start(bf16[2,4,64,128]{3,2,1,0:T(8,128)(2,1)S(1)} %bitcast.9), channel_id=1, source_target_pairs={{0,6},{2,0},{4,2},{6,4},{1,7},{3,1},{5,3},{7,5},{8,14},{10,8},{12,... | collective-permute-start | bytes 393224 | tf_op jit(solution)/shard_map/ppermute | solution.py:232
  75.2 3.1 %collective-permute-done.2.rest_2_ = bf16[2,4,64,128]{3,2,1,0:T(8,128)(2,1)S(1)} collective-permute-done((bf16[2,4,64,128]{3,2,1,0:T(8,128)(2,1)S(1)}, bf16[2,4,64,128]{3,2,1,0:T(8,128)(2,1)S(1)}, u32[]{:S(2)}, u32[]{:S(2)}) %collective-permute-start.2) | collective-permute-done | bytes 131104 | tf_op jit(solution)/shard_map/ppermute | solution.py:232
  78.3 3.0 %collective-permute-done.3.rest_3_ = bf16[2,4,64,128]{3,2,1,0:T(8,128)(2,1)S(1)} collective-permute-done((bf16[2,4,64,128]{3,2,1,0:T(8,128)(2,1)S(1)}, bf16[2,4,64,128]{3,2,1,0:T(8,128)(2,1)S(1)}, u32[]{:S(2)}, u32[]{:S(2)}) %collective-permute-start.3) | collective-permute-done | bytes 131104 | tf_op jit(solution)/shard_map/ppermute | solution.py:232
  81.3 0.0 all-to-all-done.1.sums
  81.3 1.0 shard_map.114
  82.4 6.6 %all-to-all-start.2 = ((bf16[16,32,128]{2,1,0:T(8,128)(2,1)}), bf16[16,32,128]{2,1,0:T(8,128)(2,1)S(1)}, u32[]{:S(2)}, u32[]{:S(2)}) async-start(bf16[16,32,128]{2,1,0:T(8,128)(2,1)} %get-tuple-element.43), calls=%async_computation.2 | async-start | bytes 262144 | tf_op jit(solution)/shard_map/all_to_all | solution.py:249
  89.0 3.9 %collective-permute-start.4 = (bf16[256,128]{1,0:T(8,128)(2,1)S(1)}, bf16[256,128]{1,0:T(8,128)(2,1)S(1)}, u32[]{:S(2)}, u32[]{:S(2)}) collective-permute-start(bf16[256,128]{1,0:T(8,128)(2,1)S(1)} %get-tuple-element.40), channel_id=1, source_target_pairs={{0,8},{8,16},{16,24},{24,0},{1,9},{9,17},{17,25},{25,1},{2,10},{10... | collective-permute-start | bytes 196616 | tf_op jit(solution)/shard_map/ppermute | solution.py:252
  92.9 4.6 %collective-permute-start.5 = (bf16[256,128]{1,0:T(8,128)(2,1)S(1)}, bf16[256,128]{1,0:T(8,128)(2,1)S(1)}, u32[]{:S(2)}, u32[]{:S(2)}) collective-permute-start(bf16[256,128]{1,0:T(8,128)(2,1)S(1)} %get-tuple-element.41), channel_id=1, source_target_pairs={{0,16},{8,24},{16,0},{24,8},{1,17},{9,25},{17,1},{25,9},{2,18},{10... | collective-permute-start | bytes 196616 | tf_op jit(solution)/shard_map/ppermute | solution.py:252
  97.5 3.4 %collective-permute-start.6 = (bf16[256,128]{1,0:T(8,128)(2,1)S(1)}, bf16[256,128]{1,0:T(8,128)(2,1)S(1)}, u32[]{:S(2)}, u32[]{:S(2)}) collective-permute-start(bf16[256,128]{1,0:T(8,128)(2,1)S(1)} %get-tuple-element.42), channel_id=1, source_target_pairs={{0,24},{8,0},{16,8},{24,16},{1,25},{9,1},{17,9},{25,17},{2,26},{10... | collective-permute-start | bytes 196616 | tf_op jit(solution)/shard_map/ppermute | solution.py:252
  100.9 0.0 collective-permute-done.4
  100.9 0.0 collective-permute-done.5
  100.9 2.8 %collective-permute-done.6 = bf16[256,128]{1,0:T(8,128)(2,1)S(1)} collective-permute-done((bf16[256,128]{1,0:T(8,128)(2,1)S(1)}, bf16[256,128]{1,0:T(8,128)(2,1)S(1)}, u32[]{:S(2)}, u32[]{:S(2)}) %collective-permute-start.6) | collective-permute-done | bytes 65568 | tf_op jit(solution)/shard_map/ppermute | solution.py:252
  103.7 0.7 add_convert_fusion
  104.3 0.0 all-to-all-done.2
  104.3 0.6 convert_reduce_fusion
  (2 shorter events, 0.0 us)
Async XLA Ops:
  2.7 46.5 %all-to-all-start = ((bf16[8,264,128]{2,1,0:T(8,128)(2,1)}), bf16[8,264,128]{2,1,0:T(8,128)(2,1)S(1)}, u32[]{:S(2)}, u32[]{:S(2)}) async-start(bf16[8,264,128]{2,1,0:T(8,128)(2,1)} %get-tuple-element.24), calls=%async_computation | async-start | bytes 1081344 | tf_op jit(solution)/shard_map/all_to_all | solution.py:226
  33.1 7.4 %collective-permute-start = (bf16[2,4,64,128]{3,2,1,0:T(8,128)(2,1)S(1)}, bf16[2,4,64,128]{3,2,1,0:T(8,128)(2,1)S(1)}, u32[]{:S(2)}, u32[]{:S(2)}) collective-permute-start(bf16[2,4,64,128]{3,2,1,0:T(8,128)(2,1)S(1)} %bitcast.7), channel_id=1, source_target_pairs={{0,2},{2,4},{4,6},{6,0},{1,3},{3,5},{5,7},{7,1},{8,10},{10,12},{12... | collective-permute-start | bytes 393224 | tf_op jit(solution)/shard_map/ppermute | solution.py:232
  49.2 13.4 %collective-permute-start.1 = (bf16[8,264,128]{2,1,0:T(8,128)(2,1)S(1)}, bf16[8,264,128]{2,1,0:T(8,128)(2,1)S(1)}, u32[]{:S(2)}, u32[]{:S(2)}) collective-permute-start(bf16[8,264,128]{2,1,0:T(8,128)(2,1)S(1)} %all-to-all-done.recv), channel_id=1, source_target_pairs={{0,32},{32,0},{1,33},{33,1},{2,34},{34,2},{3,35},{35,3},{4,36},{36... | collective-permute-start | bytes 1622024 | tf_op jit(solution)/shard_map/ppermute | solution.py:234
  65.5 15.9 %all-to-all-start.1 = ((bf16[4,512,128]{2,1,0:T(8,128)(2,1)}), bf16[4,512,128]{2,1,0:T(8,128)(2,1)S(1)}, u32[]{:S(2)}, u32[]{:S(2)}) async-start(bf16[4,512,128]{2,1,0:T(8,128)(2,1)} %get-tuple-element.30), calls=%async_computation.1 | async-start | bytes 1048576 | tf_op jit(solution)/shard_map/all_to_all | solution.py:244
  69.9 8.4 %collective-permute-start.2 = (bf16[2,4,64,128]{3,2,1,0:T(8,128)(2,1)S(1)}, bf16[2,4,64,128]{3,2,1,0:T(8,128)(2,1)S(1)}, u32[]{:S(2)}, u32[]{:S(2)}) collective-permute-start(bf16[2,4,64,128]{3,2,1,0:T(8,128)(2,1)S(1)} %bitcast.8), channel_id=1, source_target_pairs={{0,4},{2,6},{4,0},{6,2},{1,5},{3,7},{5,1},{7,3},{8,12},{10,14},{12... | collective-permute-start | bytes 393224 | tf_op jit(solution)/shard_map/ppermute | solution.py:232
  73.2 8.1 %collective-permute-start.3 = (bf16[2,4,64,128]{3,2,1,0:T(8,128)(2,1)S(1)}, bf16[2,4,64,128]{3,2,1,0:T(8,128)(2,1)S(1)}, u32[]{:S(2)}, u32[]{:S(2)}) collective-permute-start(bf16[2,4,64,128]{3,2,1,0:T(8,128)(2,1)S(1)} %bitcast.9), channel_id=1, source_target_pairs={{0,6},{2,0},{4,2},{6,4},{1,7},{3,1},{5,3},{7,5},{8,14},{10,8},{12,... | collective-permute-start | bytes 393224 | tf_op jit(solution)/shard_map/ppermute | solution.py:232
  82.4 22.0 %all-to-all-start.2 = ((bf16[16,32,128]{2,1,0:T(8,128)(2,1)}), bf16[16,32,128]{2,1,0:T(8,128)(2,1)S(1)}, u32[]{:S(2)}, u32[]{:S(2)}) async-start(bf16[16,32,128]{2,1,0:T(8,128)(2,1)} %get-tuple-element.43), calls=%async_computation.2 | async-start | bytes 262144 | tf_op jit(solution)/shard_map/all_to_all | solution.py:249
  89.0 11.9 %collective-permute-start.4 = (bf16[256,128]{1,0:T(8,128)(2,1)S(1)}, bf16[256,128]{1,0:T(8,128)(2,1)S(1)}, u32[]{:S(2)}, u32[]{:S(2)}) collective-permute-start(bf16[256,128]{1,0:T(8,128)(2,1)S(1)} %get-tuple-element.40), channel_id=1, source_target_pairs={{0,8},{8,16},{16,24},{24,0},{1,9},{9,17},{17,25},{25,1},{2,10},{10... | collective-permute-start | bytes 196616 | tf_op jit(solution)/shard_map/ppermute | solution.py:252
  92.9 8.0 %collective-permute-start.5 = (bf16[256,128]{1,0:T(8,128)(2,1)S(1)}, bf16[256,128]{1,0:T(8,128)(2,1)S(1)}, u32[]{:S(2)}, u32[]{:S(2)}) collective-permute-start(bf16[256,128]{1,0:T(8,128)(2,1)S(1)} %get-tuple-element.41), channel_id=1, source_target_pairs={{0,16},{8,24},{16,0},{24,8},{1,17},{9,25},{17,1},{25,9},{2,18},{10... | collective-permute-start | bytes 196616 | tf_op jit(solution)/shard_map/ppermute | solution.py:252
  97.5 6.2 %collective-permute-start.6 = (bf16[256,128]{1,0:T(8,128)(2,1)S(1)}, bf16[256,128]{1,0:T(8,128)(2,1)S(1)}, u32[]{:S(2)}, u32[]{:S(2)}) collective-permute-start(bf16[256,128]{1,0:T(8,128)(2,1)S(1)} %get-tuple-element.42), channel_id=1, source_target_pairs={{0,24},{8,0},{16,8},{24,16},{1,25},{9,1},{17,9},{25,17},{2,26},{10... | collective-permute-start | bytes 196616 | tf_op jit(solution)/shard_map/ppermute | solution.py:252

commit v12 on v11

--- a/solution.py
+++ b/solution.py
@@ -134,15 +134,20 @@
         dv[...] += more[1]
 
     def over(step, start, end):
-        twos = (end - start) // 2
-
-        def two(i, carry):
-            step(start + 2 * i, 2)
+        fours = (end - start) // 4
+
+        def four(i, carry):
+            step(start + 4 * i, 4)
             return carry
 
-        lax.fori_loop(0, twos, two, 0)
-
-        @pl.when(start + 2 * twos < end)
+        lax.fori_loop(0, fours, four, 0)
+        left = (end - start) % 4
+
+        @pl.when(left >= 2)
+        def _():
+            step(start + 4 * fours, 2)
+
+        @pl.when(left % 2 == 1)
         def _():
             step(end - 1, 1)
 
@@ -230,7 +235,7 @@
     xts = [xt]
     for d in range(1, NX):
         xts.append(lax.ppermute(xt, "x", [(i, (i + d) % NX) for i in range(NX)]))
-    recv, *xts[:2] = lax.optimization_barrier((recv, *xts[:2]))
+    recv, xts[0] = lax.optimization_barrier((recv, xts[0]))
     relayed = lax.ppermute(recv, "zl", [(0, 1), (1, 0)])
     block = (NY * T, H)
     sums = call(first_body, [(block, f32)] * 3, [], 2)(in_vmem(recv), in_vmem(grp))

time: 106 us -> 109 us (1.028)
  waiting for transfers between devices: 31.2 us -> 33.6 us
    all_to_all x1, waiting for transfers between devices: 8.62 us -> 16.1 us  [per_device(): lax.all_to_all(zsend, ('zp', 'zl'), 0, 0, axis_index_groups=GROUPS, tiled...]
    ppermute x3, waiting for transfers between devices: 11.2 us -> 6.14 us  [per_device(): xts.append(lax.ppermute(xt, 'x', [(i, (i + d) % NX) for i in range(NX)]))]
  transfers between devices with their start and end apart: 10 -> 10, of which waited for: 6 -> 5; matrix products, arithmetic and copies ran while one was open for 1% -> 1% of each run, Pallas kernels for 2% -> 2%
where the time goes in v12:
time: 109 us; the launch traced here: 108 us
  starting transfers between devices  48.4 us (44%)
  waiting for transfers between devices  33.6 us (31%)
  blocking collectives  15.8 us (14%)
  Pallas kernels  8.17 us (7%)
  other arithmetic  1.3 us (1%)
    all_to_all x1, waiting for transfers between devices, per_device(): lax.all_to_all(zsend, ('zp', 'zl'), 0, 0, axis_index_groups=GROUPS, tiled...  16.1 us
    all_to_all x1, starting transfers between devices, per_device(): lax.all_to_all(zsend, ('zp', 'zl'), 0, 0, axis_index_groups=GROUPS, tiled...  14.6 us
    all_gather x1, blocking collectives, per_device(): grp = lax.all_gather(own, 'y', axis=0, tiled=False)  13.9 us
    ppermute x3, starting transfers between devices, per_device(): lax.ppermute(kv[d], 'y', [(i, (i + d) % NY) for i in range(NY)])  11.9 us
    ppermute x1, waiting for transfers between devices, per_device(): relayed = lax.ppermute(recv, 'zl', [(0, 1), (1, 0)])  8.68 us
    ppermute x3, starting transfers between devices, per_device(): xts.append(lax.ppermute(xt, 'x', [(i, (i + d) % NX) for i in range(NX)]))  8.62 us
    all_to_all x1, starting transfers between devices, per_device(): back = lax.all_to_all(zs, ('zp', 'zl'), 0, 0, tiled=True)  6.46 us
    ppermute x3, waiting for transfers between devices, per_device(): xts.append(lax.ppermute(xt, 'x', [(i, (i + d) % NX) for i in range(NX)]))  6.14 us
  transfers between devices with their start and end apart: 10, of which 5 were waited for; matrix products, arithmetic and copies ran while one was open for 1% of the time, Pallas kernels for 2%

profile of v12, /device:TPU:6, one launch (start us, length us, event | category | flops | bytes accessed | tf_op | source)
XLA Modules:
  0.0 108.0 jit_solution(12479195656215667991)
XLA Ops:
  0.6 2.0 %shard_map.111 = (bf16[8,264,128]{2,1,0:T(8,128)(2,1)}, bf16[784,128]{1,0:T(8,128)(2,1)S(1)}) custom-call(bf16[128,128]{1,0:T(8,128)(2,1)} %q.1, bf16[128,128]{1,0:T(8,128)(2,1)} %k.1, bf16[128,128]{1,0:T(8,128)(2,1)} %v.1, f32[1,128]{1,0:T(1,128)} %bitcast.11, f32[1,128]{1,0:T(1,128)} %bitcast.12, bf16[128,128]{1,0:T(8,128)(2,1)} %o.1, ...), custom_call_target="tpu_custom_call" | custom-call | tf_op jit(solution)/shard_map/pallas_call | solution.py:230
  2.7 14.6 %all-to-all-start = ((bf16[8,264,128]{2,1,0:T(8,128)(2,1)}), bf16[8,264,128]{2,1,0:T(8,128)(2,1)S(1)}, u32[]{:S(2)}, u32[]{:S(2)}) async-start(bf16[8,264,128]{2,1,0:T(8,128)(2,1)} %get-tuple-element.23), calls=%async_computation | async-start | bytes 1081344 | tf_op jit(solution)/shard_map/all_to_all | solution.py:231
  17.3 13.9 %all-gather = bf16[3136,128]{1,0:T(8,128)(2,1)S(1)} all-gather(bf16[784,128]{1,0:T(8,128)(2,1)S(1)} %get-tuple-element.24), channel_id=2, replica_groups=mesh['zp'=8,'zl'=2,'y'=4,'x'=4,'c'=2] {'y'}, dimensions={0}, use_global_device_ids=true | all-gather | bytes 1003520 | tf_op jit(solution)/shard_map/all_gather | solution.py:232
  31.2 1.9 %all-gather.1 = bf16[8,64,128]{2,1,0:T(8,128)(2,1)S(1)} all-gather(bf16[4,64,128]{2,1,0:T(8,128)(2,1)S(1)} %pad_maximum_fusion), channel_id=3, replica_groups=mesh['zp'=8,'zl'=2,'y'=4,'x'=4,'c'=2] {'c'}, dimensions={0}, use_global_device_ids=true | all-gather | bytes 196608 | tf_op jit(solution)/shard_map/all_gather | solution.py:234
  33.1 16.1 %all-to-all-done.recv = bf16[8,264,128]{2,1,0:T(8,128)(2,1)S(1)} async-done(((bf16[8,264,128]{2,1,0:T(8,128)(2,1)}), bf16[8,264,128]{2,1,0:T(8,128)(2,1)S(1)}, u32[]{:S(2)}, u32[]{:S(2)}) %all-to-all-start) | async-done | bytes 540704 | tf_op jit(solution)/shard_map/all_to_all | solution.py:231
  49.2 2.3 %collective-permute-start = (bf16[8,264,128]{2,1,0:T(8,128)(2,1)S(1)}, bf16[8,264,128]{2,1,0:T(8,128)(2,1)S(1)}, u32[]{:S(2)}, u32[]{:S(2)}) collective-permute-start(bf16[8,264,128]{2,1,0:T(8,128)(2,1)S(1)} %all-to-all-done.recv), channel_id=1, source_target_pairs={{0,32},{32,0},{1,33},{33,1},{2,34},{34,2},{3,35},{35,3},{4,36},{36... | collective-permute-start | bytes 1622024 | tf_op jit(solution)/shard_map/ppermute | solution.py:239
  51.5 2.4 %shard_map.112 = (f32[512,128]{1,0:T(8,128)S(1)}, f32[512,128]{1,0:T(8,128)S(1)}, f32[512,128]{1,0:T(8,128)S(1)}) custom-call(bf16[8,264,128]{2,1,0:T(8,128)(2,1)S(1)} %all-to-all-done.recv, bf16[4,784,128]{2,1,0:T(8,128)(2,1)S(1)} %bitcast.5), custom_call_target="tpu_custom_call" | custom-call | tf_op jit(solution)/shard_map/pallas_call | solution.py:241
  53.8 8.7 %collective-permute-done.recv = bf16[8,264,128]{2,1,0:T(8,128)(2,1)S(1)} collective-permute-done((bf16[8,264,128]{2,1,0:T(8,128)(2,1)S(1)}, bf16[8,264,128]{2,1,0:T(8,128)(2,1)S(1)}, u32[]{:S(2)}, u32[]{:S(2)}) %collective-permute-start) | collective-permute-done | bytes 540704 | tf_op jit(solution)/shard_map/ppermute | solution.py:239
  62.5 2.7 %shard_map.113 = (bf16[4,512,128]{2,1,0:T(8,128)(2,1)}, bf16[256,128]{1,0:T(8,128)(2,1)S(1)}, bf16[256,128]{1,0:T(8,128)(2,1)S(1)}, bf16[256,128]{1,0:T(8,128)(2,1)S(1)}, bf16[256,128]{1,0:T(8,128)(2,1)S(1)}) custom-call(bf16[8,264,128]{2,1,0:T(8,128)(2,1)S(1)} %collective-permute-done.recv, bf16[4,784,128]{2,1,0:T(8,128)(2,1)S(1)} %bitcast.6, ...), custom_call_target="tpu_custom_call" | custom-call | tf_op jit(solution)/shard_map/pallas_call | solution.py:248
  65.3 4.5 %all-to-all-start.1 = ((bf16[4,512,128]{2,1,0:T(8,128)(2,1)}), bf16[4,512,128]{2,1,0:T(8,128)(2,1)S(1)}, u32[]{:S(2)}, u32[]{:S(2)}) async-start(bf16[4,512,128]{2,1,0:T(8,128)(2,1)} %get-tuple-element.29), calls=%async_computation.1 | async-start | bytes 1048576 | tf_op jit(solution)/shard_map/all_to_all | solution.py:249
  69.7 2.4 %collective-permute-start.1 = (bf16[2,4,64,128]{3,2,1,0:T(8,128)(2,1)S(1)}, bf16[2,4,64,128]{3,2,1,0:T(8,128)(2,1)S(1)}, u32[]{:S(2)}, u32[]{:S(2)}) collective-permute-start(bf16[2,4,64,128]{3,2,1,0:T(8,128)(2,1)S(1)} %bitcast.7), channel_id=1, source_target_pairs={{0,2},{2,4},{4,6},{6,0},{1,3},{3,5},{5,7},{7,1},{8,10},{10,12},{12... | collective-permute-start | bytes 393224 | tf_op jit(solution)/shard_map/ppermute | solution.py:237
  72.1 4.3 %collective-permute-start.2 = (bf16[2,4,64,128]{3,2,1,0:T(8,128)(2,1)S(1)}, bf16[2,4,64,128]{3,2,1,0:T(8,128)(2,1)S(1)}, u32[]{:S(2)}, u32[]{:S(2)}) collective-permute-start(bf16[2,4,64,128]{3,2,1,0:T(8,128)(2,1)S(1)} %bitcast.8), channel_id=1, source_target_pairs={{0,4},{2,6},{4,0},{6,2},{1,5},{3,7},{5,1},{7,3},{8,12},{10,14},{12... | collective-permute-start | bytes 393224 | tf_op jit(solution)/shard_map/ppermute | solution.py:237
  76.4 1.9 %collective-permute-start.3 = (bf16[2,4,64,128]{3,2,1,0:T(8,128)(2,1)S(1)}, bf16[2,4,64,128]{3,2,1,0:T(8,128)(2,1)S(1)}, u32[]{:S(2)}, u32[]{:S(2)}) collective-permute-start(bf16[2,4,64,128]{3,2,1,0:T(8,128)(2,1)S(1)} %bitcast.9), channel_id=1, source_target_pairs={{0,6},{2,0},{4,2},{6,4},{1,7},{3,1},{5,3},{7,5},{8,14},{10,8},{12,... | collective-permute-start | bytes 393224 | tf_op jit(solution)/shard_map/ppermute | solution.py:237
  78.4 0.0 collective-permute-done.1.rest_1_
  78.4 2.2 %collective-permute-done.2.rest_2_ = bf16[2,4,64,128]{3,2,1,0:T(8,128)(2,1)S(1)} collective-permute-done((bf16[2,4,64,128]{3,2,1,0:T(8,128)(2,1)S(1)}, bf16[2,4,64,128]{3,2,1,0:T(8,128)(2,1)S(1)}, u32[]{:S(2)}, u32[]{:S(2)}) %collective-permute-start.2) | collective-permute-done | bytes 131104 | tf_op jit(solution)/shard_map/ppermute | solution.py:237
  80.6 3.9 %collective-permute-done.3.rest_3_ = bf16[2,4,64,128]{3,2,1,0:T(8,128)(2,1)S(1)} collective-permute-done((bf16[2,4,64,128]{3,2,1,0:T(8,128)(2,1)S(1)}, bf16[2,4,64,128]{3,2,1,0:T(8,128)(2,1)S(1)}, u32[]{:S(2)}, u32[]{:S(2)}) %collective-permute-start.3) | collective-permute-done | bytes 131104 | tf_op jit(solution)/shard_map/ppermute | solution.py:237
  84.5 0.0 all-to-all-done.1.sums
  84.5 1.0 shard_map.114
  85.5 6.5 %all-to-all-start.2 = ((bf16[16,32,128]{2,1,0:T(8,128)(2,1)}), bf16[16,32,128]{2,1,0:T(8,128)(2,1)S(1)}, u32[]{:S(2)}, u32[]{:S(2)}) async-start(bf16[16,32,128]{2,1,0:T(8,128)(2,1)} %get-tuple-element.41), calls=%async_computation.2 | async-start | bytes 262144 | tf_op jit(solution)/shard_map/all_to_all | solution.py:254
  92.0 3.9 %collective-permute-start.4 = (bf16[256,128]{1,0:T(8,128)(2,1)S(1)}, bf16[256,128]{1,0:T(8,128)(2,1)S(1)}, u32[]{:S(2)}, u32[]{:S(2)}) collective-permute-start(bf16[256,128]{1,0:T(8,128)(2,1)S(1)} %get-tuple-element.38), channel_id=1, source_target_pairs={{0,8},{8,16},{16,24},{24,0},{1,9},{9,17},{17,25},{25,1},{2,10},{10... | collective-permute-start | bytes 196616 | tf_op jit(solution)/shard_map/ppermute | solution.py:257
  96.0 4.6 %collective-permute-start.5 = (bf16[256,128]{1,0:T(8,128)(2,1)S(1)}, bf16[256,128]{1,0:T(8,128)(2,1)S(1)}, u32[]{:S(2)}, u32[]{:S(2)}) collective-permute-start(bf16[256,128]{1,0:T(8,128)(2,1)S(1)} %get-tuple-element.39), channel_id=1, source_target_pairs={{0,16},{8,24},{16,0},{24,8},{1,17},{9,25},{17,1},{25,9},{2,18},{10... | collective-permute-start | bytes 196616 | tf_op jit(solution)/shard_map/ppermute | solution.py:257
  100.5 3.4 %collective-permute-start.6 = (bf16[256,128]{1,0:T(8,128)(2,1)S(1)}, bf16[256,128]{1,0:T(8,128)(2,1)S(1)}, u32[]{:S(2)}, u32[]{:S(2)}) collective-permute-start(bf16[256,128]{1,0:T(8,128)(2,1)S(1)} %get-tuple-element.40), channel_id=1, source_target_pairs={{0,24},{8,0},{16,8},{24,16},{1,25},{9,1},{17,9},{25,17},{2,26},{10... | collective-permute-start | bytes 196616 | tf_op jit(solution)/shard_map/ppermute | solution.py:257
  103.9 0.0 collective-permute-done.4
  103.9 0.0 collective-permute-done.5
  103.9 2.8 %collective-permute-done.6 = bf16[256,128]{1,0:T(8,128)(2,1)S(1)} collective-permute-done((bf16[256,128]{1,0:T(8,128)(2,1)S(1)}, bf16[256,128]{1,0:T(8,128)(2,1)S(1)}, u32[]{:S(2)}, u32[]{:S(2)}) %collective-permute-start.6) | collective-permute-done | bytes 65568 | tf_op jit(solution)/shard_map/ppermute | solution.py:257
  106.7 0.7 add_convert_fusion
  107.4 0.0 all-to-all-done.2
  107.4 0.6 convert_reduce_fusion
  (2 shorter events, 0.0 us)
Async XLA Ops:
  2.7 46.5 %all-to-all-start = ((bf16[8,264,128]{2,1,0:T(8,128)(2,1)}), bf16[8,264,128]{2,1,0:T(8,128)(2,1)S(1)}, u32[]{:S(2)}, u32[]{:S(2)}) async-start(bf16[8,264,128]{2,1,0:T(8,128)(2,1)} %get-tuple-element.23), calls=%async_computation | async-start | bytes 1081344 | tf_op jit(solution)/shard_map/all_to_all | solution.py:231
  49.2 13.4 %collective-permute-start = (bf16[8,264,128]{2,1,0:T(8,128)(2,1)S(1)}, bf16[8,264,128]{2,1,0:T(8,128)(2,1)S(1)}, u32[]{:S(2)}, u32[]{:S(2)}) collective-permute-start(bf16[8,264,128]{2,1,0:T(8,128)(2,1)S(1)} %all-to-all-done.recv), channel_id=1, source_target_pairs={{0,32},{32,0},{1,33},{33,1},{2,34},{34,2},{3,35},{35,3},{4,36},{36... | collective-permute-start | bytes 1622024 | tf_op jit(solution)/shard_map/ppermute | solution.py:239
  65.3 19.3 %all-to-all-start.1 = ((bf16[4,512,128]{2,1,0:T(8,128)(2,1)}), bf16[4,512,128]{2,1,0:T(8,128)(2,1)S(1)}, u32[]{:S(2)}, u32[]{:S(2)}) async-start(bf16[4,512,128]{2,1,0:T(8,128)(2,1)} %get-tuple-element.29), calls=%async_computation.1 | async-start | bytes 1048576 | tf_op jit(solution)/shard_map/all_to_all | solution.py:249
  69.7 8.6 %collective-permute-start.1 = (bf16[2,4,64,128]{3,2,1,0:T(8,128)(2,1)S(1)}, bf16[2,4,64,128]{3,2,1,0:T(8,128)(2,1)S(1)}, u32[]{:S(2)}, u32[]{:S(2)}) collective-permute-start(bf16[2,4,64,128]{3,2,1,0:T(8,128)(2,1)S(1)} %bitcast.7), channel_id=1, source_target_pairs={{0,2},{2,4},{4,6},{6,0},{1,3},{3,5},{5,7},{7,1},{8,10},{10,12},{12... | collective-permute-start | bytes 393224 | tf_op jit(solution)/shard_map/ppermute | solution.py:237
  72.1 8.5 %collective-permute-start.2 = (bf16[2,4,64,128]{3,2,1,0:T(8,128)(2,1)S(1)}, bf16[2,4,64,128]{3,2,1,0:T(8,128)(2,1)S(1)}, u32[]{:S(2)}, u32[]{:S(2)}) collective-permute-start(bf16[2,4,64,128]{3,2,1,0:T(8,128)(2,1)S(1)} %bitcast.8), channel_id=1, source_target_pairs={{0,4},{2,6},{4,0},{6,2},{1,5},{3,7},{5,1},{7,3},{8,12},{10,14},{12... | collective-permute-start | bytes 393224 | tf_op jit(solution)/shard_map/ppermute | solution.py:237
  76.4 8.1 %collective-permute-start.3 = (bf16[2,4,64,128]{3,2,1,0:T(8,128)(2,1)S(1)}, bf16[2,4,64,128]{3,2,1,0:T(8,128)(2,1)S(1)}, u32[]{:S(2)}, u32[]{:S(2)}) collective-permute-start(bf16[2,4,64,128]{3,2,1,0:T(8,128)(2,1)S(1)} %bitcast.9), channel_id=1, source_target_pairs={{0,6},{2,0},{4,2},{6,4},{1,7},{3,1},{5,3},{7,5},{8,14},{10,8},{12,... | collective-permute-start | bytes 393224 | tf_op jit(solution)/shard_map/ppermute | solution.py:237
  85.5 21.8 %all-to-all-start.2 = ((bf16[16,32,128]{2,1,0:T(8,128)(2,1)}), bf16[16,32,128]{2,1,0:T(8,128)(2,1)S(1)}, u32[]{:S(2)}, u32[]{:S(2)}) async-start(bf16[16,32,128]{2,1,0:T(8,128)(2,1)} %get-tuple-element.41), calls=%async_computation.2 | async-start | bytes 262144 | tf_op jit(solution)/shard_map/all_to_all | solution.py:254
  92.0 11.9 %collective-permute-start.4 = (bf16[256,128]{1,0:T(8,128)(2,1)S(1)}, bf16[256,128]{1,0:T(8,128)(2,1)S(1)}, u32[]{:S(2)}, u32[]{:S(2)}) collective-permute-start(bf16[256,128]{1,0:T(8,128)(2,1)S(1)} %get-tuple-element.38), channel_id=1, source_target_pairs={{0,8},{8,16},{16,24},{24,0},{1,9},{9,17},{17,25},{25,1},{2,10},{10... | collective-permute-start | bytes 196616 | tf_op jit(solution)/shard_map/ppermute | solution.py:257
  96.0 8.0 %collective-permute-start.5 = (bf16[256,128]{1,0:T(8,128)(2,1)S(1)}, bf16[256,128]{1,0:T(8,128)(2,1)S(1)}, u32[]{:S(2)}, u32[]{:S(2)}) collective-permute-start(bf16[256,128]{1,0:T(8,128)(2,1)S(1)} %get-tuple-element.39), channel_id=1, source_target_pairs={{0,16},{8,24},{16,0},{24,8},{1,17},{9,25},{17,1},{25,9},{2,18},{10... | collective-permute-start | bytes 196616 | tf_op jit(solution)/shard_map/ppermute | solution.py:257
  100.5 6.2 %collective-permute-start.6 = (bf16[256,128]{1,0:T(8,128)(2,1)S(1)}, bf16[256,128]{1,0:T(8,128)(2,1)S(1)}, u32[]{:S(2)}, u32[]{:S(2)}) collective-permute-start(bf16[256,128]{1,0:T(8,128)(2,1)S(1)} %get-tuple-element.40), channel_id=1, source_target_pairs={{0,24},{8,0},{16,8},{24,16},{1,25},{9,1},{17,9},{25,17},{2,26},{10... | collective-permute-start | bytes 196616 | tf_op jit(solution)/shard_map/ppermute | solution.py:257

commit v13 on v12

--- a/solution.py
+++ b/solution.py
@@ -134,6 +134,13 @@
         dv[...] += more[1]
 
     def over(step, start, end):
+        eights = (end - start) // NP
+
+        @pl.when(eights == 1)
+        def _():
+            step(0, NP)
+
+        start = start + NP * eights
         fours = (end - start) // 4
 
         def four(i, carry):
@@ -235,7 +242,7 @@
     xts = [xt]
     for d in range(1, NX):
         xts.append(lax.ppermute(xt, "x", [(i, (i + d) % NX) for i in range(NX)]))
-    recv, xts[0] = lax.optimization_barrier((recv, xts[0]))
+    recv, *xts[:2] = lax.optimization_barrier((recv, *xts[:2]))
     relayed = lax.ppermute(recv, "zl", [(0, 1), (1, 0)])
     block = (NY * T, H)
     sums = call(first_body, [(block, f32)] * 3, [], 2)(in_vmem(recv), in_vmem(grp))

time: 109 us -> 106 us (0.972)
  waiting for transfers between devices: 33.6 us -> 31.3 us
    all_to_all x1, waiting for transfers between devices: 16.1 us -> 8.62 us  [per_device(): lax.all_to_all(zsend, ('zp', 'zl'), 0, 0, axis_index_groups=GROUPS, tiled...]
    ppermute x3, waiting for transfers between devices: 6.14 us -> 11.2 us  [per_device(): xts.append(lax.ppermute(xt, 'x', [(i, (i + d) % NX) for i in range(NX)]))]
  transfers between devices with their start and end apart: 10 -> 10, of which waited for: 5 -> 6; matrix products, arithmetic and copies ran while one was open for 1% -> 1% of each run, Pallas kernels for 2% -> 2%
where the time goes in v13:
time: 106 us; the launch traced here: 105 us
  starting transfers between devices  47.5 us (45%)
  waiting for transfers between devices  31.3 us (30%)
  blocking collectives  15.8 us (15%)
  Pallas kernels  8.01 us (8%)
  other arithmetic  1.3 us (1%)
    all_to_all x1, starting transfers between devices, per_device(): lax.all_to_all(zsend, ('zp', 'zl'), 0, 0, axis_index_groups=GROUPS, tiled...  14.6 us
    all_gather x1, blocking collectives, per_device(): grp = lax.all_gather(own, 'y', axis=0, tiled=False)  13.9 us
    ppermute x3, starting transfers between devices, per_device(): lax.ppermute(kv[d], 'y', [(i, (i + d) % NY) for i in range(NY)])  11.9 us
    ppermute x3, waiting for transfers between devices, per_device(): xts.append(lax.ppermute(xt, 'x', [(i, (i + d) % NX) for i in range(NX)]))  11.2 us
    ppermute x1, waiting for transfers between devices, per_device(): relayed = lax.ppermute(recv, 'zl', [(0, 1), (1, 0)])  8.67 us
    all_to_all x1, waiting for transfers between devices, per_device(): lax.all_to_all(zsend, ('zp', 'zl'), 0, 0, axis_index_groups=GROUPS, tiled...  8.62 us
    ppermute x3, starting transfers between devices, per_device(): xts.append(lax.ppermute(xt, 'x', [(i, (i + d) % NX) for i in range(NX)]))  7.59 us
    all_to_all x1, starting transfers between devices, per_device(): back = lax.all_to_all(zs, ('zp', 'zl'), 0, 0, tiled=True)  6.67 us
  transfers between devices with their start and end apart: 10, of which 6 were waited for; matrix products, arithmetic and copies ran while one was open for 1% of the time, Pallas kernels for 2%

profile of v13, /device:TPU:6, one launch (start us, length us, event | category | flops | bytes accessed | tf_op | source)
XLA Modules:
  0.0 104.6 jit_solution(16807184297954712603)
XLA Ops:
  0.6 2.0 %shard_map.111 = (bf16[8,264,128]{2,1,0:T(8,128)(2,1)}, bf16[784,128]{1,0:T(8,128)(2,1)S(1)}) custom-call(bf16[128,128]{1,0:T(8,128)(2,1)} %q.1, bf16[128,128]{1,0:T(8,128)(2,1)} %k.1, bf16[128,128]{1,0:T(8,128)(2,1)} %v.1, f32[1,128]{1,0:T(1,128)} %bitcast.11, f32[1,128]{1,0:T(1,128)} %bitcast.12, bf16[128,128]{1,0:T(8,128)(2,1)} %o.1, ...), custom_call_target="tpu_custom_call" | custom-call | tf_op jit(solution)/shard_map/pallas_call | solution.py:237
  2.7 14.6 %all-to-all-start = ((bf16[8,264,128]{2,1,0:T(8,128)(2,1)}), bf16[8,264,128]{2,1,0:T(8,128)(2,1)S(1)}, u32[]{:S(2)}, u32[]{:S(2)}) async-start(bf16[8,264,128]{2,1,0:T(8,128)(2,1)} %get-tuple-element.24), calls=%async_computation | async-start | bytes 1081344 | tf_op jit(solution)/shard_map/all_to_all | solution.py:238
  17.3 13.9 %all-gather = bf16[3136,128]{1,0:T(8,128)(2,1)S(1)} all-gather(bf16[784,128]{1,0:T(8,128)(2,1)S(1)} %get-tuple-element.25), channel_id=2, replica_groups=mesh['zp'=8,'zl'=2,'y'=4,'x'=4,'c'=2] {'y'}, dimensions={0}, use_global_device_ids=true | all-gather | bytes 1003520 | tf_op jit(solution)/shard_map/all_gather | solution.py:239
  31.2 1.9 %all-gather.1 = bf16[8,64,128]{2,1,0:T(8,128)(2,1)S(1)} all-gather(bf16[4,64,128]{2,1,0:T(8,128)(2,1)S(1)} %pad_maximum_fusion), channel_id=3, replica_groups=mesh['zp'=8,'zl'=2,'y'=4,'x'=4,'c'=2] {'c'}, dimensions={0}, use_global_device_ids=true | all-gather | bytes 196608 | tf_op jit(solution)/shard_map/all_gather | solution.py:241
  33.1 2.4 %collective-permute-start = (bf16[2,4,64,128]{3,2,1,0:T(8,128)(2,1)S(1)}, bf16[2,4,64,128]{3,2,1,0:T(8,128)(2,1)S(1)}, u32[]{:S(2)}, u32[]{:S(2)}) collective-permute-start(bf16[2,4,64,128]{3,2,1,0:T(8,128)(2,1)S(1)} %bitcast.7), channel_id=1, source_target_pairs={{0,2},{2,4},{4,6},{6,0},{1,3},{3,5},{5,7},{7,1},{8,10},{10,12},{12... | collective-permute-start | bytes 393224 | tf_op jit(solution)/shard_map/ppermute | solution.py:244
  35.5 5.1 %collective-permute-done.rest_1_ = bf16[2,4,64,128]{3,2,1,0:T(8,128)(2,1)S(1)} collective-permute-done((bf16[2,4,64,128]{3,2,1,0:T(8,128)(2,1)S(1)}, bf16[2,4,64,128]{3,2,1,0:T(8,128)(2,1)S(1)}, u32[]{:S(2)}, u32[]{:S(2)}) %collective-permute-start) | collective-permute-done | bytes 131104 | tf_op jit(solution)/shard_map/ppermute | solution.py:244
  40.5 8.6 %all-to-all-done.recv = bf16[8,264,128]{2,1,0:T(8,128)(2,1)S(1)} async-done(((bf16[8,264,128]{2,1,0:T(8,128)(2,1)}), bf16[8,264,128]{2,1,0:T(8,128)(2,1)S(1)}, u32[]{:S(2)}, u32[]{:S(2)}) %all-to-all-start) | async-done | bytes 540704 | tf_op jit(solution)/shard_map/all_to_all | solution.py:238
  49.2 2.3 %collective-permute-start.1 = (bf16[8,264,128]{2,1,0:T(8,128)(2,1)S(1)}, bf16[8,264,128]{2,1,0:T(8,128)(2,1)S(1)}, u32[]{:S(2)}, u32[]{:S(2)}) collective-permute-start(bf16[8,264,128]{2,1,0:T(8,128)(2,1)S(1)} %all-to-all-done.recv), channel_id=1, source_target_pairs={{0,32},{32,0},{1,33},{33,1},{2,34},{34,2},{3,35},{35,3},{4,36},{36... | collective-permute-start | bytes 1622024 | tf_op jit(solution)/shard_map/ppermute | solution.py:246
  51.5 2.4 %shard_map.112 = (f32[512,128]{1,0:T(8,128)S(1)}, f32[512,128]{1,0:T(8,128)S(1)}, f32[512,128]{1,0:T(8,128)S(1)}) custom-call(bf16[8,264,128]{2,1,0:T(8,128)(2,1)S(1)} %all-to-all-done.recv, bf16[4,784,128]{2,1,0:T(8,128)(2,1)S(1)} %bitcast.5), custom_call_target="tpu_custom_call" | custom-call | tf_op jit(solution)/shard_map/pallas_call | solution.py:248
  53.9 8.7 %collective-permute-done.1.recv = bf16[8,264,128]{2,1,0:T(8,128)(2,1)S(1)} collective-permute-done((bf16[8,264,128]{2,1,0:T(8,128)(2,1)S(1)}, bf16[8,264,128]{2,1,0:T(8,128)(2,1)S(1)}, u32[]{:S(2)}, u32[]{:S(2)}) %collective-permute-start.1) | collective-permute-done | bytes 540704 | tf_op jit(solution)/shard_map/ppermute | solution.py:246
  62.5 2.5 %shard_map.113 = (bf16[4,512,128]{2,1,0:T(8,128)(2,1)}, bf16[256,128]{1,0:T(8,128)(2,1)S(1)}, bf16[256,128]{1,0:T(8,128)(2,1)S(1)}, bf16[256,128]{1,0:T(8,128)(2,1)S(1)}, bf16[256,128]{1,0:T(8,128)(2,1)S(1)}) custom-call(bf16[8,264,128]{2,1,0:T(8,128)(2,1)S(1)} %collective-permute-done.1.recv, bf16[4,784,128]{2,1,0:T(8,128)(2,1)S(1)} %bitcast.6, ...), custom_call_target="tpu_custom_call" | custom-call | tf_op jit(solution)/shard_map/pallas_call | solution.py:255
  65.1 4.5 %all-to-all-start.1 = ((bf16[4,512,128]{2,1,0:T(8,128)(2,1)}), bf16[4,512,128]{2,1,0:T(8,128)(2,1)S(1)}, u32[]{:S(2)}, u32[]{:S(2)}) async-start(bf16[4,512,128]{2,1,0:T(8,128)(2,1)} %get-tuple-element.30), calls=%async_computation.1 | async-start | bytes 1048576 | tf_op jit(solution)/shard_map/all_to_all | solution.py:256
  69.5 3.3 %collective-permute-start.2 = (bf16[2,4,64,128]{3,2,1,0:T(8,128)(2,1)S(1)}, bf16[2,4,64,128]{3,2,1,0:T(8,128)(2,1)S(1)}, u32[]{:S(2)}, u32[]{:S(2)}) collective-permute-start(bf16[2,4,64,128]{3,2,1,0:T(8,128)(2,1)S(1)} %bitcast.8), channel_id=1, source_target_pairs={{0,4},{2,6},{4,0},{6,2},{1,5},{3,7},{5,1},{7,3},{8,12},{10,14},{12... | collective-permute-start | bytes 393224 | tf_op jit(solution)/shard_map/ppermute | solution.py:244
  72.8 1.9 %collective-permute-start.3 = (bf16[2,4,64,128]{3,2,1,0:T(8,128)(2,1)S(1)}, bf16[2,4,64,128]{3,2,1,0:T(8,128)(2,1)S(1)}, u32[]{:S(2)}, u32[]{:S(2)}) collective-permute-start(bf16[2,4,64,128]{3,2,1,0:T(8,128)(2,1)S(1)} %bitcast.9), channel_id=1, source_target_pairs={{0,6},{2,0},{4,2},{6,4},{1,7},{3,1},{5,3},{7,5},{8,14},{10,8},{12,... | collective-permute-start | bytes 393224 | tf_op jit(solution)/shard_map/ppermute | solution.py:244
  74.8 3.1 %collective-permute-done.2.rest_2_ = bf16[2,4,64,128]{3,2,1,0:T(8,128)(2,1)S(1)} collective-permute-done((bf16[2,4,64,128]{3,2,1,0:T(8,128)(2,1)S(1)}, bf16[2,4,64,128]{3,2,1,0:T(8,128)(2,1)S(1)}, u32[]{:S(2)}, u32[]{:S(2)}) %collective-permute-start.2) | collective-permute-done | bytes 131104 | tf_op jit(solution)/shard_map/ppermute | solution.py:244
  77.9 3.0 %collective-permute-done.3.rest_3_ = bf16[2,4,64,128]{3,2,1,0:T(8,128)(2,1)S(1)} collective-permute-done((bf16[2,4,64,128]{3,2,1,0:T(8,128)(2,1)S(1)}, bf16[2,4,64,128]{3,2,1,0:T(8,128)(2,1)S(1)}, u32[]{:S(2)}, u32[]{:S(2)}) %collective-permute-start.3) | collective-permute-done | bytes 131104 | tf_op jit(solution)/shard_map/ppermute | solution.py:244
  80.9 0.0 all-to-all-done.1.sums
  80.9 1.0 shard_map.114
  81.9 6.7 %all-to-all-start.2 = ((bf16[16,32,128]{2,1,0:T(8,128)(2,1)}), bf16[16,32,128]{2,1,0:T(8,128)(2,1)S(1)}, u32[]{:S(2)}, u32[]{:S(2)}) async-start(bf16[16,32,128]{2,1,0:T(8,128)(2,1)} %get-tuple-element.43), calls=%async_computation.2 | async-start | bytes 262144 | tf_op jit(solution)/shard_map/all_to_all | solution.py:261
  88.6 3.9 %collective-permute-start.4 = (bf16[256,128]{1,0:T(8,128)(2,1)S(1)}, bf16[256,128]{1,0:T(8,128)(2,1)S(1)}, u32[]{:S(2)}, u32[]{:S(2)}) collective-permute-start(bf16[256,128]{1,0:T(8,128)(2,1)S(1)} %get-tuple-element.40), channel_id=1, source_target_pairs={{0,8},{8,16},{16,24},{24,0},{1,9},{9,17},{17,25},{25,1},{2,10},{10... | collective-permute-start | bytes 196616 | tf_op jit(solution)/shard_map/ppermute | solution.py:264
  92.6 4.6 %collective-permute-start.5 = (bf16[256,128]{1,0:T(8,128)(2,1)S(1)}, bf16[256,128]{1,0:T(8,128)(2,1)S(1)}, u32[]{:S(2)}, u32[]{:S(2)}) collective-permute-start(bf16[256,128]{1,0:T(8,128)(2,1)S(1)} %get-tuple-element.41), channel_id=1, source_target_pairs={{0,16},{8,24},{16,0},{24,8},{1,17},{9,25},{17,1},{25,9},{2,18},{10... | collective-permute-start | bytes 196616 | tf_op jit(solution)/shard_map/ppermute | solution.py:264
  97.1 3.4 %collective-permute-start.6 = (bf16[256,128]{1,0:T(8,128)(2,1)S(1)}, bf16[256,128]{1,0:T(8,128)(2,1)S(1)}, u32[]{:S(2)}, u32[]{:S(2)}) collective-permute-start(bf16[256,128]{1,0:T(8,128)(2,1)S(1)} %get-tuple-element.42), channel_id=1, source_target_pairs={{0,24},{8,0},{16,8},{24,16},{1,25},{9,1},{17,9},{25,17},{2,26},{10... | collective-permute-start | bytes 196616 | tf_op jit(solution)/shard_map/ppermute | solution.py:264
  100.5 0.0 collective-permute-done.4
  100.5 0.0 collective-permute-done.5
  100.5 2.8 %collective-permute-done.6 = bf16[256,128]{1,0:T(8,128)(2,1)S(1)} collective-permute-done((bf16[256,128]{1,0:T(8,128)(2,1)S(1)}, bf16[256,128]{1,0:T(8,128)(2,1)S(1)}, u32[]{:S(2)}, u32[]{:S(2)}) %collective-permute-start.6) | collective-permute-done | bytes 65568 | tf_op jit(solution)/shard_map/ppermute | solution.py:264
  103.3 0.7 add_convert_fusion
  104.0 0.0 all-to-all-done.2
  104.0 0.6 convert_reduce_fusion
  (2 shorter events, 0.0 us)
Async XLA Ops:
  2.7 46.5 %all-to-all-start = ((bf16[8,264,128]{2,1,0:T(8,128)(2,1)}), bf16[8,264,128]{2,1,0:T(8,128)(2,1)S(1)}, u32[]{:S(2)}, u32[]{:S(2)}) async-start(bf16[8,264,128]{2,1,0:T(8,128)(2,1)} %get-tuple-element.24), calls=%async_computation | async-start | bytes 1081344 | tf_op jit(solution)/shard_map/all_to_all | solution.py:238
  33.1 7.4 %collective-permute-start = (bf16[2,4,64,128]{3,2,1,0:T(8,128)(2,1)S(1)}, bf16[2,4,64,128]{3,2,1,0:T(8,128)(2,1)S(1)}, u32[]{:S(2)}, u32[]{:S(2)}) collective-permute-start(bf16[2,4,64,128]{3,2,1,0:T(8,128)(2,1)S(1)} %bitcast.7), channel_id=1, source_target_pairs={{0,2},{2,4},{4,6},{6,0},{1,3},{3,5},{5,7},{7,1},{8,10},{10,12},{12... | collective-permute-start | bytes 393224 | tf_op jit(solution)/shard_map/ppermute | solution.py:244
  49.2 13.4 %collective-permute-start.1 = (bf16[8,264,128]{2,1,0:T(8,128)(2,1)S(1)}, bf16[8,264,128]{2,1,0:T(8,128)(2,1)S(1)}, u32[]{:S(2)}, u32[]{:S(2)}) collective-permute-start(bf16[8,264,128]{2,1,0:T(8,128)(2,1)S(1)} %all-to-all-done.recv), channel_id=1, source_target_pairs={{0,32},{32,0},{1,33},{33,1},{2,34},{34,2},{3,35},{35,3},{4,36},{36... | collective-permute-start | bytes 1622024 | tf_op jit(solution)/shard_map/ppermute | solution.py:246
  65.1 15.8 %all-to-all-start.1 = ((bf16[4,512,128]{2,1,0:T(8,128)(2,1)}), bf16[4,512,128]{2,1,0:T(8,128)(2,1)S(1)}, u32[]{:S(2)}, u32[]{:S(2)}) async-start(bf16[4,512,128]{2,1,0:T(8,128)(2,1)} %get-tuple-element.30), calls=%async_computation.1 | async-start | bytes 1048576 | tf_op jit(solution)/shard_map/all_to_all | solution.py:256
  69.5 8.4 %collective-permute-start.2 = (bf16[2,4,64,128]{3,2,1,0:T(8,128)(2,1)S(1)}, bf16[2,4,64,128]{3,2,1,0:T(8,128)(2,1)S(1)}, u32[]{:S(2)}, u32[]{:S(2)}) collective-permute-start(bf16[2,4,64,128]{3,2,1,0:T(8,128)(2,1)S(1)} %bitcast.8), channel_id=1, source_target_pairs={{0,4},{2,6},{4,0},{6,2},{1,5},{3,7},{5,1},{7,3},{8,12},{10,14},{12... | collective-permute-start | bytes 393224 | tf_op jit(solution)/shard_map/ppermute | solution.py:244
  72.8 8.1 %collective-permute-start.3 = (bf16[2,4,64,128]{3,2,1,0:T(8,128)(2,1)S(1)}, bf16[2,4,64,128]{3,2,1,0:T(8,128)(2,1)S(1)}, u32[]{:S(2)}, u32[]{:S(2)}) collective-permute-start(bf16[2,4,64,128]{3,2,1,0:T(8,128)(2,1)S(1)} %bitcast.9), channel_id=1, source_target_pairs={{0,6},{2,0},{4,2},{6,4},{1,7},{3,1},{5,3},{7,5},{8,14},{10,8},{12,... | collective-permute-start | bytes 393224 | tf_op jit(solution)/shard_map/ppermute | solution.py:244
  81.9 22.0 %all-to-all-start.2 = ((bf16[16,32,128]{2,1,0:T(8,128)(2,1)}), bf16[16,32,128]{2,1,0:T(8,128)(2,1)S(1)}, u32[]{:S(2)}, u32[]{:S(2)}) async-start(bf16[16,32,128]{2,1,0:T(8,128)(2,1)} %get-tuple-element.43), calls=%async_computation.2 | async-start | bytes 262144 | tf_op jit(solution)/shard_map/all_to_all | solution.py:261
  88.6 11.9 %collective-permute-start.4 = (bf16[256,128]{1,0:T(8,128)(2,1)S(1)}, bf16[256,128]{1,0:T(8,128)(2,1)S(1)}, u32[]{:S(2)}, u32[]{:S(2)}) collective-permute-start(bf16[256,128]{1,0:T(8,128)(2,1)S(1)} %get-tuple-element.40), channel_id=1, source_target_pairs={{0,8},{8,16},{16,24},{24,0},{1,9},{9,17},{17,25},{25,1},{2,10},{10... | collective-permute-start | bytes 196616 | tf_op jit(solution)/shard_map/ppermute | solution.py:264
  92.6 8.0 %collective-permute-start.5 = (bf16[256,128]{1,0:T(8,128)(2,1)S(1)}, bf16[256,128]{1,0:T(8,128)(2,1)S(1)}, u32[]{:S(2)}, u32[]{:S(2)}) collective-permute-start(bf16[256,128]{1,0:T(8,128)(2,1)S(1)} %get-tuple-element.41), channel_id=1, source_target_pairs={{0,16},{8,24},{16,0},{24,8},{1,17},{9,25},{17,1},{25,9},{2,18},{10... | collective-permute-start | bytes 196616 | tf_op jit(solution)/shard_map/ppermute | solution.py:264
  97.1 6.2 %collective-permute-start.6 = (bf16[256,128]{1,0:T(8,128)(2,1)S(1)}, bf16[256,128]{1,0:T(8,128)(2,1)S(1)}, u32[]{:S(2)}, u32[]{:S(2)}) collective-permute-start(bf16[256,128]{1,0:T(8,128)(2,1)S(1)} %get-tuple-element.42), channel_id=1, source_target_pairs={{0,24},{8,0},{16,8},{24,16},{1,25},{9,1},{17,9},{25,17},{2,26},{10... | collective-permute-start | bytes 196616 | tf_op jit(solution)/shard_map/ppermute | solution.py:264
